TPU v7x, 512 devices: a whole 4x8x8 slice. The times are simulated.
512 devices in a mesh: fs: 64 (over z, y), tp: 8 (over x, core).
Axes of the slice: x: 4, y: 8, z: 8, core: 2. Of those that a mesh axis runs over, the one named last changes fastest.
Arguments:
- inputs: bfloat16 [32768, 2048], P('fs', 'tp'), may hold values from -6 to 6
- hidden_pre: bfloat16 [32768, 4096], P('fs', 'tp'), may hold values from -6 to 6
- norm_input: bfloat16 [32768, 2048], P('fs', 'tp'), may hold values from -48 to 48, as said below
- out_gain: float32 [2048], P('tp'), may hold values from 0.1 to 1.9
- w_up: bfloat16 [2048, 4096], P('tp', 'fs'), may hold values from -0.125 to 0.125
- w_down: bfloat16 [4096, 2048], P('tp', 'fs'), may hold values from -0.09375 to 0.09375
- cotangent: bfloat16 [32768, 2048], P('fs', 'tp'), may hold values from -16 to 16
Outputs:
- grad_input: bfloat16 [32768, 2048], P('fs', 'tp')
- grad_up: float32 [2048, 4096], P('tp', 'fs')
- grad_gain: float32 [2048], P('tp')
Inputs may be any that keep to these rules, and one draw needn't show every extreme that they name: `norm_input`: each token's features are scaled by a factor of that token, and each block of 2048 / 8 features by a factor of that block.
All inputs are finite; a program needn't handle non-finite values.
Results may differ from a plain program's by a relative error of at most 0.0058.
Values may be sent and summed in bfloat16 or wider, within the bound.
No kernel may reach another device: no remote copies, remote signals or barrier semaphores. Data moves between devices by JAX's collectives and lax.ppermute only.
A program may use at most 64 MiB of HBM per device.

v0:
```python
import jax
import jax.numpy as jnp
from jax import lax
from jax.sharding import Mesh
from jax.sharding import PartitionSpec as P

FS = ("fs_0", "fs_1")


norm_eps = 1e-06


def from_everyone(value, axis):
    devices = lax.axis_size(axis)
    return lax.all_to_all(
        jnp.broadcast_to(value[None], (devices, *value.shape)), axis, 0, 0, tiled=True
    )


def taken_together(value, axis):
    everything = from_everyone(value, axis)
    return jnp.sum(everything, axis=0)


def in_one(arrays, axis):
    ends = [0]
    for a in arrays:
        ends.append(ends[-1] + a.size)
    total = taken_together(jnp.concatenate([a.ravel() for a in arrays]), axis)
    return tuple((total[b:e].reshape(a.shape) for a, b, e in zip(arrays, ends, ends[1:])))


def one_axis_at_a_time(value, axes):
    for axis in axes:
        value = lax.psum(value, axis)
    return value


def joined_along(parts, dim):
    parts = jnp.moveaxis(parts, 0, dim)
    dims = parts.shape
    return parts.reshape(*dims[:dim], dims[dim] * dims[dim + 1], *dims[dim + 2 :])


def gather_directly(value, axis, dim):
    parts = from_everyone(value, axis)
    return joined_along(parts, dim)


def stacked_from(value, axes, order):
    parts = value[None]
    for k in order:
        parts = lax.all_gather(parts, axes[k], axis=0, tiled=True)
    block = [lax.axis_size(axes[k]) for k in reversed(order)]
    parts = parts.reshape(*block, *value.shape)
    turned = sorted(range(len(order)), key=lambda place: order[len(order) - 1 - place])
    return parts.transpose(*turned, *range(len(order), parts.ndim)).reshape(-1, *value.shape)


def gather_axes(value, axes, order, dim):
    return joined_along(stacked_from(value, axes, order), dim)


def summed_rows(value, axes, dim):
    for axis in axes:
        value = lax.psum_scatter(value, axis, scatter_dimension=dim, tiled=True)
    return value


def on_device(inputs, hidden_pre, norm_input, out_gain, w_up, w_down, cotangent):
    tok_rows = inputs.shape[0]
    width = inputs.shape[1] * lax.axis_size("tp")
    scaled = (tok_rows * lax.axis_size(FS)) ** (-0.5)
    normed = norm_input.astype(jnp.float32)
    upstream = cotangent.astype(jnp.float32)
    weighted = upstream * out_gain
    square_sum, cross_sum = in_one(
        (jnp.sum(normed * normed, axis=1), jnp.sum(weighted * normed, axis=1)), "tp"
    )
    inv_rms = lax.rsqrt(square_sum / width + norm_eps)[:, None]
    cross_mean = (cross_sum / width)[:, None]
    d_out = (weighted * inv_rms - normed * inv_rms * inv_rms * inv_rms * cross_mean).astype(
        jnp.bfloat16
    )
    grad_gain = one_axis_at_a_time(jnp.sum(upstream * normed * inv_rms, axis=0) * scaled, FS)
    out_full = gather_directly(d_out, "tp", 1)
    columns = out_full
    d_act = lax.dot_general(
        columns,
        gather_axes(w_down, FS, (0, 1), 1),
        (((1,), (1,)), ((), ())),
        preferred_element_type=jnp.float32,
    )
    d_pre = (d_act * 2.0 * jax.nn.relu(hidden_pre.astype(jnp.float32))).astype(jnp.bfloat16)
    hidden_full = lax.all_gather(d_pre, "tp", axis=1, tiled=True)
    columns = hidden_full
    grad_input = lax.dot_general(
        columns,
        lax.all_gather(w_up, FS, axis=1, tiled=True),
        (((1,), (1,)), ((), ())),
        preferred_element_type=jnp.float32,
    ).astype(jnp.bfloat16)
    whole_term = (
        lax.dot_general(
            hidden_full, inputs, (((0,), (0,)), ((), ())), preferred_element_type=jnp.float32
        )
        * scaled
    )
    grad_up = summed_rows(whole_term, FS, 0).T
    return (grad_input, grad_up, grad_gain)


def solution(mesh):
    torus = Mesh(mesh.devices.reshape(8, 8, mesh.shape["tp"]), ("fs_0", "fs_1", "tp"))
    in_specs = (
        P(FS, "tp"),
        P(FS, "tp"),
        P(FS, "tp"),
        P("tp"),
        P("tp", FS),
        P("tp", FS),
        P(FS, "tp"),
    )
    out_specs = (P(FS, "tp"), P("tp", FS), P("tp"))
    return jax.shard_map(
        on_device, mesh=torus, in_specs=in_specs, out_specs=out_specs, check_vma=False
    )
```

profile of v0, /device:TPU:6, one launch (start us, length us, event | category | flops | bytes accessed | tf_op | source)
XLA Modules:
  0.0 246.0 jit_solution(17596367826111091204)
XLA Ops:
  8.0 0.0 copy-start
  8.0 0.0 all-gather.5.cloned.1.call-start
  8.1 31.5 %all-gather = bf16[4096,32]{0,1:T(8,128)(2,1)S(1)} all-gather(bf16[512,32]{0,1:T(8,128)(2,1)} %param.12), channel_id=2, replica_groups=mesh['fs_0'=8,'fs_1'=8,'tp'=8] {'fs_0'}, dimensions={0}, use_global_device_ids=true | all-gather | bytes 294912 | tf_op jit(solution)/shard_map/all_gather | solution.py:53
  39.5 0.8 copy.27
  40.3 0.0 all-gather.5.cloned.1.call-update
  40.4 1.3 fusion.5
  41.7 8.0 %all_to_all.11 = f32[8,1,1024]{2,1,0:T(1,128)S(1)} all-to-all(f32[8,1,1024]{2,1,0:T(1,128)S(1)} %broadcast_in_dim.6), channel_id=1, replica_groups=mesh['fs_0'=8,'fs_1'=8,'tp'=8] {'tp'}, dimensions={0} | all-to-all | bytes 65536 | tf_op jit(solution)/shard_map/all_to_all | solution.py:15
  49.7 1.3 fusion.11
  51.0 0.1 copy.20
  51.1 1.5 broadcast_in_dim.7
  52.6 5.6 %all-to-all-start.1 = ((bf16[8,512,256]{1,2,0:T(8,128)(2,1)}), bf16[8,512,256]{1,2,0:T(8,128)(2,1)S(1)}, u32[]{:S(2)}, u32[]{:S(2)}) async-start(bf16[8,512,256]{1,2,0:T(8,128)(2,1)} %broadcast_in_dim.7), calls=%async_computation.1 | async-start | bytes 4194304 | tf_op jit(solution)/shard_map/all_to_all | solution.py:15
  58.2 0.0 all-gather.7.cloned.1.call-start
  58.2 24.0 %all-gather.5.cloned.1.call-done = bf16[64,512,32]{1,0,2:T(8,128)(2,1)} async-done(((bf16[8,512,32]{1,0,2:T(8,128)(2,1)}), bf16[64,512,32]{1,0,2:T(8,128)(2,1)}) %all-gather.5.cloned.1.call-update) | async-done | bytes 2097168 | tf_op jit(solution)/shard_map/all_gather | solution.py:53
  82.2 0.0 copy-start.1
  82.2 4.2 %copy.22 = bf16[8,8,512,32]{2,3,1,0:T(8,128)(2,1)} copy(bf16[8,8,512,32]{2,0,1,3:T(8,128)(2,1)} %bitcast.22) | data formatting | bytes 4194304 | tf_op jit(solution)/shard_map/transpose | solution.py:57
  86.4 0.0 all-to-all-done.1
  86.4 0.0 copy-done.1
  86.4 3.7 %fusion.1 = bf16[512,512]{1,0:T(8,128)(2,1)} fusion(bf16[512,2048]{0,1:T(8,128)(2,1)S(1)} %bitcast.23, bf16[512,2048]{0,1:T(8,128)(2,1)} %bitcast.24, bf16[512,512]{1,0:T(8,128)(2,1)S(1)} %copy-done.1), kind=kOutput, calls=%fused_computation.3 | convolution fusion | flops 1075052544 | bytes 5242880 | tf_op jit(solution)/shard_map/dot_general | solution.py:88
  90.1 0.0 all-gather.7.cloned.1.call-update
  90.1 0.0 reduce-scatter.3.cloned.1.call-start
  90.2 34.4 %all-gather.7.cloned.1.call-done = bf16[512,4096]{1,0:T(8,128)(2,1)} async-done(((bf16[512,512]{1,0:T(8,128)(2,1)}), bf16[512,4096]{1,0:T(8,128)(2,1)}) %all-gather.7.cloned.1.call-update) | async-done | bytes 4194320 | tf_op jit(solution)/shard_map/all_gather | solution.py:95
  124.6 0.0 copy-done
  124.6 5.4 %convolution_multiply_fusion = f32[4096,256]{1,0:T(8,128)} fusion(bf16[512,4096]{1,0:T(8,128)(2,1)} %all-gather.7.cloned.1.call-done, bf16[512,256]{1,0:T(8,128)(2,1)S(1)} %copy-done), kind=kOutput, calls=%fused_computation | convolution fusion | flops 1074790400 | bytes 8650752 | tf_op jit(solution)/shard_map/dot_general | solution.py:104
  130.0 0.0 reduce-scatter.3.cloned.1.call-update
  130.0 0.0 all-gather.9.cloned.1.call-start
  130.1 0.5 all-gather.9.cloned.1.call-update
  130.6 0.0 reduce-scatter.5.cloned.1.call-start
  130.7 61.3 %reduce-scatter.3.cloned.1.call-done = f32[512,256]{1,0:T(8,128)} async-done(((f32[4096,256]{1,0:T(8,128)}), f32[512,256]{1,0:T(8,128)}) %reduce-scatter.3.cloned.1.call-update) | async-done | bytes 524304 | tf_op jit(solution)/shard_map/reduce_scatter | solution.py:66
  192.0 0.0 reduce-scatter.5.cloned.1.call-update
  192.0 15.4 %psum.14 = f32[256]{0:T(256)S(1)} all-reduce(f32[256]{0:T(256)S(1)} %broadcast_multiply_fusion), channel_id=1, replica_groups=mesh['fs_0'=8,'fs_1'=8,'tp'=8] {'fs_0'}, use_global_device_ids=true, to_apply=%region_6.7 | all-reduce | flops 256 | bytes 2048 | tf_op jit(solution)/shard_map/psum | solution.py:35
  207.4 17.6 %psum.15 = f32[256]{0:T(256)} all-reduce(f32[256]{0:T(256)S(1)} %psum.14), channel_id=1, replica_groups=mesh['fs_0'=8,'fs_1'=8,'tp'=8] {'fs_1'}, use_global_device_ids=true, to_apply=%region_7.8 | all-reduce | flops 256 | bytes 2048 | tf_op jit(solution)/shard_map/psum | solution.py:35
  225.1 9.0 %all-gather.9.cloned.1.call-done = bf16[256,4096]{0,1:T(8,128)(2,1)} async-done(((bf16[256,64]{0,1:T(8,128)(2,1)}), bf16[256,4096]{0,1:T(8,128)(2,1)}) %all-gather.9.cloned.1.call-update) | async-done | bytes 2097168 | tf_op jit(solution)/shard_map/all_gather | solution.py:99
  234.1 4.8 %convolution_convert_fusion = bf16[512,256]{1,0:T(8,128)(2,1)} fusion(bf16[512,4096]{1,0:T(8,128)(2,1)} %all-gather.7.cloned.1.call-done, bf16[256,4096]{0,1:T(8,128)(2,1)} %all-gather.9.cloned.1.call-done), kind=kOutput, calls=%fused_computation.4 | convolution fusion | flops 1073872896 | bytes 6553600 | tf_op jit(solution)/shard_map/dot_general | solution.py:97
  238.9 0.0 reduce-scatter.5.cloned.1.call-done
  (5 shorter events, 0.1 us)
Async XLA Ops:
  8.0 116.6 %copy-start = (bf16[512,256]{1,0:T(8,128)(2,1)S(1)}, bf16[512,256]{1,0:T(8,128)(2,1)}, u32[]{:S(2)}) copy-start(bf16[512,256]{1,0:T(8,128)(2,1)} %param.7) | copy-start | bytes 786436
  8.0 74.2 %all-gather.5.cloned.1.call-start = ((), (), s32[]{:S(2)}) async-start(), calls=%async_computation.4 | async-start | bytes 2359296 | tf_op jit(solution)/shard_map/all_gather | solution.py:53
  52.6 33.8 %all-to-all-start.1 = ((bf16[8,512,256]{1,2,0:T(8,128)(2,1)}), bf16[8,512,256]{1,2,0:T(8,128)(2,1)S(1)}, u32[]{:S(2)}, u32[]{:S(2)}) async-start(bf16[8,512,256]{1,2,0:T(8,128)(2,1)} %broadcast_in_dim.7), calls=%async_computation.1 | async-start | bytes 4194304 | tf_op jit(solution)/shard_map/all_to_all | solution.py:15
  58.2 66.3 %all-gather.7.cloned.1.call-start = ((), (), s32[]{:S(2)}) async-start(), calls=%async_computation.5 | async-start | bytes 4718592 | tf_op jit(solution)/shard_map/all_gather | solution.py:95
  82.2 4.2 %copy-start.1 = (bf16[512,512]{1,0:T(8,128)(2,1)S(1)}, bf16[512,512]{1,0:T(8,128)(2,1)}, u32[]{:S(2)}) copy-start(bf16[512,512]{1,0:T(8,128)(2,1)} %param.8) | copy-start | bytes 1572868
  90.1 101.9 %reduce-scatter.3.cloned.1.call-start = ((), (), s32[]{:S(2)}) async-start(), calls=%async_computation.7 | async-start | bytes 4718592 | tf_op jit(solution)/shard_map/reduce_scatter | solution.py:66
  130.0 104.0 %all-gather.9.cloned.1.call-start = ((), (), s32[]{:S(2)}) async-start(), calls=%async_computation.6 | async-start | bytes 2129920 | tf_op jit(solution)/shard_map/all_gather | solution.py:99
  130.6 108.3 %reduce-scatter.5.cloned.1.call-start = ((), (), s32[]{:S(2)}) async-start(), calls=%async_computation.8 | async-start | bytes 589824 | tf_op jit(solution)/shard_map/reduce_scatter | solution.py:66
Sparse Core Ops, SparseCore 0:
  40.5 41.7 all-gather.4
  90.2 34.2 all-gather.6
  130.1 61.7 reduce-scatter.2
  195.2 38.8 reduce-scatter.4
Sparse Core Ops, SparseCore 1:
  133.6 100.4 all-gather.8
where the time goes:
time: 246 us
  waiting for transfers between devices  129 us (52%)
  blocking collectives  72.5 us (29%)
  between operations  15.3 us (6%)
  matrix products  13.9 us (6%)
  local copies, waits for them, and re-layouts  6.63 us (3%)
  starting transfers between devices  5.77 us (2%)
  other arithmetic  2.63 us (1%)
    reduce_scatter x2, waiting for transfers between devices, summed_rows(): value = lax.psum_scatter(value, axis, scatter_dimension=dim, tiled=True)  61.3 us
    all_gather x1, waiting for transfers between devices, on_device(): hidden_full = lax.all_gather(d_pre, 'tp', axis=1, tiled=True)  34.4 us
    psum x2, blocking collectives, one_axis_at_a_time(): value = lax.psum(value, axis)  33.1 us
    all_gather x1, blocking collectives, stacked_from(): parts = lax.all_gather(parts, axes[k], axis=0, tiled=True)  31.5 us
    all_gather x1, waiting for transfers between devices, stacked_from(): parts = lax.all_gather(parts, axes[k], axis=0, tiled=True)  24 us
    all_gather x1, waiting for transfers between devices, on_device(): lax.all_gather(w_up, FS, axis=1, tiled=True)  9 us
    all_to_all x1, blocking collectives, from_everyone(): lax.all_to_all(jnp.broadcast_to(value[None], (devices, *value.shape)), ax...  7.95 us
    all_to_all x1, starting transfers between devices, from_everyone(): lax.all_to_all(jnp.broadcast_to(value[None], (devices, *value.shape)), ax...  5.61 us
  transfers between devices with their start and end apart: 6, of which 4 were waited for; matrix products, arithmetic and copies ran while one was open for 5% of the time, Pallas kernels for 0%

commit v1 on v0

v1 whole, which is shorter than its diff:
```python
import jax
import jax.numpy as jnp
from jax import lax
from jax.experimental import pallas as pl
from jax.sharding import Mesh
from jax.sharding import PartitionSpec as P

FS = ("z", "y")
bf16 = jnp.bfloat16
f32 = jnp.float32
norm_eps = 1e-06


def exchange(chunks, axis):
    return lax.all_to_all(chunks, axis, 0, 0, tiled=True)


def gather_directly(value, axis):
    n = lax.axis_size(axis)
    return exchange(jnp.broadcast_to(value[None], (n, *value.shape)), axis)


def summed(parts):
    return jnp.sum(parts.astype(f32), axis=0)


def after(value, earlier):
    return lax.optimization_barrier((value, earlier))[0]


def grad_up_kernel(dout, wd, hidden, inputs, d_pre_out, g_out):
    blocks, toks, feats = dout.shape
    half = wd.shape[-1]
    for s in range(2):
        cols = slice(s * half, (s + 1) * half)
        acc = jnp.zeros((toks, half), f32)
        for k in range(blocks):
            w = wd[k, :, s].reshape(feats, half)
            acc += jnp.dot(dout[k], w, preferred_element_type=f32)
        pre = jnp.maximum(hidden[:, cols].astype(f32), 0.0)
        d_pre_out[:, cols] = (acc * 2.0 * pre).astype(bf16)
    d_pre_t = d_pre_out[...].T
    for k in range(blocks):
        g_out[k] = jnp.dot(d_pre_t, inputs[k], preferred_element_type=f32).astype(bf16)


def grad_input_kernel(d_pre, w_up, out):
    left = d_pre[...]
    for k in range(out.shape[0]):
        out[k] = jnp.dot(left, w_up[k], preferred_element_type=f32).astype(bf16)


def one_device(inputs, hidden_pre, norm_input, out_gain, w_up, w_down, cotangent):
    nz, ny, ntp = (lax.axis_size(a) for a in ("z", "y", "tp"))
    toks, feats = inputs.shape
    hid = hidden_pre.shape[1]
    width = feats * ntp
    scaled = (toks * nz * ny) ** (-0.5)
    swap = [(a * ntp + b, b * ntp + a) for a in range(nz) for b in range(ntp)]

    normed = norm_input.astype(f32)
    upstream = cotangent.astype(f32)
    weighted = upstream * out_gain
    sums = jnp.stack([jnp.sum(normed * normed, axis=1), jnp.sum(weighted * normed, axis=1)])

    wd = w_down.T
    half = hid // 2
    both = jnp.concatenate([wd[:, :half], wd[:, half:], w_up.T], axis=0)
    both = gather_directly(both, "y")
    wd_rows = 2 * wd.shape[0]
    wd = wd_y = both[:, :wd_rows].reshape(ny * wd_rows, half)
    wd = lax.all_gather(wd, "z", axis=0, tiled=True)
    wd = wd.reshape(nz, ny, 2, wd_rows // 2, half)
    wu = both[:, wd_rows:].reshape(hid, feats)
    wu = lax.ppermute(wu, ("z", "tp"), swap)

    sums = gather_directly(after(sums, wd_y), "tp")
    sums = jnp.sum(sums, axis=0)
    inv_rms = lax.rsqrt(sums[0] / width + norm_eps)[:, None]
    cross_mean = (sums[1] / width)[:, None]
    d_out = (weighted * inv_rms - normed * inv_rms * inv_rms * inv_rms * cross_mean).astype(bf16)
    gain_part = jnp.sum(upstream * normed * inv_rms, axis=0) * scaled
    dout_all = lax.all_gather(d_out, "tp", axis=0, tiled=True)
    dout_all = dout_all.reshape(ntp, toks, feats)
    inputs_all = gather_directly(after(inputs, sums), "tp")
    wu = lax.all_gather(after(wu, inputs_all), "z", axis=0, tiled=True).reshape(nz, hid, feats)

    d_pre, g = pl.pallas_call(
        grad_up_kernel,
        out_shape=(
            jax.ShapeDtypeStruct((toks, hid), bf16),
            jax.ShapeDtypeStruct((nz, hid, feats), bf16),
        ),
        name="grad_up_part",
    )(dout_all, wd, hidden_pre, inputs_all)

    grad_gain = jnp.sum(gather_directly(after(gain_part, d_pre), FS), axis=0)

    g = lax.psum_scatter(g.reshape(nz * hid, feats), "z", scatter_dimension=0, tiled=True)
    g = after(g, grad_gain)
    g = summed(exchange(g.reshape(ny, hid // ny, feats), "y")) * scaled
    grad_up = lax.ppermute(g, ("z", "tp"), swap).T

    part = pl.pallas_call(
        grad_input_kernel,
        out_shape=jax.ShapeDtypeStruct((ntp, toks, feats), bf16),
        name="grad_input_part",
    )(d_pre, wu)
    part = part.reshape(ntp * toks, feats)
    grad_input = lax.psum_scatter(part, "tp", scatter_dimension=0, tiled=True)

    return (grad_input, grad_up, grad_gain)


def solution(mesh):
    torus = Mesh(mesh.devices.reshape(8, 8, mesh.shape["tp"]), ("z", "y", "tp"))
    in_specs = (
        P(FS, "tp"),
        P(FS, "tp"),
        P(FS, "tp"),
        P("tp"),
        P("tp", FS),
        P("tp", FS),
        P(FS, "tp"),
    )
    out_specs = (P(FS, "tp"), P("tp", FS), P("tp"))
    return jax.shard_map(
        one_device, mesh=torus, in_specs=in_specs, out_specs=out_specs, check_vma=False
    )
```

time: 246 us -> 267 us (1.085); the launches traced: 246 us -> 264 us
  matrix products: 13.9 us -> 0 us
  starting transfers between devices: 5.77 us -> 19.6 us
  Pallas kernels: 0 us -> 11.2 us
  waiting for transfers between devices: 129 us -> 140 us
    all_to_all x1 -> x4, blocking collectives: 7.95 us -> 72 us  [exchange(): return lax.all_to_all(chunks, axis, 0, 0, tiled=True)]
    psum x2 -> x0, blocking collectives: 33.1 us -> none  [one_axis_at_a_time(): value = lax.psum(value, axis)]
    reduce_scatter x2, waiting for transfers between devices: 61.3 us -> 29.8 us  [the longest x1 19.7 us: one_device(): lax.psum_scatter(g.reshape(nz * hid, feats), 'z', scatter_dimension=0, ti...]
    all_gather x1 -> x0, blocking collectives: 31.5 us -> none  [stacked_from(): parts = lax.all_gather(parts, axes[k], axis=0, tiled=True)]
    ppermute x0 -> x2, waiting for transfers between devices: none -> 30.9 us  [the longest x1 23 us: one_device(): wu = lax.ppermute(wu, ('z', 'tp'), swap)]
    dot_general x3 -> x0, matrix products: 13.9 us -> none  [the longest x1 5.45 us: on_device(): lax.dot_general(hidden_full, inputs, (((0,), (0,)), ((), ())), preferred_...]
    ppermute x0 -> x2, starting transfers between devices: none -> 13.8 us  [the longest x1 10.5 us: one_device(): wu = lax.ppermute(wu, ('z', 'tp'), swap)]
    all_gather x3, waiting for transfers between devices: 67.4 us -> 79.1 us  [the longest x1 40.8 us: one_device(): lax.all_gather(after(wu, inputs_all), 'z', axis=0, tiled=True)]
  transfers between devices with their start and end apart: 6 -> 8, of which waited for: 4 -> 7; matrix products, arithmetic and copies ran while one was open for 5% -> 1% of each run, Pallas kernels for 0% -> 4%
where the time goes in v1:
time: 267 us; the launch traced here: 264 us
  waiting for transfers between devices  140 us (52%)
  blocking collectives  72 us (27%)
  starting transfers between devices  19.6 us (7%)
  between operations  13.9 us (5%)
  Pallas kernels  11.2 us (4%)
  local copies, waits for them, and re-layouts  4.44 us (2%)
  other arithmetic  2.71 us (1%)
    all_to_all x4, blocking collectives, exchange(): return lax.all_to_all(chunks, axis, 0, 0, tiled=True)  72 us
    all_gather x1, waiting for transfers between devices, one_device(): lax.all_gather(after(wu, inputs_all), 'z', axis=0, tiled=True)  40.8 us
    all_gather x1, waiting for transfers between devices, one_device(): dout_all = lax.all_gather(d_out, 'tp', axis=0, tiled=True)  30.2 us
    ppermute x1, waiting for transfers between devices, one_device(): wu = lax.ppermute(wu, ('z', 'tp'), swap)  23 us
    reduce_scatter x1, waiting for transfers between devices, one_device(): lax.psum_scatter(g.reshape(nz * hid, feats), 'z', scatter_dimension=0, ti...  19.7 us
    ppermute x1, starting transfers between devices, one_device(): wu = lax.ppermute(wu, ('z', 'tp'), swap)  10.5 us
    reduce_scatter x1, waiting for transfers between devices, one_device(): grad_input = lax.psum_scatter(part, 'tp', scatter_dimension=0, tiled=True)  10.1 us
    all_gather x1, waiting for transfers between devices, one_device(): wd = lax.all_gather(wd, 'z', axis=0, tiled=True)  8.04 us
  transfers between devices with their start and end apart: 8, of which 7 were waited for; matrix products, arithmetic and copies ran while one was open for 1% of the time, Pallas kernels for 4%

profile of v1, /device:TPU:6, one launch (start us, length us, event | category | flops | bytes accessed | tf_op | source)
XLA Modules:
  0.0 263.7 jit_solution(11842117802404533701)
XLA Ops:
  7.2 0.0 copy-start.2
  7.2 0.0 copy-start.5
  7.2 0.0 copy-start.1
  7.2 0.0 all-gather.6.cloned.1.call-start
  7.2 0.8 fusion.13
  8.0 0.8 pad_maximum_fusion
  8.8 0.0 copy-start.3
  8.8 24.5 %all_to_all.26 = bf16[8,128,256]{2,1,0:T(8,128)(2,1)S(1)} all-to-all(bf16[8,128,256]{2,1,0:T(8,128)(2,1)S(1)} %broadcast_in_dim.8), channel_id=1, replica_groups=mesh['z'=8,'y'=8,'tp'=8] {'y'}, dimensions={0} | all-to-all | bytes 1048576 | tf_op jit(solution)/shard_map/all_to_all | solution.py:15
  33.4 0.7 fusion.12
  34.1 0.0 all-gather.6.cloned.1.call-update
  34.1 0.0 all-gather.4.cloned.1.call-start
  34.2 0.0 copy-done.2
  34.2 0.0 copy-done.5
  34.2 0.0 copy-done.1
  34.2 0.2 fusion.3
  34.5 8.0 %all_to_all.27 = f32[8,2,512]{2,1,0:T(2,128)S(1)} all-to-all(f32[8,2,512]{2,1,0:T(2,128)S(1)} %broadcast_in_dim.9), channel_id=1, replica_groups=mesh['z'=8,'y'=8,'tp'=8] {'tp'}, dimensions={0} | all-to-all | bytes 65536 | tf_op jit(solution)/shard_map/all_to_all | solution.py:15
  42.5 1.0 fusion.9
  43.5 0.0 all-gather.4.cloned.1.call-update
  43.5 0.0 copy-done.3
  43.5 1.5 broadcast_in_dim.10
  45.0 5.6 %all-to-all-start.2 = ((bf16[8,512,256]{2,1,0:T(8,128)(2,1)}), bf16[8,512,256]{2,1,0:T(8,128)(2,1)S(1)}, u32[]{:S(2)}, u32[]{:S(2)}) async-start(bf16[8,512,256]{2,1,0:T(8,128)(2,1)} %broadcast_in_dim.10), calls=%async_computation.2 | async-start | bytes 4194304 | tf_op jit(solution)/shard_map/all_to_all | solution.py:15
  50.6 0.0 all-gather.8.cloned.1.call-start
  50.6 10.5 %collective-permute-start = (bf16[512,256]{1,0:T(8,128)(2,1)S(1)}, bf16[512,256]{1,0:T(8,128)(2,1)S(1)}, u32[]{:S(2)}, u32[]{:S(2)}) collective-permute-start(bf16[512,256]{1,0:T(8,128)(2,1)S(1)} %bitcast.22), channel_id=1, source_target_pairs={{0,0},{1,64},{2,128},{3,192},{4,256},{5,320},{6,384},{7,448},{64,1... | collective-permute-start | bytes 786440 | tf_op jit(solution)/shard_map/ppermute | solution.py:75
  61.1 23.0 %collective-permute-done = bf16[512,256]{1,0:T(8,128)(2,1)S(1)} collective-permute-done((bf16[512,256]{1,0:T(8,128)(2,1)S(1)}, bf16[512,256]{1,0:T(8,128)(2,1)S(1)}, u32[]{:S(2)}, u32[]{:S(2)}) %collective-permute-start) | collective-permute-done | bytes 262176 | tf_op jit(solution)/shard_map/ppermute | solution.py:75
  84.1 0.0 copy-start.4
  84.1 0.0 all-to-all-done.2.inputs
  84.1 0.0 copy-start
  84.1 0.7 copy-done.4
  84.8 0.0 all-gather.8.cloned.1.call-update
  84.8 0.0 reduce-scatter.5.cloned.1.call-start
  84.9 8.0 %all-gather.6.cloned.1.call-done = bf16[4096,256]{1,0:T(8,128)(2,1)} async-done(((bf16[512,256]{1,0:T(8,128)(2,1)}), bf16[4096,256]{1,0:T(8,128)(2,1)}) %all-gather.6.cloned.1.call-update) | async-done | bytes 2097168 | tf_op jit(solution)/shard_map/all_gather | solution.py:72
  92.9 30.2 %all-gather.4.cloned.1.call-done = bf16[4096,256]{1,0:T(8,128)(2,1)} async-done(((bf16[512,256]{1,0:T(8,128)(2,1)}), bf16[4096,256]{1,0:T(8,128)(2,1)}) %all-gather.4.cloned.1.call-update) | async-done | bytes 2097168 | tf_op jit(solution)/shard_map/all_gather | solution.py:83
  123.2 0.0 copy-done
  123.2 6.8 %grad_up_part.1 = (bf16[512,512]{1,0:T(8,128)(2,1)}, bf16[8,512,256]{2,1,0:T(8,128)(2,1)}) custom-call(bf16[8,512,256]{2,1,0:T(8,128)(2,1)} %bitcast.17, bf16[8,8,2,32,256]{4,3,2,1,0:T(8,128)(2,1)} %bitcast.16, bf16[512,512]{1,0:T(8,128)(2,1)} %hidden.1, bf16[8,512,256]{2,1,0:T(8,128)(2,1)} %copy-done), custom_call_target="tpu_custom_call" | custom-call | tf_op jit(solution)/shard_map/grad_up_part/pallas_call | solution.py:88
  130.0 0.0 reduce-scatter.5.cloned.1.call-update
  130.0 0.0 reduce-scatter.3.cloned.1.call-start
  130.1 40.8 %all-gather.8.cloned.1.call-done = bf16[4096,256]{1,0:T(8,128)(2,1)} async-done(((bf16[512,256]{1,0:T(8,128)(2,1)}), bf16[4096,256]{1,0:T(8,128)(2,1)}) %all-gather.8.cloned.1.call-update) | async-done | bytes 2097168 | tf_op jit(solution)/shard_map/all_gather | solution.py:86
  170.9 4.4 %grad_input_part.1 = bf16[8,512,256]{2,1,0:T(8,128)(2,1)} custom-call(bf16[512,512]{1,0:T(8,128)(2,1)} %get-tuple-element.12.d_pre, bf16[8,512,256]{2,1,0:T(8,128)(2,1)} %bitcast.19), custom_call_target="tpu_custom_call" | custom-call | tf_op jit(solution)/shard_map/grad_input_part/pallas_call | solution.py:104
  175.3 0.0 reduce-scatter.3.cloned.1.call-update
  175.4 22.3 %all_to_all.28 = f32[64,1,256]{2,1,0:T(1,128)S(1)} all-to-all(f32[64,1,256]{2,1,0:T(1,128)S(1)} %broadcast_in_dim.11), channel_id=1, replica_groups=mesh['z'=8,'y'=8,'tp'=8] {'z','y'}, dimensions={0} | all-to-all | bytes 131072 | tf_op jit(solution)/shard_map/all_to_all | solution.py:15
  197.6 0.7 reduce_sum.58
  198.3 19.7 %reduce-scatter.5.cloned.1.call-done = bf16[512,256]{1,0:T(8,128)(2,1)} async-done(((bf16[4096,256]{1,0:T(8,128)(2,1)}), bf16[512,256]{1,0:T(8,128)(2,1)}) %reduce-scatter.5.cloned.1.call-update) | async-done | bytes 262160 | tf_op jit(solution)/shard_map/reduce_scatter | solution.py:99
  218.0 17.3 %all_to_all.29 = bf16[8,64,256]{2,1,0:T(8,128)(2,1)S(1)} all-to-all(bf16[8,64,256]{2,1,0:T(8,128)(2,1)} %bitcast.21), channel_id=1, replica_groups=mesh['z'=8,'y'=8,'tp'=8] {'y'}, dimensions={0} | all-to-all | bytes 524288 | tf_op jit(solution)/shard_map/all_to_all | solution.py:15
  235.3 3.3 %collective-permute-start.1 = (f32[64,256]{1,0:T(8,128)S(1)}, f32[64,256]{1,0:T(8,128)S(1)}, u32[]{:S(2)}, u32[]{:S(2)}) collective-permute-start(f32[64,256]{1,0:T(8,128)S(1)} %broadcast_multiply_fusion), channel_id=1, source_target_pairs={{0,0},{1,64},{2,128},{3,192},{4,256},{5,320},{6,384},{7,448},{64,1... | collective-permute-start | bytes 196616 | tf_op jit(solution)/shard_map/ppermute | solution.py:102
  238.6 7.8 %collective-permute-done.1 = f32[64,256]{1,0:T(8,128)S(1)} collective-permute-done((f32[64,256]{1,0:T(8,128)S(1)}, f32[64,256]{1,0:T(8,128)S(1)}, u32[]{:S(2)}, u32[]{:S(2)}) %collective-permute-start.1) | collective-permute-done | bytes 65568 | tf_op jit(solution)/shard_map/ppermute | solution.py:102
  246.5 10.1 %reduce-scatter.3.cloned.1.call-done = bf16[512,256]{1,0:T(8,128)(2,1)} async-done(((bf16[4096,256]{1,0:T(8,128)(2,1)}), bf16[512,256]{1,0:T(8,128)(2,1)}) %reduce-scatter.3.cloned.1.call-update) | async-done | bytes 262160 | tf_op jit(solution)/shard_map/reduce_scatter | solution.py:110
  256.6 0.6 copy.15
  (9 shorter events, 0.2 us)
Async XLA Ops:
  7.2 27.0 %copy-start.2 = (bf16[512,256]{1,0:T(8,128)(2,1)S(1)}, bf16[512,256]{1,0:T(8,128)(2,1)}, u32[]{:S(2)}) copy-start(bf16[512,256]{1,0:T(8,128)(2,1)} %param.13) | copy-start | bytes 786436
  7.2 27.0 %copy-start.5 = (f32[256]{0:T(256)S(1)}, f32[256]{0:T(256)}, u32[]{:S(2)}) copy-start(f32[256]{0:T(256)} %param.10) | copy-start | bytes 3076
  7.2 27.0 %copy-start.1 = (bf16[512,256]{1,0:T(8,128)(2,1)S(1)}, bf16[512,256]{1,0:T(8,128)(2,1)}, u32[]{:S(2)}) copy-start(bf16[512,256]{1,0:T(8,128)(2,1)} %param.9) | copy-start | bytes 786436
  7.2 85.7 %all-gather.6.cloned.1.call-start = ((), (), s32[]{:S(2)}) async-start(), calls=%async_computation.8 | async-start | bytes 2359296 | tf_op jit(solution)/shard_map/all_gather | solution.py:72
  8.8 34.6 %copy-start.3 = (bf16[512,256]{1,0:T(8,128)(2,1)S(1)}, bf16[512,256]{1,0:T(8,128)(2,1)}, u32[]{:S(2)}) copy-start(bf16[512,256]{1,0:T(8,128)(2,1)} %param.7) | copy-start | bytes 786436
  34.1 89.0 %all-gather.4.cloned.1.call-start = ((), (), s32[]{:S(2)}) async-start(), calls=%async_computation.7 | async-start | bytes 2359296 | tf_op jit(solution)/shard_map/all_gather | solution.py:83
  45.0 39.2 %all-to-all-start.2 = ((bf16[8,512,256]{2,1,0:T(8,128)(2,1)}), bf16[8,512,256]{2,1,0:T(8,128)(2,1)S(1)}, u32[]{:S(2)}, u32[]{:S(2)}) async-start(bf16[8,512,256]{2,1,0:T(8,128)(2,1)} %broadcast_in_dim.10), calls=%async_computation.2 | async-start | bytes 4194304 | tf_op jit(solution)/shard_map/all_to_all | solution.py:15
  50.6 120.4 %all-gather.8.cloned.1.call-start = ((), (), s32[]{:S(2)}) async-start(), calls=%async_computation.9 | async-start | bytes 2359296 | tf_op jit(solution)/shard_map/all_gather | solution.py:86
  50.6 33.5 %collective-permute-start = (bf16[512,256]{1,0:T(8,128)(2,1)S(1)}, bf16[512,256]{1,0:T(8,128)(2,1)S(1)}, u32[]{:S(2)}, u32[]{:S(2)}) collective-permute-start(bf16[512,256]{1,0:T(8,128)(2,1)S(1)} %bitcast.22), channel_id=1, source_target_pairs={{0,0},{1,64},{2,128},{3,192},{4,256},{5,320},{6,384},{7,448},{64,1... | collective-permute-start | bytes 786440 | tf_op jit(solution)/shard_map/ppermute | solution.py:75
  84.1 0.7 copy-start.4
  84.1 39.1 %copy-start = (bf16[8,512,256]{2,1,0:T(8,128)(2,1)}, bf16[8,512,256]{2,1,0:T(8,128)(2,1)S(1)}, u32[]{:S(2)}) copy-start(bf16[8,512,256]{2,1,0:T(8,128)(2,1)S(1)} %all-to-all-done.2.inputs) | copy-start | bytes 6291460
  84.8 133.1 %reduce-scatter.5.cloned.1.call-start = ((), (), s32[]{:S(2)}) async-start(), calls=%async_computation.11 | async-start | bytes 2359296 | tf_op jit(solution)/shard_map/reduce_scatter | solution.py:99
  130.0 126.5 %reduce-scatter.3.cloned.1.call-start = ((), (), s32[]{:S(2)}) async-start(), calls=%async_computation.10 | async-start | bytes 2359296 | tf_op jit(solution)/shard_map/reduce_scatter | solution.py:110
  235.3 11.2 %collective-permute-start.1 = (f32[64,256]{1,0:T(8,128)S(1)}, f32[64,256]{1,0:T(8,128)S(1)}, u32[]{:S(2)}, u32[]{:S(2)}) collective-permute-start(f32[64,256]{1,0:T(8,128)S(1)} %broadcast_multiply_fusion), channel_id=1, source_target_pairs={{0,0},{1,64},{2,128},{3,192},{4,256},{5,320},{6,384},{7,448},{64,1... | collective-permute-start | bytes 196616 | tf_op jit(solution)/shard_map/ppermute | solution.py:102
Sparse Core Ops, SparseCore 0:
  34.3 58.6 all-gather.5
  95.6 27.4 all-gather.3
  125.3 45.6 all-gather.7
  173.6 44.3 reduce-scatter.4
  221.2 35.2 reduce-scatter.2

commit v2 on v1

--- a/solution.py
+++ b/solution.py
@@ -28,6 +28,16 @@
     return lax.optimization_barrier((value, earlier))[0]
 
 
+def butterfly(value, axes):
+    for axis in axes:
+        n = lax.axis_size(axis)
+        step = 1
+        while step < n:
+            value = value + lax.ppermute(value, axis, [(i, i ^ step) for i in range(n)])
+            step *= 2
+    return value
+
+
 def grad_up_kernel(dout, wd, hidden, inputs, d_pre_out, g_out):
     blocks, toks, feats = dout.shape
     half = wd.shape[-1]
@@ -40,8 +50,11 @@
         pre = jnp.maximum(hidden[:, cols].astype(f32), 0.0)
         d_pre_out[:, cols] = (acc * 2.0 * pre).astype(bf16)
     d_pre_t = d_pre_out[...].T
+    rows = g_out.shape[1]
     for k in range(blocks):
-        g_out[k] = jnp.dot(d_pre_t, inputs[k], preferred_element_type=f32).astype(bf16)
+        g = jnp.dot(d_pre_t, inputs[k], preferred_element_type=f32).astype(bf16)
+        for j in range(blocks):
+            g_out[k * blocks + j] = g[j * rows : (j + 1) * rows]
 
 
 def grad_input_kernel(d_pre, w_up, out):
@@ -63,49 +76,45 @@
     weighted = upstream * out_gain
     sums = jnp.stack([jnp.sum(normed * normed, axis=1), jnp.sum(weighted * normed, axis=1)])
 
+    inputs_all = lax.all_gather(inputs, "tp", axis=0, tiled=True).reshape(ntp, toks, feats)
     wd = w_down.T
     half = hid // 2
     both = jnp.concatenate([wd[:, :half], wd[:, half:], w_up.T], axis=0)
     both = gather_directly(both, "y")
     wd_rows = 2 * wd.shape[0]
     wd = wd_y = both[:, :wd_rows].reshape(ny * wd_rows, half)
-    wd = lax.all_gather(wd, "z", axis=0, tiled=True)
-    wd = wd.reshape(nz, ny, 2, wd_rows // 2, half)
+    wd = lax.all_gather(wd, "z", axis=0, tiled=True).reshape(nz, ny, 2, wd_rows // 2, half)
     wu = both[:, wd_rows:].reshape(hid, feats)
-    wu = lax.ppermute(wu, ("z", "tp"), swap)
+    wu = lax.ppermute(after(wu, wd_y), ("z", "tp"), swap)
 
-    sums = gather_directly(after(sums, wd_y), "tp")
-    sums = jnp.sum(sums, axis=0)
+    sums = jnp.sum(gather_directly(after(sums, wd_y), "tp"), axis=0)
     inv_rms = lax.rsqrt(sums[0] / width + norm_eps)[:, None]
     cross_mean = (sums[1] / width)[:, None]
     d_out = (weighted * inv_rms - normed * inv_rms * inv_rms * inv_rms * cross_mean).astype(bf16)
     gain_part = jnp.sum(upstream * normed * inv_rms, axis=0) * scaled
-    dout_all = lax.all_gather(d_out, "tp", axis=0, tiled=True)
-    dout_all = dout_all.reshape(ntp, toks, feats)
-    inputs_all = gather_directly(after(inputs, sums), "tp")
-    wu = lax.all_gather(after(wu, inputs_all), "z", axis=0, tiled=True).reshape(nz, hid, feats)
+    dout_all = gather_directly(d_out, "tp")
 
     d_pre, g = pl.pallas_call(
         grad_up_kernel,
         out_shape=(
             jax.ShapeDtypeStruct((toks, hid), bf16),
-            jax.ShapeDtypeStruct((nz, hid, feats), bf16),
+            jax.ShapeDtypeStruct((nz * ny, hid // ny, feats), bf16),
         ),
         name="grad_up_part",
     )(dout_all, wd, hidden_pre, inputs_all)
 
-    grad_gain = jnp.sum(gather_directly(after(gain_part, d_pre), FS), axis=0)
-
-    g = lax.psum_scatter(g.reshape(nz * hid, feats), "z", scatter_dimension=0, tiled=True)
-    g = after(g, grad_gain)
-    g = summed(exchange(g.reshape(ny, hid // ny, feats), "y")) * scaled
+    g = exchange(g, FS)
+    g = summed(g) * scaled
     grad_up = lax.ppermute(g, ("z", "tp"), swap).T
 
+    grad_gain = butterfly(after(gain_part, d_pre), ("z", "y"))
+
+    wu = lax.all_gather(after(wu, dout_all), "z", axis=0, tiled=True).reshape(nz, hid, feats)
     part = pl.pallas_call(
         grad_input_kernel,
         out_shape=jax.ShapeDtypeStruct((ntp, toks, feats), bf16),
         name="grad_input_part",
-    )(d_pre, wu)
+    )(after(d_pre, grad_gain), wu)
     part = part.reshape(ntp * toks, feats)
     grad_input = lax.psum_scatter(part, "tp", scatter_dimension=0, tiled=True)
 

time: 267 us -> 252 us (0.944)
  blocking collectives: 72 us -> 32.3 us
  starting transfers between devices: 19.6 us -> 49.2 us
  waiting for transfers between devices: 140 us -> 135 us
    ppermute x1 -> x7, waiting for transfers between devices: 23 us -> 83.1 us  [the longest x6 60.5 us: butterfly(): value = value + lax.ppermute(value, axis, [(i, i ^ step) for i in range(n)])]
    all_gather x3, waiting for transfers between devices: 79.1 us -> 19.5 us  [the longest x1 19.5 us: one_device(): lax.all_gather(wd, 'z', axis=0, tiled=True)]
    all_to_all x4 -> x2, blocking collectives: 72 us -> 32.3 us  [exchange(): return lax.all_to_all(chunks, axis, 0, 0, tiled=True)]
    ppermute x1 -> x7, starting transfers between devices: 10.5 us -> 34.9 us  [the longest x6 24.4 us: butterfly(): value = value + lax.ppermute(value, axis, [(i, i ^ step) for i in range(n)])]
    reduce_scatter x1 -> x0, waiting for transfers between devices: 19.7 us -> none  [one_device(): lax.psum_scatter(g.reshape(nz * hid, feats), 'z', scatter_dimension=0, ti...]
    reduce_scatter x1, waiting for transfers between devices: 10.1 us -> 24.1 us  [one_device(): grad_input = lax.psum_scatter(part, 'tp', scatter_dimension=0, tiled=True)]
    all_to_all x1 -> x2, starting transfers between devices: 5.61 us -> 11.1 us  [exchange(): return lax.all_to_all(chunks, axis, 0, 0, tiled=True)]
  transfers between devices with their start and end apart: 8 -> 14, of which waited for: 7 -> 10; matrix products, arithmetic and copies ran while one was open for 1% -> 2% of each run, Pallas kernels for 4% -> 5%
where the time goes in v2:
time: 252 us; the launch traced here: 248 us
  waiting for transfers between devices  135 us (54%)
  starting transfers between devices  49.2 us (20%)
  blocking collectives  32.3 us (13%)
  between operations  13.9 us (6%)
  Pallas kernels  11.2 us (4%)
  local copies, waits for them, and re-layouts  4.34 us (2%)
    ppermute x6, waiting for transfers between devices, butterfly(): value = value + lax.ppermute(value, axis, [(i, i ^ step) for i in range(n)])  60.5 us
    all_to_all x2, blocking collectives, exchange(): return lax.all_to_all(chunks, axis, 0, 0, tiled=True)  32.3 us
    ppermute x6, starting transfers between devices, butterfly(): value = value + lax.ppermute(value, axis, [(i, i ^ step) for i in range(n)])  24.4 us
    reduce_scatter x1, waiting for transfers between devices, one_device(): grad_input = lax.psum_scatter(part, 'tp', scatter_dimension=0, tiled=True)  24.1 us
    ppermute x1, waiting for transfers between devices, one_device(): wu = lax.ppermute(after(wu, wd_y), ('z', 'tp'), swap)  22.6 us
    all_gather x1, waiting for transfers between devices, one_device(): lax.all_gather(wd, 'z', axis=0, tiled=True)  19.5 us
    all_to_all x2, starting transfers between devices, exchange(): return lax.all_to_all(chunks, axis, 0, 0, tiled=True)  11.1 us
    ppermute x1, starting transfers between devices, one_device(): wu = lax.ppermute(after(wu, wd_y), ('z', 'tp'), swap)  10.5 us
  transfers between devices with their start and end apart: 14, of which 10 were waited for; matrix products, arithmetic and copies ran while one was open for 2% of the time, Pallas kernels for 5%

profile of v2, /device:TPU:6, one launch (start us, length us, event | category | flops | bytes accessed | tf_op | source)
XLA Modules:
  0.0 247.9 jit_solution(14886228768437560364)
XLA Ops:
  7.2 0.0 copy-start.2
  7.2 0.0 copy-start.4
  7.2 0.0 copy-start.1
  7.2 0.0 all-gather.6.cloned.1.call-start
  7.2 0.7 all-gather.6.cloned.1.call-update
  7.9 0.0 all-gather.4.cloned.1.call-start
  8.0 0.7 fusion.13
  8.7 0.8 pad_maximum_fusion
  9.5 24.4 %all_to_all.20 = bf16[8,128,256]{2,1,0:T(8,128)(2,1)S(1)} all-to-all(bf16[8,128,256]{2,1,0:T(8,128)(2,1)S(1)} %broadcast_in_dim.6), channel_id=1, replica_groups=mesh['z'=8,'y'=8,'tp'=8] {'y'}, dimensions={0} | all-to-all | bytes 1048576 | tf_op jit(solution)/shard_map/all_to_all | solution.py:15
  33.9 0.7 fusion.12
  34.7 0.0 all-gather.4.cloned.1.call-update
  34.7 0.0 copy-done.2
  34.7 0.0 copy-done.4
  34.7 0.0 copy-done.1
  34.7 0.2 fusion.3
  35.0 8.0 %all_to_all.21 = f32[8,2,512]{2,1,0:T(2,128)S(1)} all-to-all(f32[8,2,512]{2,1,0:T(2,128)S(1)} %broadcast_in_dim.7), channel_id=1, replica_groups=mesh['z'=8,'y'=8,'tp'=8] {'tp'}, dimensions={0} | all-to-all | bytes 65536 | tf_op jit(solution)/shard_map/all_to_all | solution.py:15
  43.0 0.3 fusion.9
  43.3 1.5 broadcast_in_dim.8
  44.8 5.6 %all-to-all-start.2 = ((bf16[8,512,256]{2,1,0:T(8,128)(2,1)}), bf16[8,512,256]{2,1,0:T(8,128)(2,1)S(1)}, u32[]{:S(2)}, u32[]{:S(2)}) async-start(bf16[8,512,256]{2,1,0:T(8,128)(2,1)} %broadcast_in_dim.8), calls=%async_computation.2 | async-start | bytes 4194304 | tf_op jit(solution)/shard_map/all_to_all | solution.py:15
  50.4 0.0 all-gather.8.cloned.1.call-start
  50.4 10.5 %collective-permute-start.6 = (bf16[512,256]{1,0:T(8,128)(2,1)S(1)}, bf16[512,256]{1,0:T(8,128)(2,1)S(1)}, u32[]{:S(2)}, u32[]{:S(2)}) collective-permute-start(bf16[512,256]{1,0:T(8,128)(2,1)S(1)} %bitcast.18), channel_id=1, source_target_pairs={{0,0},{1,64},{2,128},{3,192},{4,256},{5,320},{6,384},{7,448},{64,1... | collective-permute-start | bytes 786440 | tf_op jit(solution)/shard_map/ppermute | solution.py:88
  60.9 22.6 %collective-permute-done.6 = bf16[512,256]{1,0:T(8,128)(2,1)S(1)} collective-permute-done((bf16[512,256]{1,0:T(8,128)(2,1)S(1)}, bf16[512,256]{1,0:T(8,128)(2,1)S(1)}, u32[]{:S(2)}, u32[]{:S(2)}) %collective-permute-start.6) | collective-permute-done | bytes 262176 | tf_op jit(solution)/shard_map/ppermute | solution.py:88
  83.5 0.0 copy-start.3
  83.5 0.0 all-to-all-done.2.dout
  83.5 0.0 copy-start
  83.5 0.7 copy-done.3
  84.1 0.0 all-gather.8.cloned.1.call-update
  84.2 0.0 all-gather.6.cloned.1.call-done
  84.2 19.5 %all-gather.4.cloned.1.call-done = bf16[4096,256]{1,0:T(8,128)(2,1)} async-done(((bf16[512,256]{1,0:T(8,128)(2,1)}), bf16[4096,256]{1,0:T(8,128)(2,1)}) %all-gather.4.cloned.1.call-update) | async-done | bytes 2097168 | tf_op jit(solution)/shard_map/all_gather | solution.py:86
  103.7 0.0 copy-done
  103.7 6.8 %grad_up_part.1 = (bf16[512,512]{1,0:T(8,128)(2,1)}, bf16[64,64,256]{2,1,0:T(8,128)(2,1)}) custom-call(bf16[8,512,256]{2,1,0:T(8,128)(2,1)} %copy-done, bf16[8,8,2,32,256]{4,3,2,1,0:T(8,128)(2,1)} %bitcast.16, bf16[512,512]{1,0:T(8,128)(2,1)} %hidden.1, bf16[8,512,256]{2,1,0:T(8,128)(2,1)} %bitcast.14), custom_call_target="tpu_custom_call" | custom-call | tf_op jit(solution)/shard_map/grad_up_part/pallas_call | solution.py:97
  110.5 5.5 %all-to-all-start.3 = ((bf16[64,64,256]{2,1,0:T(8,128)(2,1)}), bf16[64,64,256]{2,1,0:T(8,128)(2,1)S(1)}, u32[]{:S(2)}, u32[]{:S(2)}) async-start(bf16[64,64,256]{2,1,0:T(8,128)(2,1)} %get-tuple-element.16), calls=%async_computation.4 | async-start | bytes 4194304 | tf_op jit(solution)/shard_map/all_to_all | solution.py:15
  116.0 0.0 reduce-scatter.2.cloned.1.call-start
  116.1 3.5 %collective-permute-start = (f32[256]{0:T(256)S(1)}, f32[256]{0:T(256)S(1)}, u32[]{:S(2)}, u32[]{:S(2)}) collective-permute-start(f32[256]{0:T(256)S(1)} %broadcast_multiply_fusion.1), channel_id=1, source_target_pairs={{0,64},{64,0},{128,192},{192,128},{256,320},{320,256},{384,448},{4... | collective-permute-start | bytes 3080 | tf_op jit(solution)/shard_map/ppermute | solution.py:36
  119.6 44.5 %collective-permute-done = f32[256]{0:T(256)S(1)} collective-permute-done((f32[256]{0:T(256)S(1)}, f32[256]{0:T(256)S(1)}, u32[]{:S(2)}, u32[]{:S(2)}) %collective-permute-start) | collective-permute-done | bytes 1056 | tf_op jit(solution)/shard_map/ppermute | solution.py:36
  164.1 3.3 %collective-permute-start.1 = (f32[256]{0:T(256)S(1)}, f32[256]{0:T(256)S(1)}, u32[]{:S(2)}, u32[]{:S(2)}) collective-permute-start(f32[256]{0:T(256)S(1)} %add.33), channel_id=1, source_target_pairs={{0,128},{64,192},{128,0},{192,64},{256,384},{320,448},{384,256},{4... | collective-permute-start | bytes 3080 | tf_op jit(solution)/shard_map/ppermute | solution.py:36
  167.4 3.1 %collective-permute-done.1 = f32[256]{0:T(256)S(1)} collective-permute-done((f32[256]{0:T(256)S(1)}, f32[256]{0:T(256)S(1)}, u32[]{:S(2)}, u32[]{:S(2)}) %collective-permute-start.1) | collective-permute-done | bytes 1056 | tf_op jit(solution)/shard_map/ppermute | solution.py:36
  170.4 5.6 %collective-permute-start.2 = (f32[256]{0:T(256)S(1)}, f32[256]{0:T(256)S(1)}, u32[]{:S(2)}, u32[]{:S(2)}) collective-permute-start(f32[256]{0:T(256)S(1)} %add.34), channel_id=1, source_target_pairs={{0,256},{64,320},{128,384},{192,448},{256,0},{320,64},{384,128},{4... | collective-permute-start | bytes 3080 | tf_op jit(solution)/shard_map/ppermute | solution.py:36
  176.1 3.7 %collective-permute-done.2 = f32[256]{0:T(256)S(1)} collective-permute-done((f32[256]{0:T(256)S(1)}, f32[256]{0:T(256)S(1)}, u32[]{:S(2)}, u32[]{:S(2)}) %collective-permute-start.2) | collective-permute-done | bytes 1056 | tf_op jit(solution)/shard_map/ppermute | solution.py:36
  179.8 1.9 collective-permute-start.3
  181.7 3.5 %collective-permute-done.3 = f32[256]{0:T(256)S(1)} collective-permute-done((f32[256]{0:T(256)S(1)}, f32[256]{0:T(256)S(1)}, u32[]{:S(2)}, u32[]{:S(2)}) %collective-permute-start.3) | collective-permute-done | bytes 1056 | tf_op jit(solution)/shard_map/ppermute | solution.py:36
  185.3 4.5 %collective-permute-start.4 = (f32[256]{0:T(256)S(1)}, f32[256]{0:T(256)S(1)}, u32[]{:S(2)}, u32[]{:S(2)}) collective-permute-start(f32[256]{0:T(256)S(1)} %add.36), channel_id=1, source_target_pairs={{0,16},{8,24},{16,0},{24,8},{32,48},{40,56},{48,32},{56,40},{1,17}... | collective-permute-start | bytes 3080 | tf_op jit(solution)/shard_map/ppermute | solution.py:36
  189.8 1.9 collective-permute-done.4
  191.6 5.6 %collective-permute-start.5 = (f32[256]{0:T(256)S(1)}, f32[256]{0:T(256)S(1)}, u32[]{:S(2)}, u32[]{:S(2)}) collective-permute-start(f32[256]{0:T(256)S(1)} %add.37), channel_id=1, source_target_pairs={{0,32},{8,40},{16,48},{24,56},{32,0},{40,8},{48,16},{56,24},{1,33}... | collective-permute-start | bytes 3080 | tf_op jit(solution)/shard_map/ppermute | solution.py:36
  197.3 3.7 %collective-permute-done.5 = f32[256]{0:T(256)S(1)} collective-permute-done((f32[256]{0:T(256)S(1)}, f32[256]{0:T(256)S(1)}, u32[]{:S(2)}, u32[]{:S(2)}) %collective-permute-start.5) | collective-permute-done | bytes 1056 | tf_op jit(solution)/shard_map/ppermute | solution.py:36
  201.0 0.6 add.38
  201.6 0.0 all-gather.8.cloned.1.call-done
  201.6 4.4 %grad_input_part.1 = bf16[8,512,256]{2,1,0:T(8,128)(2,1)} custom-call(bf16[512,512]{1,0:T(8,128)(2,1)} %get-tuple-element.13.d_pre, bf16[8,512,256]{2,1,0:T(8,128)(2,1)} %bitcast.15), custom_call_target="tpu_custom_call" | custom-call | tf_op jit(solution)/shard_map/grad_input_part/pallas_call | solution.py:113
  205.9 0.0 reduce-scatter.2.cloned.1.call-update
  206.0 0.0 all-to-all-done.3
  206.0 0.3 convert_reduce_fusion
  206.3 3.0 %collective-permute-start.7 = (f32[64,256]{1,0:T(8,128)S(1)}, f32[64,256]{1,0:T(8,128)S(1)}, u32[]{:S(2)}, u32[]{:S(2)}) collective-permute-start(f32[64,256]{1,0:T(8,128)S(1)} %broadcast_multiply_fusion), channel_id=1, source_target_pairs={{0,0},{1,64},{2,128},{3,192},{4,256},{5,320},{6,384},{7,448},{64,1... | collective-permute-start | bytes 196616 | tf_op jit(solution)/shard_map/ppermute | solution.py:108
  209.3 7.3 %collective-permute-done.7 = f32[64,256]{1,0:T(8,128)S(1)} collective-permute-done((f32[64,256]{1,0:T(8,128)S(1)}, f32[64,256]{1,0:T(8,128)S(1)}, u32[]{:S(2)}, u32[]{:S(2)}) %collective-permute-start.7) | collective-permute-done | bytes 65568 | tf_op jit(solution)/shard_map/ppermute | solution.py:108
  216.7 24.1 %reduce-scatter.2.cloned.1.call-done = bf16[512,256]{1,0:T(8,128)(2,1)} async-done(((bf16[4096,256]{1,0:T(8,128)(2,1)}), bf16[512,256]{1,0:T(8,128)(2,1)}) %reduce-scatter.2.cloned.1.call-update) | async-done | bytes 262160 | tf_op jit(solution)/shard_map/reduce_scatter | solution.py:119
  240.8 0.6 copy.15
  (12 shorter events, 0.1 us)
Async XLA Ops:
  7.2 27.5 %copy-start.2 = (bf16[512,256]{1,0:T(8,128)(2,1)S(1)}, bf16[512,256]{1,0:T(8,128)(2,1)}, u32[]{:S(2)}) copy-start(bf16[512,256]{1,0:T(8,128)(2,1)} %param.13) | copy-start | bytes 786436
  7.2 27.5 %copy-start.4 = (f32[256]{0:T(256)S(1)}, f32[256]{0:T(256)}, u32[]{:S(2)}) copy-start(f32[256]{0:T(256)} %param.10) | copy-start | bytes 3076
  7.2 27.5 %copy-start.1 = (bf16[512,256]{1,0:T(8,128)(2,1)S(1)}, bf16[512,256]{1,0:T(8,128)(2,1)}, u32[]{:S(2)}) copy-start(bf16[512,256]{1,0:T(8,128)(2,1)} %param.9) | copy-start | bytes 786436
  7.2 77.0 %all-gather.6.cloned.1.call-start = ((), (), s32[]{:S(2)}) async-start(), calls=%async_computation.6 | async-start | bytes 2359296 | tf_op jit(solution)/shard_map/all_gather | solution.py:79
  7.9 95.7 %all-gather.4.cloned.1.call-start = ((), (), s32[]{:S(2)}) async-start(), calls=%async_computation.5 | async-start | bytes 2359296 | tf_op jit(solution)/shard_map/all_gather | solution.py:86
  44.8 38.7 %all-to-all-start.2 = ((bf16[8,512,256]{2,1,0:T(8,128)(2,1)}), bf16[8,512,256]{2,1,0:T(8,128)(2,1)S(1)}, u32[]{:S(2)}, u32[]{:S(2)}) async-start(bf16[8,512,256]{2,1,0:T(8,128)(2,1)} %broadcast_in_dim.8), calls=%async_computation.2 | async-start | bytes 4194304 | tf_op jit(solution)/shard_map/all_to_all | solution.py:15
  50.4 151.2 %all-gather.8.cloned.1.call-start = ((), (), s32[]{:S(2)}) async-start(), calls=%async_computation.7 | async-start | bytes 2359296 | tf_op jit(solution)/shard_map/all_gather | solution.py:112
  50.4 33.1 %collective-permute-start.6 = (bf16[512,256]{1,0:T(8,128)(2,1)S(1)}, bf16[512,256]{1,0:T(8,128)(2,1)S(1)}, u32[]{:S(2)}, u32[]{:S(2)}) collective-permute-start(bf16[512,256]{1,0:T(8,128)(2,1)S(1)} %bitcast.18), channel_id=1, source_target_pairs={{0,0},{1,64},{2,128},{3,192},{4,256},{5,320},{6,384},{7,448},{64,1... | collective-permute-start | bytes 786440 | tf_op jit(solution)/shard_map/ppermute | solution.py:88
  83.5 0.7 copy-start.3
  83.5 20.2 %copy-start = (bf16[8,512,256]{2,1,0:T(8,128)(2,1)}, bf16[8,512,256]{2,1,0:T(8,128)(2,1)S(1)}, u32[]{:S(2)}) copy-start(bf16[8,512,256]{2,1,0:T(8,128)(2,1)S(1)} %all-to-all-done.2.dout) | copy-start | bytes 6291460
  110.5 95.5 %all-to-all-start.3 = ((bf16[64,64,256]{2,1,0:T(8,128)(2,1)}), bf16[64,64,256]{2,1,0:T(8,128)(2,1)S(1)}, u32[]{:S(2)}, u32[]{:S(2)}) async-start(bf16[64,64,256]{2,1,0:T(8,128)(2,1)} %get-tuple-element.16), calls=%async_computation.4 | async-start | bytes 4194304 | tf_op jit(solution)/shard_map/all_to_all | solution.py:15
  116.0 124.7 %reduce-scatter.2.cloned.1.call-start = ((), (), s32[]{:S(2)}) async-start(), calls=%async_computation.8 | async-start | bytes 2359296 | tf_op jit(solution)/shard_map/reduce_scatter | solution.py:119
  116.1 48.0 %collective-permute-start = (f32[256]{0:T(256)S(1)}, f32[256]{0:T(256)S(1)}, u32[]{:S(2)}, u32[]{:S(2)}) collective-permute-start(f32[256]{0:T(256)S(1)} %broadcast_multiply_fusion.1), channel_id=1, source_target_pairs={{0,64},{64,0},{128,192},{192,128},{256,320},{320,256},{384,448},{4... | collective-permute-start | bytes 3080 | tf_op jit(solution)/shard_map/ppermute | solution.py:36
  164.1 6.4 %collective-permute-start.1 = (f32[256]{0:T(256)S(1)}, f32[256]{0:T(256)S(1)}, u32[]{:S(2)}, u32[]{:S(2)}) collective-permute-start(f32[256]{0:T(256)S(1)} %add.33), channel_id=1, source_target_pairs={{0,128},{64,192},{128,0},{192,64},{256,384},{320,448},{384,256},{4... | collective-permute-start | bytes 3080 | tf_op jit(solution)/shard_map/ppermute | solution.py:36
  170.4 9.4 %collective-permute-start.2 = (f32[256]{0:T(256)S(1)}, f32[256]{0:T(256)S(1)}, u32[]{:S(2)}, u32[]{:S(2)}) collective-permute-start(f32[256]{0:T(256)S(1)} %add.34), channel_id=1, source_target_pairs={{0,256},{64,320},{128,384},{192,448},{256,0},{320,64},{384,128},{4... | collective-permute-start | bytes 3080 | tf_op jit(solution)/shard_map/ppermute | solution.py:36
  179.8 5.5 %collective-permute-start.3 = (f32[256]{0:T(256)S(1)}, f32[256]{0:T(256)S(1)}, u32[]{:S(2)}, u32[]{:S(2)}) collective-permute-start(f32[256]{0:T(256)S(1)} %add.35), channel_id=1, source_target_pairs={{0,8},{8,0},{16,24},{24,16},{32,40},{40,32},{48,56},{56,48},{1,9},... | collective-permute-start | bytes 3080 | tf_op jit(solution)/shard_map/ppermute | solution.py:36
  185.3 6.4 %collective-permute-start.4 = (f32[256]{0:T(256)S(1)}, f32[256]{0:T(256)S(1)}, u32[]{:S(2)}, u32[]{:S(2)}) collective-permute-start(f32[256]{0:T(256)S(1)} %add.36), channel_id=1, source_target_pairs={{0,16},{8,24},{16,0},{24,8},{32,48},{40,56},{48,32},{56,40},{1,17}... | collective-permute-start | bytes 3080 | tf_op jit(solution)/shard_map/ppermute | solution.py:36
  191.6 9.4 %collective-permute-start.5 = (f32[256]{0:T(256)S(1)}, f32[256]{0:T(256)S(1)}, u32[]{:S(2)}, u32[]{:S(2)}) collective-permute-start(f32[256]{0:T(256)S(1)} %add.37), channel_id=1, source_target_pairs={{0,32},{8,40},{16,48},{24,56},{32,0},{40,8},{48,16},{56,24},{1,33}... | collective-permute-start | bytes 3080 | tf_op jit(solution)/shard_map/ppermute | solution.py:36
  206.3 10.4 %collective-permute-start.7 = (f32[64,256]{1,0:T(8,128)S(1)}, f32[64,256]{1,0:T(8,128)S(1)}, u32[]{:S(2)}, u32[]{:S(2)}) collective-permute-start(f32[64,256]{1,0:T(8,128)S(1)} %broadcast_multiply_fusion), channel_id=1, source_target_pairs={{0,0},{1,64},{2,128},{3,192},{4,256},{5,320},{6,384},{7,448},{64,1... | collective-permute-start | bytes 196616 | tf_op jit(solution)/shard_map/ppermute | solution.py:108
Sparse Core Ops, SparseCore 0:
  10.2 33.9 all-gather.5
  46.8 56.8 all-gather.3
  105.7 80.7 all-gather.7
  206.1 34.6 reduce-scatter.1

commit v3 on v1

v3 whole, which is shorter than its diff:
```python
import jax
import jax.numpy as jnp
from jax import lax
from jax.experimental import pallas as pl
from jax.experimental.pallas import tpu as pltpu
from jax.sharding import Mesh
from jax.sharding import PartitionSpec as P

FS = ("z", "y")
TP = ("x", "c")
bf16 = jnp.bfloat16
f32 = jnp.float32
norm_eps = 1e-06


def exchange(chunks, axis):
    return lax.all_to_all(chunks, axis, 0, 0, tiled=True)


def gather_directly(value, axis):
    n = lax.axis_size(axis)
    return exchange(jnp.broadcast_to(value[None], (n, *value.shape)), axis)


def gather_two_steps(value):
    mine = gather_directly(value, "x")
    theirs = lax.ppermute(mine, "c", [(0, 1), (1, 0)])
    return mine, theirs


def after(value, earlier):
    return lax.optimization_barrier((value, earlier))[0]


def summed(parts):
    return jnp.sum(parts.astype(f32), axis=0)


def d_pre_kernel(core, mine, theirs, wd, hidden, out):
    chips, toks, feats = mine.shape
    half = wd.shape[-1]
    c = core[0]
    for s in range(2):
        cols = slice(s * half, (s + 1) * half)
        acc = jnp.zeros((toks, half), f32)
        for k in range(chips):
            w = wd[2 * k + c, :, s].reshape(feats, half)
            acc += jnp.dot(mine[k], w, preferred_element_type=f32)
            w = wd[2 * k + 1 - c, :, s].reshape(feats, half)
            acc += jnp.dot(theirs[k], w, preferred_element_type=f32)
        pre = jnp.maximum(hidden[:, cols].astype(f32), 0.0)
        out[:, cols] = (acc * 2.0 * pre).astype(bf16)


def grad_up_kernel(core, mine, theirs, inputs, out):
    c = core[0]
    right = inputs[...]
    for k in range(mine.shape[0]):
        g = jnp.dot(mine[k].T, right, preferred_element_type=f32)
        out[2 * k + c] = g.astype(bf16)
        g = jnp.dot(theirs[k].T, right, preferred_element_type=f32)
        out[2 * k + 1 - c] = g.astype(bf16)


def grad_input_kernel(core, mine, theirs, wu, out):
    c = core[0]
    acc = jnp.zeros(out.shape, f32)
    for k in range(mine.shape[0]):
        acc += jnp.dot(mine[k], wu[2 * k + c], preferred_element_type=f32)
        acc += jnp.dot(theirs[k], wu[2 * k + 1 - c], preferred_element_type=f32)
    out[...] = acc.astype(bf16)


def run(kernel, shape, *operands):
    scalar = pl.BlockSpec(memory_space=pltpu.SMEM)
    whole = pl.BlockSpec(memory_space=pltpu.VMEM)
    return pl.pallas_call(
        kernel,
        out_shape=jax.ShapeDtypeStruct(shape, bf16),
        in_specs=[scalar] + [whole] * (len(operands) - 1),
        out_specs=whole,
        name=kernel.__name__,
    )(*operands)


def on_device(inputs, hidden_pre, norm_input, out_gain, w_up, w_down, cotangent):
    nz, ny, ntp = (lax.axis_size(a) for a in ("z", "y", TP))
    toks, feats = inputs.shape
    hid = hidden_pre.shape[1]
    half = hid // 2
    width = feats * ntp
    scaled = (toks * nz * ny) ** (-0.5)
    core = lax.axis_index("c").astype(jnp.int32).reshape(1)

    normed = norm_input.astype(f32)
    upstream = cotangent.astype(f32)
    weighted = upstream * out_gain
    sums = jnp.stack([jnp.sum(normed * normed, axis=1), jnp.sum(weighted * normed, axis=1)])

    wd = w_down.T
    both = jnp.concatenate([wd[:, :half], wd[:, half:], w_up.T], axis=0)
    both = gather_directly(both, "y")
    wd_rows = 2 * wd.shape[0]
    wd = wd_y = both[:, :wd_rows].reshape(ny * wd_rows, half)
    wd = lax.all_gather(wd, "z", axis=0, tiled=True).reshape(nz, ny, 2, wd_rows // 2, half)
    wu = both[:, wd_rows:].reshape(hid, feats)

    sums = jnp.sum(gather_directly(after(sums, wd_y), TP), axis=0)
    inv_rms = lax.rsqrt(sums[0] / width + norm_eps)[:, None]
    cross_mean = (sums[1] / width)[:, None]
    d_out = (weighted * inv_rms - normed * inv_rms * inv_rms * inv_rms * cross_mean).astype(bf16)
    gain_part = jnp.sum(upstream * normed * inv_rms, axis=0) * scaled

    mine, theirs = gather_two_steps(d_out)
    d_pre = run(d_pre_kernel, (toks, hid), core, mine, theirs, wd, hidden_pre)
    wu = lax.all_gather(after(wu, mine), "z", axis=0, tiled=True).reshape(nz, hid, feats)

    mine, theirs = gather_two_steps(d_pre)
    g = run(grad_up_kernel, (ntp, hid, feats), core, mine, theirs, after(inputs, wu))
    g = lax.psum_scatter(g.reshape(nz * hid, feats), "z", scatter_dimension=0, tiled=True)
    grad_input = run(grad_input_kernel, (toks, feats), core, mine, theirs, wu)

    grad_gain = jnp.sum(gather_directly(after(gain_part, theirs), FS), axis=0)
    g = after(g, grad_gain)
    grad_up = (summed(exchange(g.reshape(ny, hid // ny, feats), "y")) * scaled).T
    return (grad_input, grad_up, grad_gain)


def solution(mesh):
    torus = Mesh(mesh.devices.reshape(8, 8, mesh.shape["tp"] // 2, 2), ("z", "y", "x", "c"))
    in_specs = (
        P(FS, TP),
        P(FS, TP),
        P(FS, TP),
        P(TP),
        P(TP, FS),
        P(TP, FS),
        P(FS, TP),
    )
    out_specs = (P(FS, TP), P(TP, FS), P(TP))
    return jax.shard_map(
        on_device, mesh=torus, in_specs=in_specs, out_specs=out_specs, check_vma=False
    )
```

time: 267 us -> 197 us (0.74); the launches traced: 264 us -> 197 us
  waiting for transfers between devices: 140 us -> 55.4 us
  blocking collectives: 72 us -> 96.9 us
  starting transfers between devices: 19.6 us -> 10.6 us
  Pallas kernels: 11.2 us -> 14.1 us
    all_gather x3 -> x2, waiting for transfers between devices: 79.1 us -> 25.5 us  [the longest x1 12.9 us: on_device(): lax.all_gather(after(wu, mine), 'z', axis=0, tiled=True)]
    ppermute x2, waiting for transfers between devices: 30.9 us -> 2.55 us  [gather_two_steps(): theirs = lax.ppermute(mine, 'c', [(0, 1), (1, 0)])]
    all_to_all x4 -> x5, blocking collectives: 72 us -> 96.9 us  [exchange(): return lax.all_to_all(chunks, axis, 0, 0, tiled=True)]
    ppermute x2, starting transfers between devices: 13.8 us -> 3.82 us  [gather_two_steps(): theirs = lax.ppermute(mine, 'c', [(0, 1), (1, 0)])]
    reduce_scatter x2 -> x1, waiting for transfers between devices: 29.8 us -> 21.7 us  [on_device(): lax.psum_scatter(g.reshape(nz * hid, feats), 'z', scatter_dimension=0, ti...]
    all_to_all x1, waiting for transfers between devices: 0.01 us -> 5.67 us  [exchange(): return lax.all_to_all(chunks, axis, 0, 0, tiled=True)]
    pallas_call x2 -> x3, Pallas kernels: 11.2 us -> 14.1 us  [run(): pl.pallas_call(kernel, out_shape=jax.ShapeDtypeStruct(shape, bf16), in_sp...]
  transfers between devices with their start and end apart: 8 -> 6, of which waited for: 7 -> 5; matrix products, arithmetic and copies ran while one was open for 1% -> 1% of each run, Pallas kernels for 4% -> 5%
where the time goes in v3:
time: 197 us
  blocking collectives  96.9 us (49%)
  waiting for transfers between devices  55.4 us (28%)
  Pallas kernels  14.1 us (7%)
  between operations  13.9 us (7%)
  starting transfers between devices  10.6 us (5%)
  local copies, waits for them, and re-layouts  2.98 us (2%)
  other arithmetic  2.67 us (1%)
    all_to_all x5, blocking collectives, exchange(): return lax.all_to_all(chunks, axis, 0, 0, tiled=True)  96.9 us
    reduce_scatter x1, waiting for transfers between devices, on_device(): lax.psum_scatter(g.reshape(nz * hid, feats), 'z', scatter_dimension=0, ti...  21.7 us
    pallas_call x3, Pallas kernels, run(): pl.pallas_call(kernel, out_shape=jax.ShapeDtypeStruct(shape, bf16), in_sp...  14.1 us
    all_gather x1, waiting for transfers between devices, on_device(): lax.all_gather(after(wu, mine), 'z', axis=0, tiled=True)  12.9 us
    all_gather x1, waiting for transfers between devices, on_device(): lax.all_gather(wd, 'z', axis=0, tiled=True)  12.6 us
    all_to_all x1, starting transfers between devices, exchange(): return lax.all_to_all(chunks, axis, 0, 0, tiled=True)  6.65 us
    all_to_all x1, waiting for transfers between devices, exchange(): return lax.all_to_all(chunks, axis, 0, 0, tiled=True)  5.67 us
  transfers between devices with their start and end apart: 6, of which 5 were waited for; matrix products, arithmetic and copies ran while one was open for 1% of the time, Pallas kernels for 5%

profile of v3, /device:TPU:6, one launch (start us, length us, event | category | flops | bytes accessed | tf_op | source)
XLA Modules:
  0.0 196.5 jit_solution(17009998734663896680)
XLA Ops:
  7.2 0.0 copy-start.2
  7.2 0.0 copy-start.3
  7.2 0.0 copy-start.5
  7.2 0.0 all-gather.3.cloned.1.call-start
  7.2 0.8 fusion.13
  8.0 0.8 pad_maximum_fusion
  8.8 24.4 %all_to_all.31 = bf16[8,128,256]{2,1,0:T(8,128)(2,1)S(1)} all-to-all(bf16[8,128,256]{2,1,0:T(8,128)(2,1)S(1)} %broadcast_in_dim.10), channel_id=1, replica_groups=mesh['z'=8,'y'=8,'x'=4,'c'=2] {'y'}, dimensions={0} | all-to-all | bytes 1048576 | tf_op jit(solution)/shard_map/all_to_all | solution.py:17
  33.2 0.8 fusion.12
  34.0 0.0 all-gather.3.cloned.1.call-update
  34.1 0.0 all-gather.5.cloned.1.call-start
  34.1 0.0 copy-done.2
  34.1 0.0 copy-done.3
  34.1 0.0 copy-done.5
  34.2 0.2 fusion.3
  34.4 8.0 %all_to_all.32 = f32[8,2,512]{2,1,0:T(2,128)S(1)} all-to-all(f32[8,2,512]{2,1,0:T(2,128)S(1)} %broadcast_in_dim.11), channel_id=1, replica_groups=mesh['z'=8,'y'=8,'x'=4,'c'=2] {'x','c'}, dimensions={0} | all-to-all | bytes 65536 | tf_op jit(solution)/shard_map/all_to_all | solution.py:17
  42.4 0.3 fusion.9
  42.7 0.1 broadcast_in_dim.12
  42.8 17.7 %all_to_all.33.mine = bf16[4,512,256]{2,1,0:T(8,128)(2,1)S(1)} all-to-all(bf16[4,512,256]{2,1,0:T(8,128)(2,1)S(1)} %broadcast_in_dim.12), channel_id=1, replica_groups=mesh['z'=8,'y'=8,'x'=4,'c'=2] {'x'}, dimensions={0} | all-to-all | bytes 2097152 | tf_op jit(solution)/shard_map/all_to_all | solution.py:17
  60.5 0.0 copy-start.1
  60.5 1.9 collective-permute-start
  62.4 0.0 all-gather.5.cloned.1.call-update
  62.5 0.0 reduce-scatter.2.cloned.1.call-start
  62.5 2.5 %collective-permute-done.theirs = bf16[4,512,256]{2,1,0:T(8,128)(2,1)S(1)} collective-permute-done((bf16[4,512,256]{2,1,0:T(8,128)(2,1)S(1)}, bf16[4,512,256]{2,1,0:T(8,128)(2,1)S(1)}, u32[]{:S(2)}, u32[]{:S(2)}) %collective-permute-start) | collective-permute-done | bytes 1048608 | tf_op jit(solution)/shard_map/ppermute | solution.py:27
  65.1 0.0 copy-start.4
  65.1 12.6 %all-gather.3.cloned.1.call-done = bf16[4096,256]{1,0:T(8,128)(2,1)} async-done(((bf16[512,256]{1,0:T(8,128)(2,1)}), bf16[4096,256]{1,0:T(8,128)(2,1)}) %all-gather.3.cloned.1.call-update) | async-done | bytes 2097168 | tf_op jit(solution)/shard_map/all_gather | solution.py:105
  77.6 0.0 copy-done.1
  77.7 0.0 copy-done.4
  77.7 4.4 %d_pre_kernel.1 = bf16[512,512]{1,0:T(8,128)(2,1)} custom-call(s32[1]{0:T(128)} %bitcast.core, bf16[4,512,256]{2,1,0:T(8,128)(2,1)} %copy-done.1, bf16[4,512,256]{2,1,0:T(8,128)(2,1)} %copy-done.4, bf16[8,8,2,32,256]{4,3,2,1,0:T(8,128)(2,1)} %bitcast.16, bf16[512,512]{1,0:T(8,128)(2,1)} %hidden.1), custom_call_target="tpu_custom_call" | custom-call | tf_op jit(solution)/shard_map/d_pre_kernel/pallas_call | solution.py:77
  82.0 1.2 broadcast_in_dim.13
  83.2 24.6 %all_to_all.34.mine = bf16[4,512,512]{2,1,0:T(8,128)(2,1)S(1)} all-to-all(bf16[4,512,512]{2,1,0:T(8,128)(2,1)S(1)} %broadcast_in_dim.13), channel_id=1, replica_groups=mesh['z'=8,'y'=8,'x'=4,'c'=2] {'x'}, dimensions={0} | all-to-all | bytes 4194304 | tf_op jit(solution)/shard_map/all_to_all | solution.py:17
  107.9 0.0 copy-start
  107.9 1.9 collective-permute-start.1
  109.8 12.9 %all-gather.5.cloned.1.call-done = bf16[4096,256]{1,0:T(8,128)(2,1)} async-done(((bf16[512,256]{1,0:T(8,128)(2,1)}), bf16[4096,256]{1,0:T(8,128)(2,1)}) %all-gather.5.cloned.1.call-update) | async-done | bytes 2097168 | tf_op jit(solution)/shard_map/all_gather | solution.py:116
  122.7 0.0 collective-permute-done.1.theirs
  122.7 0.0 copy-done
  122.7 5.0 %grad_up_kernel.1 = bf16[8,512,256]{2,1,0:T(8,128)(2,1)} custom-call(s32[1]{0:T(128)} %bitcast.core, bf16[4,512,512]{2,1,0:T(8,128)(2,1)} %copy-done, bf16[4,512,512]{2,1,0:T(8,128)(2,1)} %collective-permute-done.1.theirs, bf16[512,256]{1,0:T(8,128)(2,1)} %inputs), custom_call_target="tpu_custom_call" | custom-call | tf_op jit(solution)/shard_map/grad_up_kernel/pallas_call | solution.py:77
  127.7 0.0 reduce-scatter.2.cloned.1.call-update
  127.8 22.1 %all_to_all.35 = f32[64,1,256]{2,1,0:T(1,128)S(1)} all-to-all(f32[64,1,256]{2,1,0:T(1,128)S(1)} %broadcast_in_dim.14), channel_id=1, replica_groups=mesh['z'=8,'y'=8,'x'=4,'c'=2] {'z','y'}, dimensions={0} | all-to-all | bytes 131072 | tf_op jit(solution)/shard_map/all_to_all | solution.py:17
  149.9 0.7 reduce_sum.58
  150.5 21.7 %reduce-scatter.2.cloned.1.call-done = bf16[512,256]{1,0:T(8,128)(2,1)} async-done(((bf16[4096,256]{1,0:T(8,128)(2,1)}), bf16[512,256]{1,0:T(8,128)(2,1)}) %reduce-scatter.2.cloned.1.call-update) | async-done | bytes 262160 | tf_op jit(solution)/shard_map/reduce_scatter | solution.py:120
  172.2 6.7 %all-to-all-start.5 = ((bf16[8,64,256]{2,1,0:T(8,128)(2,1)}), bf16[8,64,256]{2,1,0:T(8,128)(2,1)S(1)}, u32[]{:S(2)}, u32[]{:S(2)}) async-start(bf16[8,64,256]{2,1,0:T(8,128)(2,1)} %bitcast.20), calls=%async_computation.6 | async-start | bytes 524288 | tf_op jit(solution)/shard_map/all_to_all | solution.py:17
  178.9 4.8 %grad_input_kernel.1 = bf16[512,256]{1,0:T(8,128)(2,1)} custom-call(s32[1]{0:T(128)} %bitcast.core, bf16[4,512,512]{2,1,0:T(8,128)(2,1)} %copy-done, bf16[4,512,512]{2,1,0:T(8,128)(2,1)} %collective-permute-done.1.theirs, bf16[8,512,256]{2,1,0:T(8,128)(2,1)} %bitcast.17), custom_call_target="tpu_custom_call" | custom-call | tf_op jit(solution)/shard_map/grad_input_kernel/pallas_call | solution.py:77
  183.7 5.7 %all-to-all-done.5 = bf16[8,64,256]{2,1,0:T(8,128)(2,1)S(1)} async-done(((bf16[8,64,256]{2,1,0:T(8,128)(2,1)}), bf16[8,64,256]{2,1,0:T(8,128)(2,1)S(1)}, u32[]{:S(2)}, u32[]{:S(2)}) %all-to-all-start.5) | async-done | bytes 262176 | tf_op jit(solution)/shard_map/all_to_all | solution.py:17
  189.4 0.6 multiply_bitcast_fusion
  (8 shorter events, 0.2 us)
Async XLA Ops:
  7.2 27.0 %copy-start.2 = (bf16[512,256]{1,0:T(8,128)(2,1)S(1)}, bf16[512,256]{1,0:T(8,128)(2,1)}, u32[]{:S(2)}) copy-start(bf16[512,256]{1,0:T(8,128)(2,1)} %param.9) | copy-start | bytes 786436
  7.2 27.0 %copy-start.3 = (bf16[512,256]{1,0:T(8,128)(2,1)S(1)}, bf16[512,256]{1,0:T(8,128)(2,1)}, u32[]{:S(2)}) copy-start(bf16[512,256]{1,0:T(8,128)(2,1)} %param.13) | copy-start | bytes 786436
  7.2 27.0 %copy-start.5 = (f32[256]{0:T(256)S(1)}, f32[256]{0:T(256)}, u32[]{:S(2)}) copy-start(f32[256]{0:T(256)} %param.10) | copy-start | bytes 3076
  7.2 70.5 %all-gather.3.cloned.1.call-start = ((), (), s32[]{:S(2)}) async-start(), calls=%async_computation.7 | async-start | bytes 2359296 | tf_op jit(solution)/shard_map/all_gather | solution.py:105
  34.1 88.6 %all-gather.5.cloned.1.call-start = ((), (), s32[]{:S(2)}) async-start(), calls=%async_computation.8 | async-start | bytes 2359296 | tf_op jit(solution)/shard_map/all_gather | solution.py:116
  60.5 17.1 %copy-start.1 = (bf16[4,512,256]{2,1,0:T(8,128)(2,1)}, bf16[4,512,256]{2,1,0:T(8,128)(2,1)S(1)}, u32[]{:S(2)}) copy-start(bf16[4,512,256]{2,1,0:T(8,128)(2,1)S(1)} %all_to_all.33.mine) | copy-start | bytes 3145732
  60.5 4.5 %collective-permute-start = (bf16[4,512,256]{2,1,0:T(8,128)(2,1)S(1)}, bf16[4,512,256]{2,1,0:T(8,128)(2,1)S(1)}, u32[]{:S(2)}, u32[]{:S(2)}) collective-permute-start(bf16[4,512,256]{2,1,0:T(8,128)(2,1)S(1)} %all_to_all.33.mine), channel_id=1, source_target_pairs={{0,1},{1,0},{2,3},{3,2},{4,5},{5,4},{6,7},{7,6},{8,9},{9,8},{10,11... | collective-permute-start | bytes 3145736 | tf_op jit(solution)/shard_map/ppermute | solution.py:27
  62.5 109.7 %reduce-scatter.2.cloned.1.call-start = ((), (), s32[]{:S(2)}) async-start(), calls=%async_computation.9 | async-start | bytes 2359296 | tf_op jit(solution)/shard_map/reduce_scatter | solution.py:120
  65.1 12.6 %copy-start.4 = (bf16[4,512,256]{2,1,0:T(8,128)(2,1)}, bf16[4,512,256]{2,1,0:T(8,128)(2,1)S(1)}, u32[]{:S(2)}) copy-start(bf16[4,512,256]{2,1,0:T(8,128)(2,1)S(1)} %collective-permute-done.theirs) | copy-start | bytes 3145732
  107.9 14.8 %copy-start = (bf16[4,512,512]{2,1,0:T(8,128)(2,1)}, bf16[4,512,512]{2,1,0:T(8,128)(2,1)S(1)}, u32[]{:S(2)}) copy-start(bf16[4,512,512]{2,1,0:T(8,128)(2,1)S(1)} %all_to_all.34.mine) | copy-start | bytes 6291460
  107.9 14.8 %collective-permute-start.1 = (bf16[4,512,512]{2,1,0:T(8,128)(2,1)S(1)}, bf16[4,512,512]{2,1,0:T(8,128)(2,1)}, u32[]{:S(2)}, u32[]{:S(2)}) collective-permute-start(bf16[4,512,512]{2,1,0:T(8,128)(2,1)S(1)} %all_to_all.34.mine), channel_id=1, source_target_pairs={{0,1},{1,0},{2,3},{3,2},{4,5},{5,4},{6,7},{7,6},{8,9},{9,8},{10,11... | collective-permute-start | bytes 6291464 | tf_op jit(solution)/shard_map/ppermute | solution.py:27
  172.2 17.1 %all-to-all-start.5 = ((bf16[8,64,256]{2,1,0:T(8,128)(2,1)}), bf16[8,64,256]{2,1,0:T(8,128)(2,1)S(1)}, u32[]{:S(2)}, u32[]{:S(2)}) async-start(bf16[8,64,256]{2,1,0:T(8,128)(2,1)} %bitcast.20), calls=%async_computation.6 | async-start | bytes 524288 | tf_op jit(solution)/shard_map/all_to_all | solution.py:17
Sparse Core Ops, SparseCore 0:
  34.2 43.4 all-gather.2
  80.3 42.3 all-gather.4
  127.8 44.3 reduce-scatter.1

commit v4 on v3

v4 whole, which is shorter than its diff:
```python
import jax
import jax.numpy as jnp
from jax import lax
from jax.experimental import pallas as pl
from jax.experimental.pallas import tpu as pltpu
from jax.sharding import Mesh
from jax.sharding import PartitionSpec as P

FS = ("z", "y")
TP = ("x", "c")
bf16 = jnp.bfloat16
f32 = jnp.float32
norm_eps = 1e-06


def exchange(chunks, axis):
    return lax.all_to_all(chunks, axis, 0, 0, tiled=True)


def gather_directly(value, axis):
    n = lax.axis_size(axis)
    return exchange(jnp.broadcast_to(value[None], (n, *value.shape)), axis)


def swapped(value):
    return lax.ppermute(value, "c", [(0, 1), (1, 0)])


def gather_two_steps(value):
    mine = gather_directly(value, "x")
    return mine, swapped(mine)


def after(value, earlier):
    return lax.optimization_barrier((value, earlier))[0]


def summed(parts):
    return jnp.sum(parts.astype(f32), axis=0)


def in_three(value):
    high = lax.reduce_precision(value, 8, 7)
    middle = lax.reduce_precision(value - high, 8, 7)
    return jnp.stack([high, middle, value - high - middle])


def grad_up_kernel(place, mine, theirs, wd, hidden, gain_rows, d_pre_out, g_out):
    c = place[0]
    chips, _, toks, feats = mine.shape
    half = wd.shape[-1]
    for s in range(2):
        cols = slice(s * half, (s + 1) * half)
        acc = jnp.zeros((toks, half), f32)
        for k in range(chips):
            w = wd[:, 2 * k + c, s].reshape(feats, half)
            acc += jnp.dot(mine[k, 0], w, preferred_element_type=f32)
            w = wd[:, 2 * k + 1 - c, s].reshape(feats, half)
            acc += jnp.dot(theirs[k, 0], w, preferred_element_type=f32)
        pre = jnp.maximum(hidden[:, cols].astype(f32), 0.0)
        d_pre_out[:, cols] = (acc * 2.0 * pre).astype(bf16)
    left = d_pre_out[...].T
    hid = hidden.shape[1]
    for k in range(chips):
        g = jnp.dot(left, mine[k, 1], preferred_element_type=f32)
        g_out[2 * k + c, :hid] = g.astype(bf16)
        g = jnp.dot(left, theirs[k, 1], preferred_element_type=f32)
        g_out[2 * k + 1 - c, :hid] = g.astype(bf16)
    for k in range(2 * chips):
        g_out[k, hid:] = gain_rows[...]


def grad_input_kernel(place, mine, theirs, *rest):
    *pieces, out, wu = rest
    c = place[0]
    ny = len(pieces)
    rows = pieces[0].shape[1]
    for d in range(ny):
        source = lax.rem(place[1] + ny - d, ny)
        start = pl.multiple_of(source * rows, rows)
        wu[:, pl.ds(start, rows), :] = pieces[d][...]
    acc = jnp.zeros(out.shape, f32)
    for k in range(mine.shape[0]):
        acc += jnp.dot(mine[k], wu[2 * k + c], preferred_element_type=f32)
        acc += jnp.dot(theirs[k], wu[2 * k + 1 - c], preferred_element_type=f32)
    out[...] = acc.astype(bf16)


def run(kernel, shapes, *operands, scratch=()):
    scalar = pl.BlockSpec(memory_space=pltpu.SMEM)
    whole = pl.BlockSpec(memory_space=pltpu.VMEM)
    return pl.pallas_call(
        kernel,
        out_shape=[jax.ShapeDtypeStruct(shape, bf16) for shape in shapes],
        in_specs=[scalar] + [whole] * (len(operands) - 1),
        out_specs=[whole] * len(shapes),
        scratch_shapes=[pltpu.VMEM(shape, bf16) for shape in scratch],
        name=kernel.__name__,
    )(*operands)


def on_device(inputs, hidden_pre, norm_input, out_gain, w_up, w_down, cotangent):
    nz, ny, ntp = (lax.axis_size(a) for a in ("z", "y", TP))
    toks, feats = inputs.shape
    hid = hidden_pre.shape[1]
    half = hid // 2
    width = feats * ntp
    scaled = (toks * nz * ny) ** (-0.5)
    place = jnp.stack([lax.axis_index("c"), lax.axis_index("y")]).astype(jnp.int32)
    swap = [(a * ntp + b, b * ntp + a) for a in range(nz) for b in range(ntp)]

    normed = norm_input.astype(f32)
    upstream = cotangent.astype(f32)
    weighted = upstream * out_gain
    sums = jnp.stack([jnp.sum(normed * normed, axis=1), jnp.sum(weighted * normed, axis=1)])

    wd = w_down.T
    both = jnp.concatenate([wd[:, :half], wd[:, half:], w_up.T], axis=0)
    both = gather_directly(both, "z")
    wd_rows = 2 * wd.shape[0]
    wd = wd_z = both[:, :wd_rows].reshape(nz * wd_rows, half)
    wd = lax.all_gather(wd, "y", axis=0, tiled=True)
    wd = wd.reshape(ny, nz, 2, wd_rows // 2, half)
    wu = both[:, wd_rows:]

    sums = jnp.sum(gather_directly(after(sums, wd_z), TP), axis=0)
    inv_rms = lax.rsqrt(sums[0] / width + norm_eps)[:, None]
    cross_mean = (sums[1] / width)[:, None]
    d_out = (weighted * inv_rms - normed * inv_rms * inv_rms * inv_rms * cross_mean).astype(bf16)
    gain_part = jnp.sum(upstream * normed * inv_rms, axis=0)

    mine, theirs = gather_two_steps(jnp.stack([d_out, inputs]))
    turn = (jnp.arange(nz) == lax.axis_index("z")).astype(f32)[:, None, None]
    gain_rows = (turn * in_three(gain_part)).reshape(3 * nz, feats).astype(bf16)
    d_pre, g = run(
        grad_up_kernel, [(toks, hid), (ntp, hid + 3 * nz, feats)],
        place, mine, theirs, wd, hidden_pre, gain_rows,
    )
    g = lax.psum_scatter(g.reshape(-1, feats), "z", scatter_dimension=0, tiled=True)

    wu = after(wu, d_pre)
    pieces = [wu]
    for d in range(1, ny):
        pieces.append(lax.ppermute(wu, "y", [(i, (i + d) % ny) for i in range(ny)]))
    mine = gather_directly(d_pre, "x")
    theirs = swapped(after(mine, pieces))
    [grad_input] = run(
        grad_input_kernel, [(toks, feats)], place, mine, theirs, *pieces,
        scratch=[(nz, hid, feats)],
    )

    rows = hid // ny
    gain = summed(g[hid:].reshape(nz, 3, feats))
    gain = in_three(jnp.sum(gain, axis=0)).astype(bf16)
    gain = jnp.broadcast_to(jnp.pad(gain, ((0, 5), (0, 0))), (ny, 8, feats))
    g = jnp.concatenate([g[:hid].reshape(ny, rows, feats), gain], axis=1)
    g = summed(exchange(g, "y")) * scaled
    grad_gain = jnp.sum(g[rows : rows + 3], axis=0)
    grad_up = lax.ppermute(g[:rows], ("z", "x", "c"), swap).T
    return (grad_input, grad_up, grad_gain)


def solution(mesh):
    torus = Mesh(mesh.devices.reshape(8, 8, mesh.shape["tp"] // 2, 2), ("z", "y", "x", "c"))
    in_specs = (
        P(FS, TP),
        P(FS, TP),
        P(FS, TP),
        P(TP),
        P(TP, FS),
        P(TP, FS),
        P(FS, TP),
    )
    out_specs = (P(FS, TP), P(TP, FS), P(TP))
    return jax.shard_map(
        on_device, mesh=torus, in_specs=in_specs, out_specs=out_specs, check_vma=False
    )
```

time: 197 us -> 205 us (1.041); the launches traced: 197 us -> 202 us
  blocking collectives: 96.9 us -> 29 us
  starting transfers between devices: 10.6 us -> 56.2 us
  waiting for transfers between devices: 55.4 us -> 77.1 us
  local copies, waits for them, and re-layouts: 2.98 us -> 8.22 us
  other arithmetic: 2.67 us -> 5.85 us
  Pallas kernels: 14.1 us -> 11.8 us
    all_to_all x5 -> x1, blocking collectives: 96.9 us -> 29 us  [exchange(): return lax.all_to_all(chunks, axis, 0, 0, tiled=True)]
    ppermute x2 -> x10, waiting for transfers between devices: 2.55 us -> 42.3 us  [the longest x7 34.5 us: on_device(): pieces.append(lax.ppermute(wu, 'y', [(i, (i + d) % ny) for i in range(ny)]))]
    ppermute x2 -> x10, starting transfers between devices: 3.82 us -> 32.8 us  [the longest x7 26.7 us: on_device(): pieces.append(lax.ppermute(wu, 'y', [(i, (i + d) % ny) for i in range(ny)]))]
    all_to_all x1 -> x4, waiting for transfers between devices: 5.67 us -> 27.3 us  [exchange(): return lax.all_to_all(chunks, axis, 0, 0, tiled=True)]
    reduce_scatter x1, waiting for transfers between devices: 21.7 us -> 0.02 us  [on_device(): lax.psum_scatter(g.reshape(-1, feats), 'z', scatter_dimension=0, tiled=True)]
    all_gather x2 -> x1, waiting for transfers between devices: 25.5 us -> 6.69 us  [on_device(): wd = lax.all_gather(wd, 'y', axis=0, tiled=True)]
    all_to_all x1 -> x4, starting transfers between devices: 6.65 us -> 23.3 us  [exchange(): return lax.all_to_all(chunks, axis, 0, 0, tiled=True)]
    unnamed x12 -> x29, local copies, waits for them, and re-layouts: 0.02 us -> 2.4 us
  transfers between devices with their start and end apart: 6 -> 16, of which waited for: 5 -> 10; matrix products, arithmetic and copies ran while one was open for 1% -> 4% of each run, Pallas kernels for 5% -> 2%
where the time goes in v4:
time: 205 us; the launch traced here: 202 us
  waiting for transfers between devices  77.1 us (38%)
  starting transfers between devices  56.2 us (27%)
  blocking collectives  29 us (14%)
  between operations  14.3 us (7%)
  Pallas kernels  11.8 us (6%)
  local copies, waits for them, and re-layouts  8.22 us (4%)
  other arithmetic  5.85 us (3%)
    ppermute x7, waiting for transfers between devices, on_device(): pieces.append(lax.ppermute(wu, 'y', [(i, (i + d) % ny) for i in range(ny)]))  34.5 us
    all_to_all x1, blocking collectives, exchange(): return lax.all_to_all(chunks, axis, 0, 0, tiled=True)  29 us
    all_to_all x4, waiting for transfers between devices, exchange(): return lax.all_to_all(chunks, axis, 0, 0, tiled=True)  27.3 us
    ppermute x7, starting transfers between devices, on_device(): pieces.append(lax.ppermute(wu, 'y', [(i, (i + d) % ny) for i in range(ny)]))  26.7 us
    all_to_all x4, starting transfers between devices, exchange(): return lax.all_to_all(chunks, axis, 0, 0, tiled=True)  23.3 us
    pallas_call x2, Pallas kernels, run(): pl.pallas_call(kernel, out_shape=[jax.ShapeDtypeStruct(shape, bf16) for s...  11.8 us
    ppermute x1, waiting for transfers between devices, on_device(): grad_up = lax.ppermute(g[:rows], ('z', 'x', 'c'), swap).T  7.74 us
    all_gather x1, waiting for transfers between devices, on_device(): wd = lax.all_gather(wd, 'y', axis=0, tiled=True)  6.69 us
  transfers between devices with their start and end apart: 16, of which 10 were waited for; matrix products, arithmetic and copies ran while one was open for 4% of the time, Pallas kernels for 2%

profile of v4, /device:TPU:6, one launch (start us, length us, event | category | flops | bytes accessed | tf_op | source)
XLA Modules:
  0.0 202.5 jit_solution(196985101696294894)
XLA Ops:
  7.2 0.0 copy-start.3
  7.2 0.0 copy-start.13
  7.2 0.0 copy-start.2
  7.2 0.8 fusion.20
  8.0 0.8 pad_maximum_fusion.2
  8.8 0.8 broadcast_in_dim.10
  9.6 10.3 %all-to-all-start = ((bf16[8,128,256]{2,1,0:T(8,128)(2,1)}), bf16[8,128,256]{2,1,0:T(8,128)(2,1)S(1)}, u32[]{:S(2)}, u32[]{:S(2)}) async-start(bf16[8,128,256]{2,1,0:T(8,128)(2,1)} %broadcast_in_dim.10), calls=%async_computation | async-start | bytes 1048576 | tf_op jit(solution)/shard_map/all_to_all | solution.py:17
  19.9 1.3 fusion.3
  21.2 16.2 %all-to-all-done = bf16[8,128,256]{2,1,0:T(8,128)(2,1)S(1)} async-done(((bf16[8,128,256]{2,1,0:T(8,128)(2,1)}), bf16[8,128,256]{2,1,0:T(8,128)(2,1)S(1)}, u32[]{:S(2)}, u32[]{:S(2)}) %all-to-all-start) | async-done | bytes 524320 | tf_op jit(solution)/shard_map/all_to_all | solution.py:17
  37.4 0.7 fusion.19
  38.2 0.7 broadcast_in_dim.11
  38.8 4.8 %all-to-all-start.1 = ((f32[8,2,512]{2,1,0:T(2,128)}), f32[8,2,512]{2,1,0:T(2,128)S(1)}, u32[]{:S(2)}, u32[]{:S(2)}) async-start(f32[8,2,512]{2,1,0:T(2,128)} %broadcast_in_dim.11), calls=%async_computation.1 | async-start | bytes 65536 | tf_op jit(solution)/shard_map/all_to_all | solution.py:17
  43.6 0.0 all-gather.2.cloned.1.call-start
  43.6 0.7 all-gather.2.cloned.1.call-update
  44.3 0.0 reduce-scatter.2.cloned.1.call-start
  44.4 2.6 %all-to-all-done.1 = f32[8,2,512]{2,1,0:T(2,128)S(1)} async-done(((f32[8,2,512]{2,1,0:T(2,128)}), f32[8,2,512]{2,1,0:T(2,128)S(1)}, u32[]{:S(2)}, u32[]{:S(2)}) %all-to-all-start.1) | async-done | bytes 32800 | tf_op jit(solution)/shard_map/all_to_all | solution.py:17
  47.0 0.0 copy-done.3
  47.0 0.0 copy-done.13
  47.0 0.0 copy-done.2
  47.1 0.3 fusion.9
  47.4 0.1 pad_maximum_fusion
  47.4 0.1 broadcast_in_dim.12
  47.6 29.0 %all_to_all.25.mine = bf16[4,2,512,256]{3,2,1,0:T(8,128)(2,1)S(1)} all-to-all(bf16[4,2,512,256]{3,2,1,0:T(8,128)(2,1)S(1)} %broadcast_in_dim.12), channel_id=1, replica_groups=mesh['z'=8,'y'=8,'x'=4,'c'=2] {'x'}, dimensions={0} | all-to-all | bytes 4194304 | tf_op jit(solution)/shard_map/all_to_all | solution.py:17
  76.6 1.9 collective-permute-start
  78.5 0.1 mul.94
  78.6 0.1 mul.95
  78.7 0.6 pad_add_fusion.place
  79.3 0.7 multiply_convert_fusion.gain_rows
  80.0 6.7 %all-gather.2.cloned.1.call-done = bf16[4096,256]{1,0:T(8,128)(2,1)} async-done(((bf16[512,256]{1,0:T(8,128)(2,1)}), bf16[4096,256]{1,0:T(8,128)(2,1)}) %all-gather.2.cloned.1.call-update) | async-done | bytes 2097168 | tf_op jit(solution)/shard_map/all_gather | solution.py:122
  86.7 0.0 collective-permute-done.theirs
  86.7 7.0 %grad_up_kernel.1 = (bf16[512,512]{1,0:T(8,128)(2,1)}, bf16[8,536,256]{2,1,0:T(8,128)(2,1)}) custom-call(s32[2]{0:T(128)} %pad_add_fusion.place, bf16[4,2,512,256]{3,2,1,0:T(8,128)(2,1)} %copy-done.1, bf16[4,2,512,256]{3,2,1,0:T(8,128)(2,1)} %collective-permute-done.theirs, bf16[8,8,2,32,256]{4,3,2,1,0:T(8,128)(2,1)} %bitcast.19, bf16[512,512]{1,0:T(8,128)(2,1)} %hidden.1, ...), custom_call_target="tpu_custom_call" | custom-call | tf_op jit(solution)/shard_map/grad_up_kernel/pallas_call | solution.py:92
  93.7 0.0 reduce-scatter.2.cloned.1.call-update
  93.7 1.0 copy-done.5
  94.7 1.5 broadcast_in_dim.13
  96.2 4.8 %all-to-all-start.3 = ((bf16[4,512,512]{2,1,0:T(8,128)(2,1)}), bf16[4,512,512]{2,1,0:T(8,128)(2,1)S(1)}, u32[]{:S(2)}, u32[]{:S(2)}) async-start(bf16[4,512,512]{2,1,0:T(8,128)(2,1)} %broadcast_in_dim.13), calls=%async_computation.3 | async-start | bytes 4194304 | tf_op jit(solution)/shard_map/all_to_all | solution.py:17
  101.0 3.9 %collective-permute-start.7 = (bf16[8,64,256]{2,1,0:T(8,128)(2,1)S(1)}, bf16[8,64,256]{2,1,0:T(8,128)(2,1)S(1)}, u32[]{:S(2)}, u32[]{:S(2)}) collective-permute-start(bf16[8,64,256]{2,1,0:T(8,128)(2,1)S(1)} %get-tuple-element.10.rest_0_), channel_id=1, source_target_pairs={{0,56},{8,0},{16,8},{24,16},{32,24},{40,32},{48,40},{56,48},{1,57}... | collective-permute-start | bytes 786440 | tf_op jit(solution)/shard_map/ppermute | solution.py:144
  104.8 3.2 %collective-permute-start.6 = (bf16[8,64,256]{2,1,0:T(8,128)(2,1)S(1)}, bf16[8,64,256]{2,1,0:T(8,128)(2,1)S(1)}, u32[]{:S(2)}, u32[]{:S(2)}) collective-permute-start(bf16[8,64,256]{2,1,0:T(8,128)(2,1)S(1)} %get-tuple-element.10.rest_0_), channel_id=1, source_target_pairs={{0,48},{8,56},{16,0},{24,8},{32,16},{40,24},{48,32},{56,40},{1,49}... | collective-permute-start | bytes 786440 | tf_op jit(solution)/shard_map/ppermute | solution.py:144
  108.1 4.0 %collective-permute-start.5 = (bf16[8,64,256]{2,1,0:T(8,128)(2,1)S(1)}, bf16[8,64,256]{2,1,0:T(8,128)(2,1)S(1)}, u32[]{:S(2)}, u32[]{:S(2)}) collective-permute-start(bf16[8,64,256]{2,1,0:T(8,128)(2,1)S(1)} %get-tuple-element.10.rest_0_), channel_id=1, source_target_pairs={{0,40},{8,48},{16,56},{24,0},{32,8},{40,16},{48,24},{56,32},{1,41}... | collective-permute-start | bytes 786440 | tf_op jit(solution)/shard_map/ppermute | solution.py:144
  112.1 4.8 %collective-permute-start.4 = (bf16[8,64,256]{2,1,0:T(8,128)(2,1)S(1)}, bf16[8,64,256]{2,1,0:T(8,128)(2,1)S(1)}, u32[]{:S(2)}, u32[]{:S(2)}) collective-permute-start(bf16[8,64,256]{2,1,0:T(8,128)(2,1)S(1)} %get-tuple-element.10.rest_0_), channel_id=1, source_target_pairs={{0,32},{8,40},{16,48},{24,56},{32,0},{40,8},{48,16},{56,24},{1,33}... | collective-permute-start | bytes 786440 | tf_op jit(solution)/shard_map/ppermute | solution.py:144
  116.9 3.7 %collective-permute-start.3 = (bf16[8,64,256]{2,1,0:T(8,128)(2,1)S(1)}, bf16[8,64,256]{2,1,0:T(8,128)(2,1)S(1)}, u32[]{:S(2)}, u32[]{:S(2)}) collective-permute-start(bf16[8,64,256]{2,1,0:T(8,128)(2,1)S(1)} %get-tuple-element.10.rest_0_), channel_id=1, source_target_pairs={{0,24},{8,32},{16,40},{24,48},{32,56},{40,0},{48,8},{56,16},{1,25}... | collective-permute-start | bytes 786440 | tf_op jit(solution)/shard_map/ppermute | solution.py:144
  120.6 0.0 collective-permute-done.7.rest_7_
  120.6 5.2 %collective-permute-start.2 = (bf16[8,64,256]{2,1,0:T(8,128)(2,1)S(1)}, bf16[8,64,256]{2,1,0:T(8,128)(2,1)S(1)}, u32[]{:S(2)}, u32[]{:S(2)}) collective-permute-start(bf16[8,64,256]{2,1,0:T(8,128)(2,1)S(1)} %get-tuple-element.10.rest_0_), channel_id=1, source_target_pairs={{0,16},{8,24},{16,32},{24,40},{32,48},{40,56},{48,0},{56,8},{1,17}... | collective-permute-start | bytes 786440 | tf_op jit(solution)/shard_map/ppermute | solution.py:144
  125.9 7.9 %collective-permute-done.6.rest_6_ = bf16[8,64,256]{2,1,0:T(8,128)(2,1)S(1)} collective-permute-done((bf16[8,64,256]{2,1,0:T(8,128)(2,1)S(1)}, bf16[8,64,256]{2,1,0:T(8,128)(2,1)S(1)}, u32[]{:S(2)}, u32[]{:S(2)}) %collective-permute-start.6) | collective-permute-done | bytes 262176 | tf_op jit(solution)/shard_map/ppermute | solution.py:144
  133.8 1.9 collective-permute-start.1
  135.7 12.5 %collective-permute-done.5.rest_5_ = bf16[8,64,256]{2,1,0:T(8,128)(2,1)S(1)} collective-permute-done((bf16[8,64,256]{2,1,0:T(8,128)(2,1)S(1)}, bf16[8,64,256]{2,1,0:T(8,128)(2,1)S(1)}, u32[]{:S(2)}, u32[]{:S(2)}) %collective-permute-start.5) | collective-permute-done | bytes 262176 | tf_op jit(solution)/shard_map/ppermute | solution.py:144
  148.2 0.0 collective-permute-done.4.rest_4_
  148.2 2.3 %collective-permute-done.3.rest_3_ = bf16[8,64,256]{2,1,0:T(8,128)(2,1)S(1)} collective-permute-done((bf16[8,64,256]{2,1,0:T(8,128)(2,1)S(1)}, bf16[8,64,256]{2,1,0:T(8,128)(2,1)S(1)}, u32[]{:S(2)}, u32[]{:S(2)}) %collective-permute-start.3) | collective-permute-done | bytes 262176 | tf_op jit(solution)/shard_map/ppermute | solution.py:144
  150.5 8.7 %collective-permute-done.2.rest_2_ = bf16[8,64,256]{2,1,0:T(8,128)(2,1)S(1)} collective-permute-done((bf16[8,64,256]{2,1,0:T(8,128)(2,1)S(1)}, bf16[8,64,256]{2,1,0:T(8,128)(2,1)S(1)}, u32[]{:S(2)}, u32[]{:S(2)}) %collective-permute-start.2) | collective-permute-done | bytes 262176 | tf_op jit(solution)/shard_map/ppermute | solution.py:144
  159.3 0.7 copy-done.12
  160.0 3.1 %collective-permute-done.1.rest_1_ = bf16[8,64,256]{2,1,0:T(8,128)(2,1)} collective-permute-done((bf16[8,64,256]{2,1,0:T(8,128)(2,1)S(1)}, bf16[8,64,256]{2,1,0:T(8,128)(2,1)}, u32[]{:S(2)}, u32[]{:S(2)}) %collective-permute-start.1) | collective-permute-done | bytes 262176 | tf_op jit(solution)/shard_map/ppermute | solution.py:144
  163.0 0.0 all-to-all-done.3.mine
  163.0 1.9 collective-permute-start.8
  165.0 0.0 reduce-scatter.2.cloned.1.call-done
  165.0 1.0 slice.46
  166.0 0.7 convert_reduce_fusion.1
  166.7 0.7 pad_maximum_fusion.1
  167.5 3.4 %all-to-all-start.4 = ((bf16[8,72,256]{2,1,0:T(8,128)(2,1)}), bf16[8,72,256]{2,1,0:T(8,128)(2,1)S(1)}, u32[]{:S(2)}, u32[]{:S(2)}) async-start(bf16[8,72,256]{2,1,0:T(8,128)(2,1)} %pad_maximum_fusion.1), calls=%async_computation.5 | async-start | bytes 589824 | tf_op jit(solution)/shard_map/all_to_all | solution.py:17
  170.9 0.0 collective-permute-done.8.theirs
  170.9 4.9 %grad_input_kernel.1 = bf16[512,256]{1,0:T(8,128)(2,1)} custom-call(s32[2]{0:T(128)} %pad_add_fusion.place, bf16[4,512,512]{2,1,0:T(8,128)(2,1)} %copy-done, bf16[4,512,512]{2,1,0:T(8,128)(2,1)} %collective-permute-done.8.theirs, bf16[8,64,256]{2,1,0:T(8,128)(2,1)} %copy-done.4, bf16[8,64,256]{2,1,0:T(8,128)(2,1)} %collective-permute-done.1.rest_1_, ...), custom_call_target="tpu_custom_call" | custom-call | tf_op jit(solution)/shard_map/grad_input_kernel/pallas_call | solution.py:92
  175.8 8.5 %all-to-all-done.4 = bf16[8,72,256]{2,1,0:T(8,128)(2,1)S(1)} async-done(((bf16[8,72,256]{2,1,0:T(8,128)(2,1)}), bf16[8,72,256]{2,1,0:T(8,128)(2,1)S(1)}, u32[]{:S(2)}, u32[]{:S(2)}) %all-to-all-start.4) | async-done | bytes 294944 | tf_op jit(solution)/shard_map/all_to_all | solution.py:17
  184.4 2.3 %collective-permute-start.9 = (f32[64,256]{1,0:T(8,128)S(1)}, f32[64,256]{1,0:T(8,128)S(1)}, u32[]{:S(2)}, u32[]{:S(2)}) collective-permute-start(f32[64,256]{1,0:T(8,128)S(1)} %slice.48), channel_id=1, source_target_pairs={{0,0},{1,64},{2,128},{3,192},{4,256},{5,320},{6,384},{7,448},{64,1... | collective-permute-start | bytes 196616 | tf_op jit(solution)/shard_map/ppermute | solution.py:159
  186.7 0.6 slice_reduce_fusion
  187.3 7.7 %collective-permute-done.9 = f32[64,256]{1,0:T(8,128)S(1)} collective-permute-done((f32[64,256]{1,0:T(8,128)S(1)}, f32[64,256]{1,0:T(8,128)S(1)}, u32[]{:S(2)}, u32[]{:S(2)}) %collective-permute-start.9) | collective-permute-done | bytes 65568 | tf_op jit(solution)/shard_map/ppermute | solution.py:159
  195.0 0.6 copy.15
  (34 shorter events, 0.2 us)
Async XLA Ops:
  7.2 39.9 %copy-start.3 = (bf16[512,256]{1,0:T(8,128)(2,1)S(1)}, bf16[512,256]{1,0:T(8,128)(2,1)}, u32[]{:S(2)}) copy-start(bf16[512,256]{1,0:T(8,128)(2,1)} %param.13) | copy-start | bytes 786436
  7.2 39.9 %copy-start.13 = (f32[256]{0:T(256)S(1)}, f32[256]{0:T(256)}, u32[]{:S(2)}) copy-start(f32[256]{0:T(256)} %param.10) | copy-start | bytes 3076
  7.2 39.9 %copy-start.2 = (bf16[512,256]{1,0:T(8,128)(2,1)S(1)}, bf16[512,256]{1,0:T(8,128)(2,1)}, u32[]{:S(2)}) copy-start(bf16[512,256]{1,0:T(8,128)(2,1)} %param.9) | copy-start | bytes 786436
  8.8 38.6 %copy-start.6 = (bf16[512,256]{1,0:T(8,128)(2,1)S(1)}, bf16[512,256]{1,0:T(8,128)(2,1)}, u32[]{:S(2)}) copy-start(bf16[512,256]{1,0:T(8,128)(2,1)} %param.7) | copy-start | bytes 786436
  9.6 27.8 %all-to-all-start = ((bf16[8,128,256]{2,1,0:T(8,128)(2,1)}), bf16[8,128,256]{2,1,0:T(8,128)(2,1)S(1)}, u32[]{:S(2)}, u32[]{:S(2)}) async-start(bf16[8,128,256]{2,1,0:T(8,128)(2,1)} %broadcast_in_dim.10), calls=%async_computation | async-start | bytes 1048576 | tf_op jit(solution)/shard_map/all_to_all | solution.py:17
  38.1 95.6 %copy-start.4 = (bf16[8,64,256]{2,1,0:T(8,128)(2,1)}, bf16[8,64,256]{2,1,0:T(8,128)(2,1)S(1)}, u32[]{:S(2)}) copy-start(bf16[8,64,256]{2,1,0:T(8,128)(2,1)S(1)} %get-tuple-element.10.rest_0_) | copy-start | bytes 786436
  38.8 8.2 %all-to-all-start.1 = ((f32[8,2,512]{2,1,0:T(2,128)}), f32[8,2,512]{2,1,0:T(2,128)S(1)}, u32[]{:S(2)}, u32[]{:S(2)}) async-start(f32[8,2,512]{2,1,0:T(2,128)} %broadcast_in_dim.11), calls=%async_computation.1 | async-start | bytes 65536 | tf_op jit(solution)/shard_map/all_to_all | solution.py:17
  43.6 43.1 %all-gather.2.cloned.1.call-start = ((), (), s32[]{:S(2)}) async-start(), calls=%async_computation.6 | async-start | bytes 2359296 | tf_op jit(solution)/shard_map/all_gather | solution.py:122
  44.3 120.6 %reduce-scatter.2.cloned.1.call-start = ((), (), s32[]{:S(2)}) async-start(), calls=%async_computation.7 | async-start | bytes 2469888 | tf_op jit(solution)/shard_map/reduce_scatter | solution.py:139
  76.6 10.1 %copy-start.1 = (bf16[4,2,512,256]{3,2,1,0:T(8,128)(2,1)}, bf16[4,2,512,256]{3,2,1,0:T(8,128)(2,1)S(1)}, u32[]{:S(2)}) copy-start(bf16[4,2,512,256]{3,2,1,0:T(8,128)(2,1)S(1)} %all_to_all.25.mine) | copy-start | bytes 6291460
  76.6 10.1 %collective-permute-start = (bf16[4,2,512,256]{3,2,1,0:T(8,128)(2,1)S(1)}, bf16[4,2,512,256]{3,2,1,0:T(8,128)(2,1)}, u32[]{:S(2)}, u32[]{:S(2)}) collective-permute-start(bf16[4,2,512,256]{3,2,1,0:T(8,128)(2,1)S(1)} %all_to_all.25.mine), channel_id=1, source_target_pairs={{0,1},{1,0},{2,3},{3,2},{4,5},{5,4},{6,7},{7,6},{8,9},{9,8},{10,11... | collective-permute-start | bytes 6291464 | tf_op jit(solution)/shard_map/ppermute | solution.py:26
  93.7 1.0 copy-start.5
  96.2 66.8 %all-to-all-start.3 = ((bf16[4,512,512]{2,1,0:T(8,128)(2,1)}), bf16[4,512,512]{2,1,0:T(8,128)(2,1)S(1)}, u32[]{:S(2)}, u32[]{:S(2)}) async-start(bf16[4,512,512]{2,1,0:T(8,128)(2,1)} %broadcast_in_dim.13), calls=%async_computation.3 | async-start | bytes 4194304 | tf_op jit(solution)/shard_map/all_to_all | solution.py:17
  101.0 19.6 %collective-permute-start.7 = (bf16[8,64,256]{2,1,0:T(8,128)(2,1)S(1)}, bf16[8,64,256]{2,1,0:T(8,128)(2,1)S(1)}, u32[]{:S(2)}, u32[]{:S(2)}) collective-permute-start(bf16[8,64,256]{2,1,0:T(8,128)(2,1)S(1)} %get-tuple-element.10.rest_0_), channel_id=1, source_target_pairs={{0,56},{8,0},{16,8},{24,16},{32,24},{40,32},{48,40},{56,48},{1,57}... | collective-permute-start | bytes 786440 | tf_op jit(solution)/shard_map/ppermute | solution.py:144
  104.8 28.9 %collective-permute-start.6 = (bf16[8,64,256]{2,1,0:T(8,128)(2,1)S(1)}, bf16[8,64,256]{2,1,0:T(8,128)(2,1)S(1)}, u32[]{:S(2)}, u32[]{:S(2)}) collective-permute-start(bf16[8,64,256]{2,1,0:T(8,128)(2,1)S(1)} %get-tuple-element.10.rest_0_), channel_id=1, source_target_pairs={{0,48},{8,56},{16,0},{24,8},{32,16},{40,24},{48,32},{56,40},{1,49}... | collective-permute-start | bytes 786440 | tf_op jit(solution)/shard_map/ppermute | solution.py:144
  108.1 40.1 %collective-permute-start.5 = (bf16[8,64,256]{2,1,0:T(8,128)(2,1)S(1)}, bf16[8,64,256]{2,1,0:T(8,128)(2,1)S(1)}, u32[]{:S(2)}, u32[]{:S(2)}) collective-permute-start(bf16[8,64,256]{2,1,0:T(8,128)(2,1)S(1)} %get-tuple-element.10.rest_0_), channel_id=1, source_target_pairs={{0,40},{8,48},{16,56},{24,0},{32,8},{40,16},{48,24},{56,32},{1,41}... | collective-permute-start | bytes 786440 | tf_op jit(solution)/shard_map/ppermute | solution.py:144
  112.1 36.1 %collective-permute-start.4 = (bf16[8,64,256]{2,1,0:T(8,128)(2,1)S(1)}, bf16[8,64,256]{2,1,0:T(8,128)(2,1)S(1)}, u32[]{:S(2)}, u32[]{:S(2)}) collective-permute-start(bf16[8,64,256]{2,1,0:T(8,128)(2,1)S(1)} %get-tuple-element.10.rest_0_), channel_id=1, source_target_pairs={{0,32},{8,40},{16,48},{24,56},{32,0},{40,8},{48,16},{56,24},{1,33}... | collective-permute-start | bytes 786440 | tf_op jit(solution)/shard_map/ppermute | solution.py:144
  116.9 33.6 %collective-permute-start.3 = (bf16[8,64,256]{2,1,0:T(8,128)(2,1)S(1)}, bf16[8,64,256]{2,1,0:T(8,128)(2,1)S(1)}, u32[]{:S(2)}, u32[]{:S(2)}) collective-permute-start(bf16[8,64,256]{2,1,0:T(8,128)(2,1)S(1)} %get-tuple-element.10.rest_0_), channel_id=1, source_target_pairs={{0,24},{8,32},{16,40},{24,48},{32,56},{40,0},{48,8},{56,16},{1,25}... | collective-permute-start | bytes 786440 | tf_op jit(solution)/shard_map/ppermute | solution.py:144
  120.6 50.3 %copy-start.7 = (bf16[8,64,256]{2,1,0:T(8,128)(2,1)}, bf16[8,64,256]{2,1,0:T(8,128)(2,1)S(1)}, u32[]{:S(2)}) copy-start(bf16[8,64,256]{2,1,0:T(8,128)(2,1)S(1)} %collective-permute-done.7.rest_7_) | copy-start | bytes 786436
  120.6 38.6 %collective-permute-start.2 = (bf16[8,64,256]{2,1,0:T(8,128)(2,1)S(1)}, bf16[8,64,256]{2,1,0:T(8,128)(2,1)S(1)}, u32[]{:S(2)}, u32[]{:S(2)}) collective-permute-start(bf16[8,64,256]{2,1,0:T(8,128)(2,1)S(1)} %get-tuple-element.10.rest_0_), channel_id=1, source_target_pairs={{0,16},{8,24},{16,32},{24,40},{32,48},{40,56},{48,0},{56,8},{1,17}... | collective-permute-start | bytes 786440 | tf_op jit(solution)/shard_map/ppermute | solution.py:144
  133.8 37.2 %copy-start.8 = (bf16[8,64,256]{2,1,0:T(8,128)(2,1)}, bf16[8,64,256]{2,1,0:T(8,128)(2,1)S(1)}, u32[]{:S(2)}) copy-start(bf16[8,64,256]{2,1,0:T(8,128)(2,1)S(1)} %collective-permute-done.6.rest_6_) | copy-start | bytes 786436
  133.8 29.3 %collective-permute-start.1 = (bf16[8,64,256]{2,1,0:T(8,128)(2,1)S(1)}, bf16[8,64,256]{2,1,0:T(8,128)(2,1)}, u32[]{:S(2)}, u32[]{:S(2)}) collective-permute-start(bf16[8,64,256]{2,1,0:T(8,128)(2,1)S(1)} %get-tuple-element.10.rest_0_), channel_id=1, source_target_pairs={{0,8},{8,16},{16,24},{24,32},{32,40},{40,48},{48,56},{56,0},{1,9},... | collective-permute-start | bytes 786440 | tf_op jit(solution)/shard_map/ppermute | solution.py:144
  148.2 22.7 %copy-start.9 = (bf16[8,64,256]{2,1,0:T(8,128)(2,1)}, bf16[8,64,256]{2,1,0:T(8,128)(2,1)S(1)}, u32[]{:S(2)}) copy-start(bf16[8,64,256]{2,1,0:T(8,128)(2,1)S(1)} %collective-permute-done.5.rest_5_) | copy-start | bytes 786436
  148.2 19.3 %copy-start.10 = (bf16[8,64,256]{2,1,0:T(8,128)(2,1)}, bf16[8,64,256]{2,1,0:T(8,128)(2,1)S(1)}, u32[]{:S(2)}) copy-start(bf16[8,64,256]{2,1,0:T(8,128)(2,1)S(1)} %collective-permute-done.4.rest_4_) | copy-start | bytes 786436
  150.5 8.7 %copy-start.11 = (bf16[8,64,256]{2,1,0:T(8,128)(2,1)}, bf16[8,64,256]{2,1,0:T(8,128)(2,1)S(1)}, u32[]{:S(2)}) copy-start(bf16[8,64,256]{2,1,0:T(8,128)(2,1)S(1)} %collective-permute-done.3.rest_3_) | copy-start | bytes 786436
  159.3 0.7 copy-start.12
  163.0 7.9 %copy-start = (bf16[4,512,512]{2,1,0:T(8,128)(2,1)}, bf16[4,512,512]{2,1,0:T(8,128)(2,1)S(1)}, u32[]{:S(2)}) copy-start(bf16[4,512,512]{2,1,0:T(8,128)(2,1)S(1)} %all-to-all-done.3.mine) | copy-start | bytes 6291460
  163.0 7.9 %collective-permute-start.8 = (bf16[4,512,512]{2,1,0:T(8,128)(2,1)S(1)}, bf16[4,512,512]{2,1,0:T(8,128)(2,1)}, u32[]{:S(2)}, u32[]{:S(2)}) collective-permute-start(bf16[4,512,512]{2,1,0:T(8,128)(2,1)S(1)} %all-to-all-done.3.mine), channel_id=1, source_target_pairs={{0,1},{1,0},{2,3},{3,2},{4,5},{5,4},{6,7},{7,6},{8,9},{9,8},{10,11... | collective-permute-start | bytes 6291464 | tf_op jit(solution)/shard_map/ppermute | solution.py:26
  167.5 16.9 %all-to-all-start.4 = ((bf16[8,72,256]{2,1,0:T(8,128)(2,1)}), bf16[8,72,256]{2,1,0:T(8,128)(2,1)S(1)}, u32[]{:S(2)}, u32[]{:S(2)}) async-start(bf16[8,72,256]{2,1,0:T(8,128)(2,1)} %pad_maximum_fusion.1), calls=%async_computation.5 | async-start | bytes 589824 | tf_op jit(solution)/shard_map/all_to_all | solution.py:17
  184.4 10.6 %collective-permute-start.9 = (f32[64,256]{1,0:T(8,128)S(1)}, f32[64,256]{1,0:T(8,128)S(1)}, u32[]{:S(2)}, u32[]{:S(2)}) collective-permute-start(f32[64,256]{1,0:T(8,128)S(1)} %slice.48), channel_id=1, source_target_pairs={{0,0},{1,64},{2,128},{3,192},{4,256},{5,320},{6,384},{7,448},{64,1... | collective-permute-start | bytes 196616 | tf_op jit(solution)/shard_map/ppermute | solution.py:159
Sparse Core Ops, SparseCore 0:
  47.1 39.6 all-gather.1
  93.8 44.9 reduce-scatter.1

commit v5 on v4

--- a/solution.py
+++ b/solution.py
@@ -22,8 +22,13 @@
     return exchange(jnp.broadcast_to(value[None], (n, *value.shape)), axis)
 
 
+def shifted(value, axis, by):
+    n = lax.axis_size(axis)
+    return lax.ppermute(value, axis, [(i, (i + by) % n) for i in range(n)])
+
+
 def swapped(value):
-    return lax.ppermute(value, "c", [(0, 1), (1, 0)])
+    return shifted(value, "c", 1)
 
 
 def gather_two_steps(value):
@@ -95,11 +100,10 @@
         in_specs=[scalar] + [whole] * (len(operands) - 1),
         out_specs=[whole] * len(shapes),
         scratch_shapes=[pltpu.VMEM(shape, bf16) for shape in scratch],
-        name=kernel.__name__,
     )(*operands)
 
 
-def on_device(inputs, hidden_pre, norm_input, out_gain, w_up, w_down, cotangent):
+def one_device(inputs, hidden_pre, norm_input, out_gain, w_up, w_down, cotangent):
     nz, ny, ntp = (lax.axis_size(a) for a in ("z", "y", TP))
     toks, feats = inputs.shape
     hid = hidden_pre.shape[1]
@@ -123,7 +127,8 @@
     wd = wd.reshape(ny, nz, 2, wd_rows // 2, half)
     wu = both[:, wd_rows:]
 
-    sums = jnp.sum(gather_directly(after(sums, wd_z), TP), axis=0)
+    sums = gather_directly(after(sums, wd_z), TP)
+    sums = jnp.sum(sums, axis=0)
     inv_rms = lax.rsqrt(sums[0] / width + norm_eps)[:, None]
     cross_mean = (sums[1] / width)[:, None]
     d_out = (weighted * inv_rms - normed * inv_rms * inv_rms * inv_rms * cross_mean).astype(bf16)
@@ -139,9 +144,11 @@
     g = lax.psum_scatter(g.reshape(-1, feats), "z", scatter_dimension=0, tiled=True)
 
     wu = after(wu, d_pre)
-    pieces = [wu]
-    for d in range(1, ny):
-        pieces.append(lax.ppermute(wu, "y", [(i, (i + d) % ny) for i in range(ny)]))
+    pieces = [wu] * ny
+    for d in range(1, ny // 2 + 1):
+        pieces[d] = shifted(pieces[d - 1], "y", 1)
+        if ny - d > d:
+            pieces[ny - d] = shifted(pieces[(ny - d + 1) % ny], "y", -1)
     mine = gather_directly(d_pre, "x")
     theirs = swapped(after(mine, pieces))
     [grad_input] = run(
@@ -173,5 +180,5 @@
     )
     out_specs = (P(FS, TP), P(TP, FS), P(TP))
     return jax.shard_map(
-        on_device, mesh=torus, in_specs=in_specs, out_specs=out_specs, check_vma=False
+        one_device, mesh=torus, in_specs=in_specs, out_specs=out_specs, check_vma=False
     )

time: 205 us -> 184 us (0.90)
  waiting for transfers between devices: 77.1 us -> 51.8 us
  starting transfers between devices: 56.2 us -> 60 us
    ppermute x10, waiting for transfers between devices: 42.3 us -> 17.2 us  [the longest x9 14.1 us: shifted(): return lax.ppermute(value, axis, [(i, (i + by) % n) for i in range(n)])]
    all_to_all x4, starting transfers between devices: 23.3 us -> 26.4 us  [exchange(): return lax.all_to_all(chunks, axis, 0, 0, tiled=True)]
  transfers between devices with their start and end apart: 16 -> 16, of which waited for: 10 -> 9; matrix products, arithmetic and copies ran while one was open for 4% -> 4% of each run, Pallas kernels for 2% -> 3%
where the time goes in v5:
time: 184 us; the launch traced here: 181 us
  starting transfers between devices  60 us (33%)
  waiting for transfers between devices  51.8 us (28%)
  blocking collectives  29 us (16%)
  between operations  14.4 us (8%)
  Pallas kernels  11.8 us (6%)
  local copies, waits for them, and re-layouts  8.21 us (4%)
  other arithmetic  5.85 us (3%)
    all_to_all x1, blocking collectives, exchange(): return lax.all_to_all(chunks, axis, 0, 0, tiled=True)  29 us
    all_to_all x4, waiting for transfers between devices, exchange(): return lax.all_to_all(chunks, axis, 0, 0, tiled=True)  27.2 us
    ppermute x9, starting transfers between devices, shifted(): return lax.ppermute(value, axis, [(i, (i + by) % n) for i in range(n)])  26.9 us
    all_to_all x4, starting transfers between devices, exchange(): return lax.all_to_all(chunks, axis, 0, 0, tiled=True)  26.4 us
    ppermute x9, waiting for transfers between devices, shifted(): return lax.ppermute(value, axis, [(i, (i + by) % n) for i in range(n)])  14.1 us
    pallas_call x2, Pallas kernels, run(): pl.pallas_call(kernel, out_shape=[jax.ShapeDtypeStruct(shape, bf16) for s...  11.8 us
    all_gather x1, waiting for transfers between devices, one_device(): wd = lax.all_gather(wd, 'y', axis=0, tiled=True)  6.69 us
    ppermute x1, starting transfers between devices, one_device(): grad_up = lax.ppermute(g[:rows], ('z', 'x', 'c'), swap).T  6.69 us
  transfers between devices with their start and end apart: 16, of which 9 were waited for; matrix products, arithmetic and copies ran while one was open for 4% of the time, Pallas kernels for 3%

profile of v5, /device:TPU:6, one launch (start us, length us, event | category | flops | bytes accessed | tf_op | source)
XLA Modules:
  0.0 181.1 jit_solution(11270562538109753854)
XLA Ops:
  7.2 0.0 copy-start.3
  7.2 0.0 copy-start.13
  7.2 0.0 copy-start.2
  7.2 0.8 fusion.20
  8.0 0.8 pad_maximum_fusion.2
  8.8 0.8 broadcast_in_dim.10
  9.6 10.3 %all-to-all-start = ((bf16[8,128,256]{2,1,0:T(8,128)(2,1)}), bf16[8,128,256]{2,1,0:T(8,128)(2,1)S(1)}, u32[]{:S(2)}, u32[]{:S(2)}) async-start(bf16[8,128,256]{2,1,0:T(8,128)(2,1)} %broadcast_in_dim.10), calls=%async_computation | async-start | bytes 1048576 | tf_op jit(solution)/shard_map/all_to_all | solution.py:17
  19.9 1.3 fusion.3
  21.2 16.2 %all-to-all-done = bf16[8,128,256]{2,1,0:T(8,128)(2,1)S(1)} async-done(((bf16[8,128,256]{2,1,0:T(8,128)(2,1)}), bf16[8,128,256]{2,1,0:T(8,128)(2,1)S(1)}, u32[]{:S(2)}, u32[]{:S(2)}) %all-to-all-start) | async-done | bytes 524320 | tf_op jit(solution)/shard_map/all_to_all | solution.py:17
  37.4 0.7 fusion.19
  38.2 0.7 broadcast_in_dim.11
  38.8 4.8 %all-to-all-start.1 = ((f32[8,2,512]{2,1,0:T(2,128)}), f32[8,2,512]{2,1,0:T(2,128)S(1)}, u32[]{:S(2)}, u32[]{:S(2)}) async-start(f32[8,2,512]{2,1,0:T(2,128)} %broadcast_in_dim.11), calls=%async_computation.1 | async-start | bytes 65536 | tf_op jit(solution)/shard_map/all_to_all | solution.py:17
  43.6 0.0 all-gather.2.cloned.1.call-start
  43.6 0.7 all-gather.2.cloned.1.call-update
  44.3 0.0 reduce-scatter.2.cloned.1.call-start
  44.4 2.6 %all-to-all-done.1 = f32[8,2,512]{2,1,0:T(2,128)S(1)} async-done(((f32[8,2,512]{2,1,0:T(2,128)}), f32[8,2,512]{2,1,0:T(2,128)S(1)}, u32[]{:S(2)}, u32[]{:S(2)}) %all-to-all-start.1) | async-done | bytes 32800 | tf_op jit(solution)/shard_map/all_to_all | solution.py:17
  47.1 0.3 fusion.9
  47.4 0.0 copy-done.6
  47.4 0.1 pad_maximum_fusion
  47.4 0.1 broadcast_in_dim.12
  47.6 29.0 %all_to_all.25.mine = bf16[4,2,512,256]{3,2,1,0:T(8,128)(2,1)S(1)} all-to-all(bf16[4,2,512,256]{3,2,1,0:T(8,128)(2,1)S(1)} %broadcast_in_dim.12), channel_id=1, replica_groups=mesh['z'=8,'y'=8,'x'=4,'c'=2] {'x'}, dimensions={0} | all-to-all | bytes 4194304 | tf_op jit(solution)/shard_map/all_to_all | solution.py:17
  76.6 1.9 %collective-permute-start = (bf16[4,2,512,256]{3,2,1,0:T(8,128)(2,1)S(1)}, bf16[4,2,512,256]{3,2,1,0:T(8,128)(2,1)}, u32[]{:S(2)}, u32[]{:S(2)}) collective-permute-start(bf16[4,2,512,256]{3,2,1,0:T(8,128)(2,1)S(1)} %all_to_all.25.mine), channel_id=1, source_target_pairs={{0,1},{1,0},{2,3},{3,2},{4,5},{5,4},{6,7},{7,6},{8,9},{9,8},{10,11... | collective-permute-start | bytes 6291464 | tf_op jit(solution)/shard_map/ppermute | solution.py:27
  78.5 0.1 mul.94
  78.6 0.1 mul.95
  78.7 0.6 pad_add_fusion.place
  79.3 0.7 multiply_convert_fusion.gain_rows
  80.0 6.7 %all-gather.2.cloned.1.call-done = bf16[4096,256]{1,0:T(8,128)(2,1)} async-done(((bf16[512,256]{1,0:T(8,128)(2,1)}), bf16[4096,256]{1,0:T(8,128)(2,1)}) %all-gather.2.cloned.1.call-update) | async-done | bytes 2097168 | tf_op jit(solution)/shard_map/all_gather | solution.py:126
  86.7 0.0 collective-permute-done.theirs
  86.7 0.0 copy-done.1
  86.7 7.0 %shard_map.94 = (bf16[512,512]{1,0:T(8,128)(2,1)}, bf16[8,536,256]{2,1,0:T(8,128)(2,1)}) custom-call(s32[2]{0:T(128)} %pad_add_fusion.place, bf16[4,2,512,256]{3,2,1,0:T(8,128)(2,1)} %copy-done.1, bf16[4,2,512,256]{3,2,1,0:T(8,128)(2,1)} %collective-permute-done.theirs, bf16[8,8,2,32,256]{4,3,2,1,0:T(8,128)(2,1)} %bitcast.19, bf16[512,512]{1,0:T(8,128)(2,1)} %hidden.1, ...), custom_call_target="tpu_custom_call" | custom-call | tf_op jit(solution)/shard_map/pallas_call | solution.py:97
  93.7 0.0 reduce-scatter.2.cloned.1.call-update
  93.7 1.0 copy-done.5
  94.7 1.5 broadcast_in_dim.13
  96.2 4.8 %all-to-all-start.3 = ((bf16[4,512,512]{2,1,0:T(8,128)(2,1)}), bf16[4,512,512]{2,1,0:T(8,128)(2,1)S(1)}, u32[]{:S(2)}, u32[]{:S(2)}) async-start(bf16[4,512,512]{2,1,0:T(8,128)(2,1)} %broadcast_in_dim.13), calls=%async_computation.3 | async-start | bytes 4194304 | tf_op jit(solution)/shard_map/all_to_all | solution.py:17
  101.0 3.1 %collective-permute-start.1 = (bf16[8,64,256]{2,1,0:T(8,128)(2,1)S(1)}, bf16[8,64,256]{2,1,0:T(8,128)(2,1)S(1)}, u32[]{:S(2)}, u32[]{:S(2)}) collective-permute-start(bf16[8,64,256]{2,1,0:T(8,128)(2,1)S(1)} %get-tuple-element.10.rest_0_), channel_id=1, source_target_pairs={{0,8},{8,16},{16,24},{24,32},{32,40},{40,48},{48,56},{56,0},{1,9},... | collective-permute-start | bytes 786440 | tf_op jit(solution)/shard_map/ppermute | solution.py:27
  104.1 3.9 %collective-permute-start.5 = (bf16[8,64,256]{2,1,0:T(8,128)(2,1)S(1)}, bf16[8,64,256]{2,1,0:T(8,128)(2,1)S(1)}, u32[]{:S(2)}, u32[]{:S(2)}) collective-permute-start(bf16[8,64,256]{2,1,0:T(8,128)(2,1)S(1)} %get-tuple-element.10.rest_0_), channel_id=1, source_target_pairs={{0,56},{8,0},{16,8},{24,16},{32,24},{40,32},{48,40},{56,48},{1,57}... | collective-permute-start | bytes 786440 | tf_op jit(solution)/shard_map/ppermute | solution.py:27
  108.0 2.4 %collective-permute-done.1.rest_1_ = bf16[8,64,256]{2,1,0:T(8,128)(2,1)S(1)} collective-permute-done((bf16[8,64,256]{2,1,0:T(8,128)(2,1)S(1)}, bf16[8,64,256]{2,1,0:T(8,128)(2,1)S(1)}, u32[]{:S(2)}, u32[]{:S(2)}) %collective-permute-start.1) | collective-permute-done | bytes 262176 | tf_op jit(solution)/shard_map/ppermute | solution.py:27
  110.4 1.9 %collective-permute-start.2 = (bf16[8,64,256]{2,1,0:T(8,128)(2,1)S(1)}, bf16[8,64,256]{2,1,0:T(8,128)(2,1)S(1)}, u32[]{:S(2)}, u32[]{:S(2)}) collective-permute-start(bf16[8,64,256]{2,1,0:T(8,128)(2,1)S(1)} %collective-permute-done.1.rest_1_), channel_id=1, source_target_pairs={{0,8},{8,16},{16,24},{24,32},{32,40},{40,48},{48,56},{56,0},{1,9},... | collective-permute-start | bytes 786440 | tf_op jit(solution)/shard_map/ppermute | solution.py:27
  112.4 0.0 collective-permute-done.5.rest_7_
  112.4 5.1 %collective-permute-start.6 = (bf16[8,64,256]{2,1,0:T(8,128)(2,1)S(1)}, bf16[8,64,256]{2,1,0:T(8,128)(2,1)S(1)}, u32[]{:S(2)}, u32[]{:S(2)}) collective-permute-start(bf16[8,64,256]{2,1,0:T(8,128)(2,1)S(1)} %collective-permute-done.5.rest_7_), channel_id=1, source_target_pairs={{0,56},{8,0},{16,8},{24,16},{32,24},{40,32},{48,40},{56,48},{1,57}... | collective-permute-start | bytes 786440 | tf_op jit(solution)/shard_map/ppermute | solution.py:27
  117.5 2.4 %collective-permute-done.2.rest_2_ = bf16[8,64,256]{2,1,0:T(8,128)(2,1)S(1)} collective-permute-done((bf16[8,64,256]{2,1,0:T(8,128)(2,1)S(1)}, bf16[8,64,256]{2,1,0:T(8,128)(2,1)S(1)}, u32[]{:S(2)}, u32[]{:S(2)}) %collective-permute-start.2) | collective-permute-done | bytes 262176 | tf_op jit(solution)/shard_map/ppermute | solution.py:27
  119.9 1.9 %collective-permute-start.3 = (bf16[8,64,256]{2,1,0:T(8,128)(2,1)S(1)}, bf16[8,64,256]{2,1,0:T(8,128)(2,1)S(1)}, u32[]{:S(2)}, u32[]{:S(2)}) collective-permute-start(bf16[8,64,256]{2,1,0:T(8,128)(2,1)S(1)} %collective-permute-done.2.rest_2_), channel_id=1, source_target_pairs={{0,8},{8,16},{16,24},{24,32},{32,40},{40,48},{48,56},{56,0},{1,9},... | collective-permute-start | bytes 786440 | tf_op jit(solution)/shard_map/ppermute | solution.py:27
  121.8 0.0 collective-permute-done.6.rest_6_
  121.8 0.0 copy-start.10
  121.8 5.1 %collective-permute-start.7 = (bf16[8,64,256]{2,1,0:T(8,128)(2,1)S(1)}, bf16[8,64,256]{2,1,0:T(8,128)(2,1)S(1)}, u32[]{:S(2)}, u32[]{:S(2)}) collective-permute-start(bf16[8,64,256]{2,1,0:T(8,128)(2,1)S(1)} %collective-permute-done.6.rest_6_), channel_id=1, source_target_pairs={{0,56},{8,0},{16,8},{24,16},{32,24},{40,32},{48,40},{56,48},{1,57}... | collective-permute-start | bytes 786440 | tf_op jit(solution)/shard_map/ppermute | solution.py:27
  127.0 2.4 %collective-permute-done.3.rest_3_ = bf16[8,64,256]{2,1,0:T(8,128)(2,1)S(1)} collective-permute-done((bf16[8,64,256]{2,1,0:T(8,128)(2,1)S(1)}, bf16[8,64,256]{2,1,0:T(8,128)(2,1)S(1)}, u32[]{:S(2)}, u32[]{:S(2)}) %collective-permute-start.3) | collective-permute-done | bytes 262176 | tf_op jit(solution)/shard_map/ppermute | solution.py:27
  129.4 1.9 %collective-permute-start.4 = (bf16[8,64,256]{2,1,0:T(8,128)(2,1)S(1)}, bf16[8,64,256]{2,1,0:T(8,128)(2,1)}, u32[]{:S(2)}, u32[]{:S(2)}) collective-permute-start(bf16[8,64,256]{2,1,0:T(8,128)(2,1)S(1)} %collective-permute-done.3.rest_3_), channel_id=1, source_target_pairs={{0,8},{8,16},{16,24},{24,32},{32,40},{40,48},{48,56},{56,0},{1,9},... | collective-permute-start | bytes 786440 | tf_op jit(solution)/shard_map/ppermute | solution.py:27
  131.3 0.0 collective-permute-done.7.rest_5_
  131.3 0.7 copy-done.12
  132.0 6.9 %collective-permute-done.4.rest_4_ = bf16[8,64,256]{2,1,0:T(8,128)(2,1)} collective-permute-done((bf16[8,64,256]{2,1,0:T(8,128)(2,1)S(1)}, bf16[8,64,256]{2,1,0:T(8,128)(2,1)}, u32[]{:S(2)}, u32[]{:S(2)}) %collective-permute-start.4) | collective-permute-done | bytes 262176 | tf_op jit(solution)/shard_map/ppermute | solution.py:27
  138.9 0.0 all-to-all-done.3.mine
  139.0 1.9 %collective-permute-start.8 = (bf16[4,512,512]{2,1,0:T(8,128)(2,1)S(1)}, bf16[4,512,512]{2,1,0:T(8,128)(2,1)}, u32[]{:S(2)}, u32[]{:S(2)}) collective-permute-start(bf16[4,512,512]{2,1,0:T(8,128)(2,1)S(1)} %all-to-all-done.3.mine), channel_id=1, source_target_pairs={{0,1},{1,0},{2,3},{3,2},{4,5},{5,4},{6,7},{7,6},{8,9},{9,8},{10,11... | collective-permute-start | bytes 6291464 | tf_op jit(solution)/shard_map/ppermute | solution.py:27
  140.9 0.0 reduce-scatter.2.cloned.1.call-done
  140.9 1.0 slice.46
  141.9 0.7 convert_reduce_fusion.1
  142.6 0.7 pad_maximum_fusion.1
  143.4 6.5 %all-to-all-start.4 = ((bf16[8,72,256]{2,1,0:T(8,128)(2,1)}), bf16[8,72,256]{2,1,0:T(8,128)(2,1)S(1)}, u32[]{:S(2)}, u32[]{:S(2)}) async-start(bf16[8,72,256]{2,1,0:T(8,128)(2,1)} %pad_maximum_fusion.1), calls=%async_computation.5 | async-start | bytes 589824 | tf_op jit(solution)/shard_map/all_to_all | solution.py:17
  149.9 0.0 collective-permute-done.8.theirs
  149.9 4.9 %shard_map.95 = bf16[512,256]{1,0:T(8,128)(2,1)} custom-call(s32[2]{0:T(128)} %pad_add_fusion.place, bf16[4,512,512]{2,1,0:T(8,128)(2,1)} %copy-done, bf16[4,512,512]{2,1,0:T(8,128)(2,1)} %collective-permute-done.8.theirs, bf16[8,64,256]{2,1,0:T(8,128)(2,1)} %copy-done.4, bf16[8,64,256]{2,1,0:T(8,128)(2,1)} %copy-done.7, bf16[8,64,256]{2,1,0:T(8,128)(2,1)} %copy-done.9, ...), custom_call_target="tpu_custom_call" | custom-call | tf_op jit(solution)/shard_map/pallas_call | solution.py:97
  154.8 8.3 %all-to-all-done.4 = bf16[8,72,256]{2,1,0:T(8,128)(2,1)S(1)} async-done(((bf16[8,72,256]{2,1,0:T(8,128)(2,1)}), bf16[8,72,256]{2,1,0:T(8,128)(2,1)S(1)}, u32[]{:S(2)}, u32[]{:S(2)}) %all-to-all-start.4) | async-done | bytes 294944 | tf_op jit(solution)/shard_map/all_to_all | solution.py:17
  163.2 6.7 %collective-permute-start.9 = (f32[64,256]{1,0:T(8,128)S(1)}, f32[64,256]{1,0:T(8,128)S(1)}, u32[]{:S(2)}, u32[]{:S(2)}) collective-permute-start(f32[64,256]{1,0:T(8,128)S(1)} %slice.48), channel_id=1, source_target_pairs={{0,0},{1,64},{2,128},{3,192},{4,256},{5,320},{6,384},{7,448},{64,1... | collective-permute-start | bytes 196616 | tf_op jit(solution)/shard_map/ppermute | solution.py:166
  169.9 0.6 slice_reduce_fusion
  170.5 3.1 %collective-permute-done.9 = f32[64,256]{1,0:T(8,128)S(1)} collective-permute-done((f32[64,256]{1,0:T(8,128)S(1)}, f32[64,256]{1,0:T(8,128)S(1)}, u32[]{:S(2)}, u32[]{:S(2)}) %collective-permute-start.9) | collective-permute-done | bytes 65568 | tf_op jit(solution)/shard_map/ppermute | solution.py:166
  173.6 0.6 copy.15
  (34 shorter events, 0.2 us)
Async XLA Ops:
  7.2 39.9 %copy-start.3 = (bf16[512,256]{1,0:T(8,128)(2,1)S(1)}, bf16[512,256]{1,0:T(8,128)(2,1)}, u32[]{:S(2)}) copy-start(bf16[512,256]{1,0:T(8,128)(2,1)} %param.13) | copy-start | bytes 786436
  7.2 39.9 %copy-start.13 = (f32[256]{0:T(256)S(1)}, f32[256]{0:T(256)}, u32[]{:S(2)}) copy-start(f32[256]{0:T(256)} %param.10) | copy-start | bytes 3076
  7.2 39.9 %copy-start.2 = (bf16[512,256]{1,0:T(8,128)(2,1)S(1)}, bf16[512,256]{1,0:T(8,128)(2,1)}, u32[]{:S(2)}) copy-start(bf16[512,256]{1,0:T(8,128)(2,1)} %param.9) | copy-start | bytes 786436
  8.8 38.6 %copy-start.6 = (bf16[512,256]{1,0:T(8,128)(2,1)S(1)}, bf16[512,256]{1,0:T(8,128)(2,1)}, u32[]{:S(2)}) copy-start(bf16[512,256]{1,0:T(8,128)(2,1)} %param.7) | copy-start | bytes 786436
  9.6 27.8 %all-to-all-start = ((bf16[8,128,256]{2,1,0:T(8,128)(2,1)}), bf16[8,128,256]{2,1,0:T(8,128)(2,1)S(1)}, u32[]{:S(2)}, u32[]{:S(2)}) async-start(bf16[8,128,256]{2,1,0:T(8,128)(2,1)} %broadcast_in_dim.10), calls=%async_computation | async-start | bytes 1048576 | tf_op jit(solution)/shard_map/all_to_all | solution.py:17
  38.1 65.9 %copy-start.4 = (bf16[8,64,256]{2,1,0:T(8,128)(2,1)}, bf16[8,64,256]{2,1,0:T(8,128)(2,1)S(1)}, u32[]{:S(2)}) copy-start(bf16[8,64,256]{2,1,0:T(8,128)(2,1)S(1)} %get-tuple-element.10.rest_0_) | copy-start | bytes 786436
  38.8 8.2 %all-to-all-start.1 = ((f32[8,2,512]{2,1,0:T(2,128)}), f32[8,2,512]{2,1,0:T(2,128)S(1)}, u32[]{:S(2)}, u32[]{:S(2)}) async-start(f32[8,2,512]{2,1,0:T(2,128)} %broadcast_in_dim.11), calls=%async_computation.1 | async-start | bytes 65536 | tf_op jit(solution)/shard_map/all_to_all | solution.py:17
  43.6 43.1 %all-gather.2.cloned.1.call-start = ((), (), s32[]{:S(2)}) async-start(), calls=%async_computation.6 | async-start | bytes 2359296 | tf_op jit(solution)/shard_map/all_gather | solution.py:126
  44.3 96.6 %reduce-scatter.2.cloned.1.call-start = ((), (), s32[]{:S(2)}) async-start(), calls=%async_computation.7 | async-start | bytes 2469888 | tf_op jit(solution)/shard_map/reduce_scatter | solution.py:144
  76.6 10.1 %copy-start.1 = (bf16[4,2,512,256]{3,2,1,0:T(8,128)(2,1)}, bf16[4,2,512,256]{3,2,1,0:T(8,128)(2,1)S(1)}, u32[]{:S(2)}) copy-start(bf16[4,2,512,256]{3,2,1,0:T(8,128)(2,1)S(1)} %all_to_all.25.mine) | copy-start | bytes 6291460
  76.6 10.1 %collective-permute-start = (bf16[4,2,512,256]{3,2,1,0:T(8,128)(2,1)S(1)}, bf16[4,2,512,256]{3,2,1,0:T(8,128)(2,1)}, u32[]{:S(2)}, u32[]{:S(2)}) collective-permute-start(bf16[4,2,512,256]{3,2,1,0:T(8,128)(2,1)S(1)} %all_to_all.25.mine), channel_id=1, source_target_pairs={{0,1},{1,0},{2,3},{3,2},{4,5},{5,4},{6,7},{7,6},{8,9},{9,8},{10,11... | collective-permute-start | bytes 6291464 | tf_op jit(solution)/shard_map/ppermute | solution.py:27
  93.7 1.0 copy-start.5
  96.2 42.8 %all-to-all-start.3 = ((bf16[4,512,512]{2,1,0:T(8,128)(2,1)}), bf16[4,512,512]{2,1,0:T(8,128)(2,1)S(1)}, u32[]{:S(2)}, u32[]{:S(2)}) async-start(bf16[4,512,512]{2,1,0:T(8,128)(2,1)} %broadcast_in_dim.13), calls=%async_computation.3 | async-start | bytes 4194304 | tf_op jit(solution)/shard_map/all_to_all | solution.py:17
  101.0 9.5 %collective-permute-start.1 = (bf16[8,64,256]{2,1,0:T(8,128)(2,1)S(1)}, bf16[8,64,256]{2,1,0:T(8,128)(2,1)S(1)}, u32[]{:S(2)}, u32[]{:S(2)}) collective-permute-start(bf16[8,64,256]{2,1,0:T(8,128)(2,1)S(1)} %get-tuple-element.10.rest_0_), channel_id=1, source_target_pairs={{0,8},{8,16},{16,24},{24,32},{32,40},{40,48},{48,56},{56,0},{1,9},... | collective-permute-start | bytes 786440 | tf_op jit(solution)/shard_map/ppermute | solution.py:27
  104.1 8.3 %collective-permute-start.5 = (bf16[8,64,256]{2,1,0:T(8,128)(2,1)S(1)}, bf16[8,64,256]{2,1,0:T(8,128)(2,1)S(1)}, u32[]{:S(2)}, u32[]{:S(2)}) collective-permute-start(bf16[8,64,256]{2,1,0:T(8,128)(2,1)S(1)} %get-tuple-element.10.rest_0_), channel_id=1, source_target_pairs={{0,56},{8,0},{16,8},{24,16},{32,24},{40,32},{48,40},{56,48},{1,57}... | collective-permute-start | bytes 786440 | tf_op jit(solution)/shard_map/ppermute | solution.py:27
  110.4 39.5 %copy-start.7 = (bf16[8,64,256]{2,1,0:T(8,128)(2,1)}, bf16[8,64,256]{2,1,0:T(8,128)(2,1)S(1)}, u32[]{:S(2)}) copy-start(bf16[8,64,256]{2,1,0:T(8,128)(2,1)S(1)} %collective-permute-done.1.rest_1_) | copy-start | bytes 786436
  110.4 9.5 %collective-permute-start.2 = (bf16[8,64,256]{2,1,0:T(8,128)(2,1)S(1)}, bf16[8,64,256]{2,1,0:T(8,128)(2,1)S(1)}, u32[]{:S(2)}, u32[]{:S(2)}) collective-permute-start(bf16[8,64,256]{2,1,0:T(8,128)(2,1)S(1)} %collective-permute-done.1.rest_1_), channel_id=1, source_target_pairs={{0,8},{8,16},{16,24},{24,32},{32,40},{40,48},{48,56},{56,0},{1,9},... | collective-permute-start | bytes 786440 | tf_op jit(solution)/shard_map/ppermute | solution.py:27
  112.4 37.6 %copy-start.8 = (bf16[8,64,256]{2,1,0:T(8,128)(2,1)}, bf16[8,64,256]{2,1,0:T(8,128)(2,1)S(1)}, u32[]{:S(2)}) copy-start(bf16[8,64,256]{2,1,0:T(8,128)(2,1)S(1)} %collective-permute-done.5.rest_7_) | copy-start | bytes 786436
  112.4 9.4 %collective-permute-start.6 = (bf16[8,64,256]{2,1,0:T(8,128)(2,1)S(1)}, bf16[8,64,256]{2,1,0:T(8,128)(2,1)S(1)}, u32[]{:S(2)}, u32[]{:S(2)}) collective-permute-start(bf16[8,64,256]{2,1,0:T(8,128)(2,1)S(1)} %collective-permute-done.5.rest_7_), channel_id=1, source_target_pairs={{0,56},{8,0},{16,8},{24,16},{32,24},{40,32},{48,40},{56,48},{1,57}... | collective-permute-start | bytes 786440 | tf_op jit(solution)/shard_map/ppermute | solution.py:27
  119.9 30.0 %copy-start.9 = (bf16[8,64,256]{2,1,0:T(8,128)(2,1)}, bf16[8,64,256]{2,1,0:T(8,128)(2,1)S(1)}, u32[]{:S(2)}) copy-start(bf16[8,64,256]{2,1,0:T(8,128)(2,1)S(1)} %collective-permute-done.2.rest_2_) | copy-start | bytes 786436
  119.9 9.5 %collective-permute-start.3 = (bf16[8,64,256]{2,1,0:T(8,128)(2,1)S(1)}, bf16[8,64,256]{2,1,0:T(8,128)(2,1)S(1)}, u32[]{:S(2)}, u32[]{:S(2)}) collective-permute-start(bf16[8,64,256]{2,1,0:T(8,128)(2,1)S(1)} %collective-permute-done.2.rest_2_), channel_id=1, source_target_pairs={{0,8},{8,16},{16,24},{24,32},{32,40},{40,48},{48,56},{56,0},{1,9},... | collective-permute-start | bytes 786440 | tf_op jit(solution)/shard_map/ppermute | solution.py:27
  121.8 19.0 %copy-start.10 = (bf16[8,64,256]{2,1,0:T(8,128)(2,1)}, bf16[8,64,256]{2,1,0:T(8,128)(2,1)S(1)}, u32[]{:S(2)}) copy-start(bf16[8,64,256]{2,1,0:T(8,128)(2,1)S(1)} %collective-permute-done.6.rest_6_) | copy-start | bytes 786436
  121.8 9.5 %collective-permute-start.7 = (bf16[8,64,256]{2,1,0:T(8,128)(2,1)S(1)}, bf16[8,64,256]{2,1,0:T(8,128)(2,1)S(1)}, u32[]{:S(2)}, u32[]{:S(2)}) collective-permute-start(bf16[8,64,256]{2,1,0:T(8,128)(2,1)S(1)} %collective-permute-done.6.rest_6_), channel_id=1, source_target_pairs={{0,56},{8,0},{16,8},{24,16},{32,24},{40,32},{48,40},{56,48},{1,57}... | collective-permute-start | bytes 786440 | tf_op jit(solution)/shard_map/ppermute | solution.py:27
  129.4 14.0 %copy-start.11 = (bf16[8,64,256]{2,1,0:T(8,128)(2,1)}, bf16[8,64,256]{2,1,0:T(8,128)(2,1)S(1)}, u32[]{:S(2)}) copy-start(bf16[8,64,256]{2,1,0:T(8,128)(2,1)S(1)} %collective-permute-done.3.rest_3_) | copy-start | bytes 786436
  129.4 9.6 %collective-permute-start.4 = (bf16[8,64,256]{2,1,0:T(8,128)(2,1)S(1)}, bf16[8,64,256]{2,1,0:T(8,128)(2,1)}, u32[]{:S(2)}, u32[]{:S(2)}) collective-permute-start(bf16[8,64,256]{2,1,0:T(8,128)(2,1)S(1)} %collective-permute-done.3.rest_3_), channel_id=1, source_target_pairs={{0,8},{8,16},{16,24},{24,32},{32,40},{40,48},{48,56},{56,0},{1,9},... | collective-permute-start | bytes 786440 | tf_op jit(solution)/shard_map/ppermute | solution.py:27
  131.3 0.7 copy-start.12
  139.0 11.0 %copy-start = (bf16[4,512,512]{2,1,0:T(8,128)(2,1)}, bf16[4,512,512]{2,1,0:T(8,128)(2,1)S(1)}, u32[]{:S(2)}) copy-start(bf16[4,512,512]{2,1,0:T(8,128)(2,1)S(1)} %all-to-all-done.3.mine) | copy-start | bytes 6291460
  139.0 11.0 %collective-permute-start.8 = (bf16[4,512,512]{2,1,0:T(8,128)(2,1)S(1)}, bf16[4,512,512]{2,1,0:T(8,128)(2,1)}, u32[]{:S(2)}, u32[]{:S(2)}) collective-permute-start(bf16[4,512,512]{2,1,0:T(8,128)(2,1)S(1)} %all-to-all-done.3.mine), channel_id=1, source_target_pairs={{0,1},{1,0},{2,3},{3,2},{4,5},{5,4},{6,7},{7,6},{8,9},{9,8},{10,11... | collective-permute-start | bytes 6291464 | tf_op jit(solution)/shard_map/ppermute | solution.py:27
  143.4 19.8 %all-to-all-start.4 = ((bf16[8,72,256]{2,1,0:T(8,128)(2,1)}), bf16[8,72,256]{2,1,0:T(8,128)(2,1)S(1)}, u32[]{:S(2)}, u32[]{:S(2)}) async-start(bf16[8,72,256]{2,1,0:T(8,128)(2,1)} %pad_maximum_fusion.1), calls=%async_computation.5 | async-start | bytes 589824 | tf_op jit(solution)/shard_map/all_to_all | solution.py:17
  163.2 10.4 %collective-permute-start.9 = (f32[64,256]{1,0:T(8,128)S(1)}, f32[64,256]{1,0:T(8,128)S(1)}, u32[]{:S(2)}, u32[]{:S(2)}) collective-permute-start(f32[64,256]{1,0:T(8,128)S(1)} %slice.48), channel_id=1, source_target_pairs={{0,0},{1,64},{2,128},{3,192},{4,256},{5,320},{6,384},{7,448},{64,1... | collective-permute-start | bytes 196616 | tf_op jit(solution)/shard_map/ppermute | solution.py:166
Sparse Core Ops, SparseCore 0:
  47.1 39.6 all-gather.1
  93.8 45.0 reduce-scatter.1

commit v6 on v5

--- a/solution.py
+++ b/solution.py
@@ -145,25 +145,26 @@
 
     wu = after(wu, d_pre)
     pieces = [wu] * ny
-    for d in range(1, ny // 2 + 1):
+    for d in range(1, ny // 2):
         pieces[d] = shifted(pieces[d - 1], "y", 1)
-        if ny - d > d:
-            pieces[ny - d] = shifted(pieces[(ny - d + 1) % ny], "y", -1)
+        pieces[ny - d] = shifted(pieces[(ny - d + 1) % ny], "y", -1)
     mine = gather_directly(d_pre, "x")
     theirs = swapped(after(mine, pieces))
-    [grad_input] = run(
-        grad_input_kernel, [(toks, feats)], place, mine, theirs, *pieces,
-        scratch=[(nz, hid, feats)],
-    )
-
     rows = hid // ny
     gain = summed(g[hid:].reshape(nz, 3, feats))
     gain = in_three(jnp.sum(gain, axis=0)).astype(bf16)
     gain = jnp.broadcast_to(jnp.pad(gain, ((0, 5), (0, 0))), (ny, 8, feats))
     g = jnp.concatenate([g[:hid].reshape(ny, rows, feats), gain], axis=1)
+    last = after(pieces[ny // 2 - 1], g)
     g = summed(exchange(g, "y")) * scaled
     grad_gain = jnp.sum(g[rows : rows + 3], axis=0)
     grad_up = lax.ppermute(g[:rows], ("z", "x", "c"), swap).T
+
+    pieces[ny // 2] = shifted(last, "y", 1)
+    [grad_input] = run(
+        grad_input_kernel, [(toks, feats)], place, mine, theirs, *pieces,
+        scratch=[(nz, hid, feats)],
+    )
     return (grad_input, grad_up, grad_gain)
 
 

time: 184 us -> 186 us (1.011)
    all_to_all x4, waiting for transfers between devices: 27.2 us -> 18.8 us  [exchange(): return lax.all_to_all(chunks, axis, 0, 0, tiled=True)]
    ppermute x9, waiting for transfers between devices: 14.1 us -> 19.5 us  [shifted(): return lax.ppermute(value, axis, [(i, (i + by) % n) for i in range(n)])]
    reduce_scatter x1, waiting for transfers between devices: 0.02 us -> 3.52 us  [one_device(): lax.psum_scatter(g.reshape(-1, feats), 'z', scatter_dimension=0, tiled=True)]
  transfers between devices with their start and end apart: 16 -> 16, of which waited for: 9 -> 10; matrix products, arithmetic and copies ran while one was open for 4% -> 4% of each run, Pallas kernels for 3% -> 3%
where the time goes in v6:
time: 186 us; the launch traced here: 184 us
  starting transfers between devices  61.8 us (33%)
  waiting for transfers between devices  53.1 us (29%)
  blocking collectives  29 us (16%)
  between operations  14.3 us (8%)
  Pallas kernels  11.8 us (6%)
  local copies, waits for them, and re-layouts  8.2 us (4%)
  other arithmetic  5.85 us (3%)
    all_to_all x1, blocking collectives, exchange(): return lax.all_to_all(chunks, axis, 0, 0, tiled=True)  29 us
    ppermute x9, starting transfers between devices, shifted(): return lax.ppermute(value, axis, [(i, (i + by) % n) for i in range(n)])  28.2 us
    all_to_all x4, starting transfers between devices, exchange(): return lax.all_to_all(chunks, axis, 0, 0, tiled=True)  26.5 us
    ppermute x9, waiting for transfers between devices, shifted(): return lax.ppermute(value, axis, [(i, (i + by) % n) for i in range(n)])  19.5 us
    all_to_all x4, waiting for transfers between devices, exchange(): return lax.all_to_all(chunks, axis, 0, 0, tiled=True)  18.8 us
    pallas_call x2, Pallas kernels, run(): pl.pallas_call(kernel, out_shape=[jax.ShapeDtypeStruct(shape, bf16) for s...  11.8 us
    ppermute x1, starting transfers between devices, one_device(): grad_up = lax.ppermute(g[:rows], ('z', 'x', 'c'), swap).T  7.04 us
    all_gather x1, waiting for transfers between devices, one_device(): wd = lax.all_gather(wd, 'y', axis=0, tiled=True)  6.69 us
  transfers between devices with their start and end apart: 16, of which 10 were waited for; matrix products, arithmetic and copies ran while one was open for 4% of the time, Pallas kernels for 3%

profile of v6, /device:TPU:6, one launch (start us, length us, event | category | flops | bytes accessed | tf_op | source)
XLA Modules:
  0.0 184.0 jit_solution(6332495920646194468)
XLA Ops:
  7.2 0.0 copy-start.3
  7.2 0.0 copy-start.13
  7.2 0.0 copy-start.2
  7.2 0.8 fusion.20
  8.0 0.8 pad_maximum_fusion.2
  8.8 0.8 broadcast_in_dim.10
  9.6 10.3 %all-to-all-start = ((bf16[8,128,256]{2,1,0:T(8,128)(2,1)}), bf16[8,128,256]{2,1,0:T(8,128)(2,1)S(1)}, u32[]{:S(2)}, u32[]{:S(2)}) async-start(bf16[8,128,256]{2,1,0:T(8,128)(2,1)} %broadcast_in_dim.10), calls=%async_computation | async-start | bytes 1048576 | tf_op jit(solution)/shard_map/all_to_all | solution.py:17
  19.9 1.3 fusion.3
  21.2 16.2 %all-to-all-done = bf16[8,128,256]{2,1,0:T(8,128)(2,1)S(1)} async-done(((bf16[8,128,256]{2,1,0:T(8,128)(2,1)}), bf16[8,128,256]{2,1,0:T(8,128)(2,1)S(1)}, u32[]{:S(2)}, u32[]{:S(2)}) %all-to-all-start) | async-done | bytes 524320 | tf_op jit(solution)/shard_map/all_to_all | solution.py:17
  37.4 0.7 fusion.19
  38.2 0.7 broadcast_in_dim.11
  38.8 4.8 %all-to-all-start.1 = ((f32[8,2,512]{2,1,0:T(2,128)}), f32[8,2,512]{2,1,0:T(2,128)S(1)}, u32[]{:S(2)}, u32[]{:S(2)}) async-start(f32[8,2,512]{2,1,0:T(2,128)} %broadcast_in_dim.11), calls=%async_computation.1 | async-start | bytes 65536 | tf_op jit(solution)/shard_map/all_to_all | solution.py:17
  43.6 0.0 all-gather.2.cloned.1.call-start
  43.6 0.7 all-gather.2.cloned.1.call-update
  44.3 0.0 reduce-scatter.2.cloned.1.call-start
  44.4 2.6 %all-to-all-done.1 = f32[8,2,512]{2,1,0:T(2,128)S(1)} async-done(((f32[8,2,512]{2,1,0:T(2,128)}), f32[8,2,512]{2,1,0:T(2,128)S(1)}, u32[]{:S(2)}, u32[]{:S(2)}) %all-to-all-start.1) | async-done | bytes 32800 | tf_op jit(solution)/shard_map/all_to_all | solution.py:17
  47.1 0.3 fusion.9
  47.4 0.0 copy-done.6
  47.4 0.1 pad_maximum_fusion
  47.4 0.1 broadcast_in_dim.12
  47.6 29.0 %all_to_all.25.mine = bf16[4,2,512,256]{3,2,1,0:T(8,128)(2,1)S(1)} all-to-all(bf16[4,2,512,256]{3,2,1,0:T(8,128)(2,1)S(1)} %broadcast_in_dim.12), channel_id=1, replica_groups=mesh['z'=8,'y'=8,'x'=4,'c'=2] {'x'}, dimensions={0} | all-to-all | bytes 4194304 | tf_op jit(solution)/shard_map/all_to_all | solution.py:17
  76.6 1.9 %collective-permute-start = (bf16[4,2,512,256]{3,2,1,0:T(8,128)(2,1)S(1)}, bf16[4,2,512,256]{3,2,1,0:T(8,128)(2,1)}, u32[]{:S(2)}, u32[]{:S(2)}) collective-permute-start(bf16[4,2,512,256]{3,2,1,0:T(8,128)(2,1)S(1)} %all_to_all.25.mine), channel_id=1, source_target_pairs={{0,1},{1,0},{2,3},{3,2},{4,5},{5,4},{6,7},{7,6},{8,9},{9,8},{10,11... | collective-permute-start | bytes 6291464 | tf_op jit(solution)/shard_map/ppermute | solution.py:27
  78.5 0.1 mul.94
  78.6 0.1 mul.95
  78.7 0.6 pad_add_fusion.place
  79.3 0.7 multiply_convert_fusion.gain_rows
  80.0 6.7 %all-gather.2.cloned.1.call-done = bf16[4096,256]{1,0:T(8,128)(2,1)} async-done(((bf16[512,256]{1,0:T(8,128)(2,1)}), bf16[4096,256]{1,0:T(8,128)(2,1)}) %all-gather.2.cloned.1.call-update) | async-done | bytes 2097168 | tf_op jit(solution)/shard_map/all_gather | solution.py:126
  86.7 0.0 collective-permute-done.theirs
  86.7 0.0 copy-done.1
  86.7 7.0 %shard_map.94 = (bf16[512,512]{1,0:T(8,128)(2,1)}, bf16[8,536,256]{2,1,0:T(8,128)(2,1)}) custom-call(s32[2]{0:T(128)} %pad_add_fusion.place, bf16[4,2,512,256]{3,2,1,0:T(8,128)(2,1)} %copy-done.1, bf16[4,2,512,256]{3,2,1,0:T(8,128)(2,1)} %collective-permute-done.theirs, bf16[8,8,2,32,256]{4,3,2,1,0:T(8,128)(2,1)} %bitcast.19, bf16[512,512]{1,0:T(8,128)(2,1)} %hidden.1, ...), custom_call_target="tpu_custom_call" | custom-call | tf_op jit(solution)/shard_map/pallas_call | solution.py:97
  93.7 0.0 reduce-scatter.2.cloned.1.call-update
  93.7 1.0 copy-done.5
  94.7 1.5 broadcast_in_dim.13
  96.2 4.8 %all-to-all-start.3 = ((bf16[4,512,512]{2,1,0:T(8,128)(2,1)}), bf16[4,512,512]{2,1,0:T(8,128)(2,1)S(1)}, u32[]{:S(2)}, u32[]{:S(2)}) async-start(bf16[4,512,512]{2,1,0:T(8,128)(2,1)} %broadcast_in_dim.13), calls=%async_computation.3 | async-start | bytes 4194304 | tf_op jit(solution)/shard_map/all_to_all | solution.py:17
  101.0 3.9 %collective-permute-start.4 = (bf16[8,64,256]{2,1,0:T(8,128)(2,1)S(1)}, bf16[8,64,256]{2,1,0:T(8,128)(2,1)S(1)}, u32[]{:S(2)}, u32[]{:S(2)}) collective-permute-start(bf16[8,64,256]{2,1,0:T(8,128)(2,1)S(1)} %get-tuple-element.11.rest_0_), channel_id=1, source_target_pairs={{0,56},{8,0},{16,8},{24,16},{32,24},{40,32},{48,40},{56,48},{1,57}... | collective-permute-start | bytes 786440 | tf_op jit(solution)/shard_map/ppermute | solution.py:27
  104.9 2.0 %collective-permute-start.1 = (bf16[8,64,256]{2,1,0:T(8,128)(2,1)S(1)}, bf16[8,64,256]{2,1,0:T(8,128)(2,1)S(1)}, u32[]{:S(2)}, u32[]{:S(2)}) collective-permute-start(bf16[8,64,256]{2,1,0:T(8,128)(2,1)S(1)} %get-tuple-element.11.rest_0_), channel_id=1, source_target_pairs={{0,8},{8,16},{16,24},{24,32},{32,40},{40,48},{48,56},{56,0},{1,9},... | collective-permute-start | bytes 786440 | tf_op jit(solution)/shard_map/ppermute | solution.py:27
  106.8 2.4 %collective-permute-done.4.rest_7_ = bf16[8,64,256]{2,1,0:T(8,128)(2,1)S(1)} collective-permute-done((bf16[8,64,256]{2,1,0:T(8,128)(2,1)S(1)}, bf16[8,64,256]{2,1,0:T(8,128)(2,1)S(1)}, u32[]{:S(2)}, u32[]{:S(2)}) %collective-permute-start.4) | collective-permute-done | bytes 262176 | tf_op jit(solution)/shard_map/ppermute | solution.py:27
  109.2 5.2 %collective-permute-start.5 = (bf16[8,64,256]{2,1,0:T(8,128)(2,1)S(1)}, bf16[8,64,256]{2,1,0:T(8,128)(2,1)S(1)}, u32[]{:S(2)}, u32[]{:S(2)}) collective-permute-start(bf16[8,64,256]{2,1,0:T(8,128)(2,1)S(1)} %collective-permute-done.4.rest_7_), channel_id=1, source_target_pairs={{0,56},{8,0},{16,8},{24,16},{32,24},{40,32},{48,40},{56,48},{1,57}... | collective-permute-start | bytes 786440 | tf_op jit(solution)/shard_map/ppermute | solution.py:27
  114.4 0.0 collective-permute-done.1.rest_1_
  114.5 0.0 copy-start.8
  114.5 1.9 %collective-permute-start.2 = (bf16[8,64,256]{2,1,0:T(8,128)(2,1)S(1)}, bf16[8,64,256]{2,1,0:T(8,128)(2,1)S(1)}, u32[]{:S(2)}, u32[]{:S(2)}) collective-permute-start(bf16[8,64,256]{2,1,0:T(8,128)(2,1)S(1)} %collective-permute-done.1.rest_1_), channel_id=1, source_target_pairs={{0,8},{8,16},{16,24},{24,32},{32,40},{40,48},{48,56},{56,0},{1,9},... | collective-permute-start | bytes 786440 | tf_op jit(solution)/shard_map/ppermute | solution.py:27
  116.4 1.9 %collective-permute-done.5.rest_6_ = bf16[8,64,256]{2,1,0:T(8,128)(2,1)S(1)} collective-permute-done((bf16[8,64,256]{2,1,0:T(8,128)(2,1)S(1)}, bf16[8,64,256]{2,1,0:T(8,128)(2,1)S(1)}, u32[]{:S(2)}, u32[]{:S(2)}) %collective-permute-start.5) | collective-permute-done | bytes 262176 | tf_op jit(solution)/shard_map/ppermute | solution.py:27
  118.3 5.6 %collective-permute-start.6 = (bf16[8,64,256]{2,1,0:T(8,128)(2,1)S(1)}, bf16[8,64,256]{2,1,0:T(8,128)(2,1)S(1)}, u32[]{:S(2)}, u32[]{:S(2)}) collective-permute-start(bf16[8,64,256]{2,1,0:T(8,128)(2,1)S(1)} %collective-permute-done.5.rest_6_), channel_id=1, source_target_pairs={{0,56},{8,0},{16,8},{24,16},{32,24},{40,32},{48,40},{56,48},{1,57}... | collective-permute-start | bytes 786440 | tf_op jit(solution)/shard_map/ppermute | solution.py:27
  123.9 0.0 collective-permute-done.2.rest_2_
  123.9 1.9 %collective-permute-start.3 = (bf16[8,64,256]{2,1,0:T(8,128)(2,1)S(1)}, bf16[8,64,256]{2,1,0:T(8,128)(2,1)}, u32[]{:S(2)}, u32[]{:S(2)}) collective-permute-start(bf16[8,64,256]{2,1,0:T(8,128)(2,1)S(1)} %collective-permute-done.2.rest_2_), channel_id=1, source_target_pairs={{0,8},{8,16},{16,24},{24,32},{32,40},{40,48},{48,56},{56,0},{1,9},... | collective-permute-start | bytes 786440 | tf_op jit(solution)/shard_map/ppermute | solution.py:27
  125.9 1.9 %collective-permute-done.6.rest_5_ = bf16[8,64,256]{2,1,0:T(8,128)(2,1)S(1)} collective-permute-done((bf16[8,64,256]{2,1,0:T(8,128)(2,1)S(1)}, bf16[8,64,256]{2,1,0:T(8,128)(2,1)S(1)}, u32[]{:S(2)}, u32[]{:S(2)}) %collective-permute-start.6) | collective-permute-done | bytes 262176 | tf_op jit(solution)/shard_map/ppermute | solution.py:27
  127.8 5.7 %collective-permute-done.3.rest_3_ = bf16[8,64,256]{2,1,0:T(8,128)(2,1)} collective-permute-done((bf16[8,64,256]{2,1,0:T(8,128)(2,1)S(1)}, bf16[8,64,256]{2,1,0:T(8,128)(2,1)}, u32[]{:S(2)}, u32[]{:S(2)}) %collective-permute-start.3) | collective-permute-done | bytes 262176 | tf_op jit(solution)/shard_map/ppermute | solution.py:27
  133.5 0.0 all-to-all-done.3.mine
  133.5 1.9 %collective-permute-start.7 = (bf16[4,512,512]{2,1,0:T(8,128)(2,1)S(1)}, bf16[4,512,512]{2,1,0:T(8,128)(2,1)}, u32[]{:S(2)}, u32[]{:S(2)}) collective-permute-start(bf16[4,512,512]{2,1,0:T(8,128)(2,1)S(1)} %all-to-all-done.3.mine), channel_id=1, source_target_pairs={{0,1},{1,0},{2,3},{3,2},{4,5},{5,4},{6,7},{7,6},{8,9},{9,8},{10,11... | collective-permute-start | bytes 6291464 | tf_op jit(solution)/shard_map/ppermute | solution.py:27
  135.4 3.5 %reduce-scatter.2.cloned.1.call-done = bf16[536,256]{1,0:T(8,128)(2,1)} async-done(((bf16[4288,256]{1,0:T(8,128)(2,1)}), bf16[536,256]{1,0:T(8,128)(2,1)}) %reduce-scatter.2.cloned.1.call-update) | async-done | bytes 274448 | tf_op jit(solution)/shard_map/reduce_scatter | solution.py:144
  139.0 1.0 slice.46
  139.9 0.7 convert_reduce_fusion.1
  140.7 0.7 pad_maximum_fusion.1
  141.4 6.6 %all-to-all-start.4 = ((bf16[8,72,256]{2,1,0:T(8,128)(2,1)}), bf16[8,72,256]{2,1,0:T(8,128)(2,1)S(1)}, u32[]{:S(2)}, u32[]{:S(2)}) async-start(bf16[8,72,256]{2,1,0:T(8,128)(2,1)} %pad_maximum_fusion.1), calls=%async_computation.5 | async-start | bytes 589824 | tf_op jit(solution)/shard_map/all_to_all | solution.py:17
  148.1 3.9 %collective-permute-start.8 = (bf16[8,64,256]{2,1,0:T(8,128)(2,1)}, bf16[8,64,256]{2,1,0:T(8,128)(2,1)S(1)}, u32[]{:S(2)}, u32[]{:S(2)}) collective-permute-start(bf16[8,64,256]{2,1,0:T(8,128)(2,1)} %collective-permute-done.3.rest_3_), channel_id=1, source_target_pairs={{0,8},{8,16},{16,24},{24,32},{32,40},{40,48},{48,56},{56,0},{1,9},... | collective-permute-start | bytes 786440 | tf_op jit(solution)/shard_map/ppermute | solution.py:27
  152.0 0.0 collective-permute-done.7.theirs
  152.0 7.5 %collective-permute-done.8.rest_4_ = bf16[8,64,256]{2,1,0:T(8,128)(2,1)S(1)} collective-permute-done((bf16[8,64,256]{2,1,0:T(8,128)(2,1)}, bf16[8,64,256]{2,1,0:T(8,128)(2,1)S(1)}, u32[]{:S(2)}, u32[]{:S(2)}) %collective-permute-start.8) | collective-permute-done | bytes 262176 | tf_op jit(solution)/shard_map/ppermute | solution.py:27
  159.6 0.7 copy-done.12
  160.2 4.9 %shard_map.95 = bf16[512,256]{1,0:T(8,128)(2,1)} custom-call(s32[2]{0:T(128)} %pad_add_fusion.place, bf16[4,512,512]{2,1,0:T(8,128)(2,1)} %copy-done, bf16[4,512,512]{2,1,0:T(8,128)(2,1)} %collective-permute-done.7.theirs, bf16[8,64,256]{2,1,0:T(8,128)(2,1)} %copy-done.4, bf16[8,64,256]{2,1,0:T(8,128)(2,1)} %copy-done.8, bf16[8,64,256]{2,1,0:T(8,128)(2,1)} %copy-done.10, ...), custom_call_target="tpu_custom_call" | custom-call | tf_op jit(solution)/shard_map/pallas_call | solution.py:97
  165.1 0.0 all-to-all-done.4
  165.2 7.0 %collective-permute-start.9 = (f32[64,256]{1,0:T(8,128)S(1)}, f32[64,256]{1,0:T(8,128)S(1)}, u32[]{:S(2)}, u32[]{:S(2)}) collective-permute-start(f32[64,256]{1,0:T(8,128)S(1)} %slice.48), channel_id=1, source_target_pairs={{0,0},{1,64},{2,128},{3,192},{4,256},{5,320},{6,384},{7,448},{64,1... | collective-permute-start | bytes 196616 | tf_op jit(solution)/shard_map/ppermute | solution.py:161
  172.2 0.6 slice_reduce_fusion
  172.8 3.8 %collective-permute-done.9 = f32[64,256]{1,0:T(8,128)S(1)} collective-permute-done((f32[64,256]{1,0:T(8,128)S(1)}, f32[64,256]{1,0:T(8,128)S(1)}, u32[]{:S(2)}, u32[]{:S(2)}) %collective-permute-start.9) | collective-permute-done | bytes 65568 | tf_op jit(solution)/shard_map/ppermute | solution.py:161
  176.6 0.6 copy.15
  (34 shorter events, 0.2 us)
Async XLA Ops:
  7.2 39.9 %copy-start.3 = (bf16[512,256]{1,0:T(8,128)(2,1)S(1)}, bf16[512,256]{1,0:T(8,128)(2,1)}, u32[]{:S(2)}) copy-start(bf16[512,256]{1,0:T(8,128)(2,1)} %param.13) | copy-start | bytes 786436
  7.2 39.9 %copy-start.13 = (f32[256]{0:T(256)S(1)}, f32[256]{0:T(256)}, u32[]{:S(2)}) copy-start(f32[256]{0:T(256)} %param.10) | copy-start | bytes 3076
  7.2 39.9 %copy-start.2 = (bf16[512,256]{1,0:T(8,128)(2,1)S(1)}, bf16[512,256]{1,0:T(8,128)(2,1)}, u32[]{:S(2)}) copy-start(bf16[512,256]{1,0:T(8,128)(2,1)} %param.9) | copy-start | bytes 786436
  8.8 38.6 %copy-start.6 = (bf16[512,256]{1,0:T(8,128)(2,1)S(1)}, bf16[512,256]{1,0:T(8,128)(2,1)}, u32[]{:S(2)}) copy-start(bf16[512,256]{1,0:T(8,128)(2,1)} %param.7) | copy-start | bytes 786436
  9.6 27.8 %all-to-all-start = ((bf16[8,128,256]{2,1,0:T(8,128)(2,1)}), bf16[8,128,256]{2,1,0:T(8,128)(2,1)S(1)}, u32[]{:S(2)}, u32[]{:S(2)}) async-start(bf16[8,128,256]{2,1,0:T(8,128)(2,1)} %broadcast_in_dim.10), calls=%async_computation | async-start | bytes 1048576 | tf_op jit(solution)/shard_map/all_to_all | solution.py:17
  38.1 66.7 %copy-start.4 = (bf16[8,64,256]{2,1,0:T(8,128)(2,1)}, bf16[8,64,256]{2,1,0:T(8,128)(2,1)S(1)}, u32[]{:S(2)}) copy-start(bf16[8,64,256]{2,1,0:T(8,128)(2,1)S(1)} %get-tuple-element.11.rest_0_) | copy-start | bytes 786436
  38.8 8.2 %all-to-all-start.1 = ((f32[8,2,512]{2,1,0:T(2,128)}), f32[8,2,512]{2,1,0:T(2,128)S(1)}, u32[]{:S(2)}, u32[]{:S(2)}) async-start(f32[8,2,512]{2,1,0:T(2,128)} %broadcast_in_dim.11), calls=%async_computation.1 | async-start | bytes 65536 | tf_op jit(solution)/shard_map/all_to_all | solution.py:17
  43.6 43.1 %all-gather.2.cloned.1.call-start = ((), (), s32[]{:S(2)}) async-start(), calls=%async_computation.6 | async-start | bytes 2359296 | tf_op jit(solution)/shard_map/all_gather | solution.py:126
  44.3 94.6 %reduce-scatter.2.cloned.1.call-start = ((), (), s32[]{:S(2)}) async-start(), calls=%async_computation.7 | async-start | bytes 2469888 | tf_op jit(solution)/shard_map/reduce_scatter | solution.py:144
  76.6 10.1 %copy-start.1 = (bf16[4,2,512,256]{3,2,1,0:T(8,128)(2,1)}, bf16[4,2,512,256]{3,2,1,0:T(8,128)(2,1)S(1)}, u32[]{:S(2)}) copy-start(bf16[4,2,512,256]{3,2,1,0:T(8,128)(2,1)S(1)} %all_to_all.25.mine) | copy-start | bytes 6291460
  76.6 10.1 %collective-permute-start = (bf16[4,2,512,256]{3,2,1,0:T(8,128)(2,1)S(1)}, bf16[4,2,512,256]{3,2,1,0:T(8,128)(2,1)}, u32[]{:S(2)}, u32[]{:S(2)}) collective-permute-start(bf16[4,2,512,256]{3,2,1,0:T(8,128)(2,1)S(1)} %all_to_all.25.mine), channel_id=1, source_target_pairs={{0,1},{1,0},{2,3},{3,2},{4,5},{5,4},{6,7},{7,6},{8,9},{9,8},{10,11... | collective-permute-start | bytes 6291464 | tf_op jit(solution)/shard_map/ppermute | solution.py:27
  93.7 1.0 copy-start.5
  96.2 37.3 %all-to-all-start.3 = ((bf16[4,512,512]{2,1,0:T(8,128)(2,1)}), bf16[4,512,512]{2,1,0:T(8,128)(2,1)S(1)}, u32[]{:S(2)}, u32[]{:S(2)}) async-start(bf16[4,512,512]{2,1,0:T(8,128)(2,1)} %broadcast_in_dim.13), calls=%async_computation.3 | async-start | bytes 4194304 | tf_op jit(solution)/shard_map/all_to_all | solution.py:17
  101.0 8.3 %collective-permute-start.4 = (bf16[8,64,256]{2,1,0:T(8,128)(2,1)S(1)}, bf16[8,64,256]{2,1,0:T(8,128)(2,1)S(1)}, u32[]{:S(2)}, u32[]{:S(2)}) collective-permute-start(bf16[8,64,256]{2,1,0:T(8,128)(2,1)S(1)} %get-tuple-element.11.rest_0_), channel_id=1, source_target_pairs={{0,56},{8,0},{16,8},{24,16},{32,24},{40,32},{48,40},{56,48},{1,57}... | collective-permute-start | bytes 786440 | tf_op jit(solution)/shard_map/ppermute | solution.py:27
  104.9 9.6 %collective-permute-start.1 = (bf16[8,64,256]{2,1,0:T(8,128)(2,1)S(1)}, bf16[8,64,256]{2,1,0:T(8,128)(2,1)S(1)}, u32[]{:S(2)}, u32[]{:S(2)}) collective-permute-start(bf16[8,64,256]{2,1,0:T(8,128)(2,1)S(1)} %get-tuple-element.11.rest_0_), channel_id=1, source_target_pairs={{0,8},{8,16},{16,24},{24,32},{32,40},{40,48},{48,56},{56,0},{1,9},... | collective-permute-start | bytes 786440 | tf_op jit(solution)/shard_map/ppermute | solution.py:27
  109.2 50.3 %copy-start.7 = (bf16[8,64,256]{2,1,0:T(8,128)(2,1)}, bf16[8,64,256]{2,1,0:T(8,128)(2,1)S(1)}, u32[]{:S(2)}) copy-start(bf16[8,64,256]{2,1,0:T(8,128)(2,1)S(1)} %collective-permute-done.4.rest_7_) | copy-start | bytes 786436
  109.2 9.1 %collective-permute-start.5 = (bf16[8,64,256]{2,1,0:T(8,128)(2,1)S(1)}, bf16[8,64,256]{2,1,0:T(8,128)(2,1)S(1)}, u32[]{:S(2)}, u32[]{:S(2)}) collective-permute-start(bf16[8,64,256]{2,1,0:T(8,128)(2,1)S(1)} %collective-permute-done.4.rest_7_), channel_id=1, source_target_pairs={{0,56},{8,0},{16,8},{24,16},{32,24},{40,32},{48,40},{56,48},{1,57}... | collective-permute-start | bytes 786440 | tf_op jit(solution)/shard_map/ppermute | solution.py:27
  114.5 45.1 %copy-start.8 = (bf16[8,64,256]{2,1,0:T(8,128)(2,1)}, bf16[8,64,256]{2,1,0:T(8,128)(2,1)S(1)}, u32[]{:S(2)}) copy-start(bf16[8,64,256]{2,1,0:T(8,128)(2,1)S(1)} %collective-permute-done.1.rest_1_) | copy-start | bytes 786436
  114.5 9.5 %collective-permute-start.2 = (bf16[8,64,256]{2,1,0:T(8,128)(2,1)S(1)}, bf16[8,64,256]{2,1,0:T(8,128)(2,1)S(1)}, u32[]{:S(2)}, u32[]{:S(2)}) collective-permute-start(bf16[8,64,256]{2,1,0:T(8,128)(2,1)S(1)} %collective-permute-done.1.rest_1_), channel_id=1, source_target_pairs={{0,8},{8,16},{16,24},{24,32},{32,40},{40,48},{48,56},{56,0},{1,9},... | collective-permute-start | bytes 786440 | tf_op jit(solution)/shard_map/ppermute | solution.py:27
  118.3 41.2 %copy-start.9 = (bf16[8,64,256]{2,1,0:T(8,128)(2,1)}, bf16[8,64,256]{2,1,0:T(8,128)(2,1)S(1)}, u32[]{:S(2)}) copy-start(bf16[8,64,256]{2,1,0:T(8,128)(2,1)S(1)} %collective-permute-done.5.rest_6_) | copy-start | bytes 786436
  118.3 9.5 %collective-permute-start.6 = (bf16[8,64,256]{2,1,0:T(8,128)(2,1)S(1)}, bf16[8,64,256]{2,1,0:T(8,128)(2,1)S(1)}, u32[]{:S(2)}, u32[]{:S(2)}) collective-permute-start(bf16[8,64,256]{2,1,0:T(8,128)(2,1)S(1)} %collective-permute-done.5.rest_6_), channel_id=1, source_target_pairs={{0,56},{8,0},{16,8},{24,16},{32,24},{40,32},{48,40},{56,48},{1,57}... | collective-permute-start | bytes 786440 | tf_op jit(solution)/shard_map/ppermute | solution.py:27
  123.9 11.5 %copy-start.10 = (bf16[8,64,256]{2,1,0:T(8,128)(2,1)}, bf16[8,64,256]{2,1,0:T(8,128)(2,1)S(1)}, u32[]{:S(2)}) copy-start(bf16[8,64,256]{2,1,0:T(8,128)(2,1)S(1)} %collective-permute-done.2.rest_2_) | copy-start | bytes 786436
  123.9 9.6 %collective-permute-start.3 = (bf16[8,64,256]{2,1,0:T(8,128)(2,1)S(1)}, bf16[8,64,256]{2,1,0:T(8,128)(2,1)}, u32[]{:S(2)}, u32[]{:S(2)}) collective-permute-start(bf16[8,64,256]{2,1,0:T(8,128)(2,1)S(1)} %collective-permute-done.2.rest_2_), channel_id=1, source_target_pairs={{0,8},{8,16},{16,24},{24,32},{32,40},{40,48},{48,56},{56,0},{1,9},... | collective-permute-start | bytes 786440 | tf_op jit(solution)/shard_map/ppermute | solution.py:27
  127.8 13.7 %copy-start.11 = (bf16[8,64,256]{2,1,0:T(8,128)(2,1)}, bf16[8,64,256]{2,1,0:T(8,128)(2,1)S(1)}, u32[]{:S(2)}) copy-start(bf16[8,64,256]{2,1,0:T(8,128)(2,1)S(1)} %collective-permute-done.6.rest_5_) | copy-start | bytes 786436
  133.5 26.0 %copy-start = (bf16[4,512,512]{2,1,0:T(8,128)(2,1)}, bf16[4,512,512]{2,1,0:T(8,128)(2,1)S(1)}, u32[]{:S(2)}) copy-start(bf16[4,512,512]{2,1,0:T(8,128)(2,1)S(1)} %all-to-all-done.3.mine) | copy-start | bytes 6291460
  133.5 18.5 %collective-permute-start.7 = (bf16[4,512,512]{2,1,0:T(8,128)(2,1)S(1)}, bf16[4,512,512]{2,1,0:T(8,128)(2,1)}, u32[]{:S(2)}, u32[]{:S(2)}) collective-permute-start(bf16[4,512,512]{2,1,0:T(8,128)(2,1)S(1)} %all-to-all-done.3.mine), channel_id=1, source_target_pairs={{0,1},{1,0},{2,3},{3,2},{4,5},{5,4},{6,7},{7,6},{8,9},{9,8},{10,11... | collective-permute-start | bytes 6291464 | tf_op jit(solution)/shard_map/ppermute | solution.py:27
  141.4 23.7 %all-to-all-start.4 = ((bf16[8,72,256]{2,1,0:T(8,128)(2,1)}), bf16[8,72,256]{2,1,0:T(8,128)(2,1)S(1)}, u32[]{:S(2)}, u32[]{:S(2)}) async-start(bf16[8,72,256]{2,1,0:T(8,128)(2,1)} %pad_maximum_fusion.1), calls=%async_computation.5 | async-start | bytes 589824 | tf_op jit(solution)/shard_map/all_to_all | solution.py:17
  148.1 11.5 %collective-permute-start.8 = (bf16[8,64,256]{2,1,0:T(8,128)(2,1)}, bf16[8,64,256]{2,1,0:T(8,128)(2,1)S(1)}, u32[]{:S(2)}, u32[]{:S(2)}) collective-permute-start(bf16[8,64,256]{2,1,0:T(8,128)(2,1)} %collective-permute-done.3.rest_3_), channel_id=1, source_target_pairs={{0,8},{8,16},{16,24},{24,32},{32,40},{40,48},{48,56},{56,0},{1,9},... | collective-permute-start | bytes 786440 | tf_op jit(solution)/shard_map/ppermute | solution.py:27
  159.6 0.7 copy-start.12
  165.2 11.4 %collective-permute-start.9 = (f32[64,256]{1,0:T(8,128)S(1)}, f32[64,256]{1,0:T(8,128)S(1)}, u32[]{:S(2)}, u32[]{:S(2)}) collective-permute-start(f32[64,256]{1,0:T(8,128)S(1)} %slice.48), channel_id=1, source_target_pairs={{0,0},{1,64},{2,128},{3,192},{4,256},{5,320},{6,384},{7,448},{64,1... | collective-permute-start | bytes 196616 | tf_op jit(solution)/shard_map/ppermute | solution.py:161
Sparse Core Ops, SparseCore 0:
  47.1 39.6 all-gather.1
  93.8 45.0 reduce-scatter.1

commit v7 on v5

--- a/solution.py
+++ b/solution.py
@@ -29,11 +29,6 @@
 
 def swapped(value):
     return shifted(value, "c", 1)
-
-
-def gather_two_steps(value):
-    mine = gather_directly(value, "x")
-    return mine, swapped(mine)
 
 
 def after(value, earlier):
@@ -134,7 +129,11 @@
     d_out = (weighted * inv_rms - normed * inv_rms * inv_rms * inv_rms * cross_mean).astype(bf16)
     gain_part = jnp.sum(upstream * normed * inv_rms, axis=0)
 
-    mine, theirs = gather_two_steps(jnp.stack([d_out, inputs]))
+    wu = after(wu, inv_rms)
+    pieces = [wu] * ny
+    pieces[1], pieces[ny - 1] = shifted(wu, "y", 1), shifted(wu, "y", -1)
+    mine = gather_directly(jnp.stack([d_out, inputs]), "x")
+    theirs = swapped(after(mine, (pieces[1], pieces[ny - 1])))
     turn = (jnp.arange(nz) == lax.axis_index("z")).astype(f32)[:, None, None]
     gain_rows = (turn * in_three(gain_part)).reshape(3 * nz, feats).astype(bf16)
     d_pre, g = run(
@@ -143,9 +142,9 @@
     )
     g = lax.psum_scatter(g.reshape(-1, feats), "z", scatter_dimension=0, tiled=True)
 
-    wu = after(wu, d_pre)
-    pieces = [wu] * ny
-    for d in range(1, ny // 2 + 1):
+    pieces[1] = after(pieces[1], d_pre)
+    pieces[ny - 1] = after(pieces[ny - 1], d_pre)
+    for d in range(2, ny // 2 + 1):
         pieces[d] = shifted(pieces[d - 1], "y", 1)
         if ny - d > d:
             pieces[ny - d] = shifted(pieces[(ny - d + 1) % ny], "y", -1)

time: 184 us -> 190 us (1.033)
  waiting for transfers between devices: 51.8 us -> 81.1 us
  blocking collectives: 29 us -> 7.95 us
  starting transfers between devices: 60 us -> 58 us
    all_to_all x1, blocking collectives: 29 us -> 7.95 us  [exchange(): return lax.all_to_all(chunks, axis, 0, 0, tiled=True)]
    all_gather x1, waiting for transfers between devices: 6.69 us -> 15.2 us  [one_device(): wd = lax.all_gather(wd, 'y', axis=0, tiled=True)]
    ppermute x9, waiting for transfers between devices: 14.1 us -> 22.1 us  [shifted(): return lax.ppermute(value, axis, [(i, (i + by) % n) for i in range(n)])]
    reduce_scatter x1, waiting for transfers between devices: 0.02 us -> 6.46 us  [one_device(): lax.psum_scatter(g.reshape(-1, feats), 'z', scatter_dimension=0, tiled=True)]
    ppermute x1, starting transfers between devices: 6.69 us -> 2.99 us  [one_device(): grad_up = lax.ppermute(g[:rows], ('z', 'x', 'c'), swap).T]
    ppermute x1, waiting for transfers between devices: 3.11 us -> 6.8 us  [one_device(): grad_up = lax.ppermute(g[:rows], ('z', 'x', 'c'), swap).T]
    all_to_all x4, waiting for transfers between devices: 27.2 us -> 29.9 us  [exchange(): return lax.all_to_all(chunks, axis, 0, 0, tiled=True)]
  transfers between devices with their start and end apart: 16 -> 16, of which waited for: 9 -> 12; matrix products, arithmetic and copies ran while one was open for 4% -> 4% of each run, Pallas kernels for 3% -> 3%
where the time goes in v7:
time: 190 us; the launch traced here: 187 us
  waiting for transfers between devices  81.1 us (43%)
  starting transfers between devices  58 us (31%)
  between operations  14.3 us (8%)
  Pallas kernels  11.8 us (6%)
  local copies, waits for them, and re-layouts  8.17 us (4%)
  blocking collectives  7.95 us (4%)
  other arithmetic  5.89 us (3%)
    all_to_all x4, waiting for transfers between devices, exchange(): return lax.all_to_all(chunks, axis, 0, 0, tiled=True)  29.9 us
    all_to_all x4, starting transfers between devices, exchange(): return lax.all_to_all(chunks, axis, 0, 0, tiled=True)  27.8 us
    ppermute x9, starting transfers between devices, shifted(): return lax.ppermute(value, axis, [(i, (i + by) % n) for i in range(n)])  27.1 us
    ppermute x9, waiting for transfers between devices, shifted(): return lax.ppermute(value, axis, [(i, (i + by) % n) for i in range(n)])  22.1 us
    all_gather x1, waiting for transfers between devices, one_device(): wd = lax.all_gather(wd, 'y', axis=0, tiled=True)  15.2 us
    pallas_call x2, Pallas kernels, run(): pl.pallas_call(kernel, out_shape=[jax.ShapeDtypeStruct(shape, bf16) for s...  11.8 us
    all_to_all x1, blocking collectives, exchange(): return lax.all_to_all(chunks, axis, 0, 0, tiled=True)  7.95 us
    ppermute x1, waiting for transfers between devices, one_device(): grad_up = lax.ppermute(g[:rows], ('z', 'x', 'c'), swap).T  6.8 us
  transfers between devices with their start and end apart: 16, of which 12 were waited for; matrix products, arithmetic and copies ran while one was open for 4% of the time, Pallas kernels for 3%

profile of v7, /device:TPU:6, one launch (start us, length us, event | category | flops | bytes accessed | tf_op | source)
XLA Modules:
  0.0 187.3 jit_solution(3460280829383485485)
XLA Ops:
  7.2 0.0 copy-start.3
  7.2 0.0 copy-start.14
  7.2 0.0 copy-start.2
  7.2 0.8 fusion.20
  8.0 0.8 pad_maximum_fusion.2
  8.8 0.8 broadcast_in_dim.10
  9.6 10.3 %all-to-all-start = ((bf16[8,128,256]{2,1,0:T(8,128)(2,1)}), bf16[8,128,256]{2,1,0:T(8,128)(2,1)S(1)}, u32[]{:S(2)}, u32[]{:S(2)}) async-start(bf16[8,128,256]{2,1,0:T(8,128)(2,1)} %broadcast_in_dim.10), calls=%async_computation | async-start | bytes 1048576 | tf_op jit(solution)/shard_map/all_to_all | solution.py:17
  19.9 1.3 fusion.3
  21.2 16.2 %all-to-all-done = bf16[8,128,256]{2,1,0:T(8,128)(2,1)S(1)} async-done(((bf16[8,128,256]{2,1,0:T(8,128)(2,1)}), bf16[8,128,256]{2,1,0:T(8,128)(2,1)S(1)}, u32[]{:S(2)}, u32[]{:S(2)}) %all-to-all-start) | async-done | bytes 524320 | tf_op jit(solution)/shard_map/all_to_all | solution.py:17
  37.4 0.7 fusion.19
  38.2 8.0 %all_to_all.25 = f32[8,2,512]{2,1,0:T(2,128)S(1)} all-to-all(f32[8,2,512]{2,1,0:T(2,128)S(1)} %broadcast_in_dim.11), channel_id=1, replica_groups=mesh['z'=8,'y'=8,'x'=4,'c'=2] {'x','c'}, dimensions={0} | all-to-all | bytes 65536 | tf_op jit(solution)/shard_map/all_to_all | solution.py:17
  46.2 0.3 fusion.9
  46.5 0.0 copy-done.6
  46.5 0.1 pad_maximum_fusion
  46.6 1.5 broadcast_in_dim.12
  48.0 5.6 %all-to-all-start.2 = ((bf16[4,2,512,256]{3,2,1,0:T(8,128)(2,1)}), bf16[4,2,512,256]{3,2,1,0:T(8,128)(2,1)S(1)}, u32[]{:S(2)}, u32[]{:S(2)}) async-start(bf16[4,2,512,256]{3,2,1,0:T(8,128)(2,1)} %broadcast_in_dim.12), calls=%async_computation.2 | async-start | bytes 4194304 | tf_op jit(solution)/shard_map/all_to_all | solution.py:17
  53.7 0.7 all-gather.2.cloned.1.call-update
  54.4 0.0 reduce-scatter.2.cloned.1.call-start
  54.4 5.4 %collective-permute-start.1 = (bf16[8,64,256]{2,1,0:T(8,128)(2,1)S(1)}, bf16[8,64,256]{2,1,0:T(8,128)(2,1)S(1)}, u32[]{:S(2)}, u32[]{:S(2)}) collective-permute-start(bf16[8,64,256]{2,1,0:T(8,128)(2,1)S(1)} %get-tuple-element.21.rest_0_), channel_id=1, source_target_pairs={{0,56},{8,0},{16,8},{24,16},{32,24},{40,32},{48,40},{56,48},{1,57}... | collective-permute-start | bytes 786440 | tf_op jit(solution)/shard_map/ppermute | solution.py:27
  59.8 1.9 %collective-permute-start = (bf16[8,64,256]{2,1,0:T(8,128)(2,1)S(1)}, bf16[8,64,256]{2,1,0:T(8,128)(2,1)S(1)}, u32[]{:S(2)}, u32[]{:S(2)}) collective-permute-start(bf16[8,64,256]{2,1,0:T(8,128)(2,1)S(1)} %get-tuple-element.21.rest_0_), channel_id=1, source_target_pairs={{0,8},{8,16},{16,24},{24,32},{32,40},{40,48},{48,56},{56,0},{1,9},... | collective-permute-start | bytes 786440 | tf_op jit(solution)/shard_map/ppermute | solution.py:27
  61.8 3.3 %collective-permute-done.1.rest_7_ = bf16[8,64,256]{2,1,0:T(8,128)(2,1)S(1)} collective-permute-done((bf16[8,64,256]{2,1,0:T(8,128)(2,1)S(1)}, bf16[8,64,256]{2,1,0:T(8,128)(2,1)S(1)}, u32[]{:S(2)}, u32[]{:S(2)}) %collective-permute-start.1) | collective-permute-done | bytes 262176 | tf_op jit(solution)/shard_map/ppermute | solution.py:27
  65.0 5.3 %collective-permute-done.rest_1_ = bf16[8,64,256]{2,1,0:T(8,128)(2,1)S(1)} collective-permute-done((bf16[8,64,256]{2,1,0:T(8,128)(2,1)S(1)}, bf16[8,64,256]{2,1,0:T(8,128)(2,1)S(1)}, u32[]{:S(2)}, u32[]{:S(2)}) %collective-permute-start) | collective-permute-done | bytes 262176 | tf_op jit(solution)/shard_map/ppermute | solution.py:27
  70.4 7.8 %all-to-all-done.2.mine = bf16[4,2,512,256]{3,2,1,0:T(8,128)(2,1)S(1)} async-done(((bf16[4,2,512,256]{3,2,1,0:T(8,128)(2,1)}), bf16[4,2,512,256]{3,2,1,0:T(8,128)(2,1)S(1)}, u32[]{:S(2)}, u32[]{:S(2)}) %all-to-all-start.2) | async-done | bytes 2097184 | tf_op jit(solution)/shard_map/all_to_all | solution.py:17
  78.2 1.9 %collective-permute-start.2 = (bf16[4,2,512,256]{3,2,1,0:T(8,128)(2,1)S(1)}, bf16[4,2,512,256]{3,2,1,0:T(8,128)(2,1)}, u32[]{:S(2)}, u32[]{:S(2)}) collective-permute-start(bf16[4,2,512,256]{3,2,1,0:T(8,128)(2,1)S(1)} %all-to-all-done.2.mine), channel_id=1, source_target_pairs={{0,1},{1,0},{2,3},{3,2},{4,5},{5,4},{6,7},{7,6},{8,9},{9,8},{10,11... | collective-permute-start | bytes 6291464 | tf_op jit(solution)/shard_map/ppermute | solution.py:27
  80.1 0.1 mul.94
  80.2 0.1 mul.95
  80.3 0.7 pad_add_fusion.place
  81.0 0.7 multiply_convert_fusion.gain_rows
  81.6 15.2 %all-gather.2.cloned.1.call-done = bf16[4096,256]{1,0:T(8,128)(2,1)} async-done(((bf16[512,256]{1,0:T(8,128)(2,1)}), bf16[4096,256]{1,0:T(8,128)(2,1)}) %all-gather.2.cloned.1.call-update) | async-done | bytes 2097168 | tf_op jit(solution)/shard_map/all_gather | solution.py:121
  96.8 0.0 collective-permute-done.2.theirs
  96.8 0.0 copy-done
  96.8 7.0 %shard_map.94 = (bf16[512,512]{1,0:T(8,128)(2,1)}, bf16[8,536,256]{2,1,0:T(8,128)(2,1)}) custom-call(s32[2]{0:T(128)} %pad_add_fusion.place, bf16[4,2,512,256]{3,2,1,0:T(8,128)(2,1)} %copy-done, bf16[4,2,512,256]{3,2,1,0:T(8,128)(2,1)} %collective-permute-done.2.theirs, bf16[8,8,2,32,256]{4,3,2,1,0:T(8,128)(2,1)} %bitcast.19, bf16[512,512]{1,0:T(8,128)(2,1)} %hidden.1, ...), custom_call_target="tpu_custom_call" | custom-call | tf_op jit(solution)/shard_map/pallas_call | solution.py:92
  103.8 0.0 reduce-scatter.2.cloned.1.call-update
  103.8 1.0 copy-done.5
  104.8 1.5 broadcast_in_dim.13
  106.3 4.8 %all-to-all-start.3 = ((bf16[4,512,512]{2,1,0:T(8,128)(2,1)}), bf16[4,512,512]{2,1,0:T(8,128)(2,1)S(1)}, u32[]{:S(2)}, u32[]{:S(2)}) async-start(bf16[4,512,512]{2,1,0:T(8,128)(2,1)} %broadcast_in_dim.13), calls=%async_computation.3 | async-start | bytes 4194304 | tf_op jit(solution)/shard_map/all_to_all | solution.py:17
  111.1 3.0 %collective-permute-start.3 = (bf16[8,64,256]{2,1,0:T(8,128)(2,1)S(1)}, bf16[8,64,256]{2,1,0:T(8,128)(2,1)S(1)}, u32[]{:S(2)}, u32[]{:S(2)}) collective-permute-start(bf16[8,64,256]{2,1,0:T(8,128)(2,1)S(1)} %collective-permute-done.rest_1_), channel_id=1, source_target_pairs={{0,8},{8,16},{16,24},{24,32},{32,40},{40,48},{48,56},{56,0},{1,9},... | collective-permute-start | bytes 786440 | tf_op jit(solution)/shard_map/ppermute | solution.py:27
  114.1 4.0 %collective-permute-start.6 = (bf16[8,64,256]{2,1,0:T(8,128)(2,1)S(1)}, bf16[8,64,256]{2,1,0:T(8,128)(2,1)S(1)}, u32[]{:S(2)}, u32[]{:S(2)}) collective-permute-start(bf16[8,64,256]{2,1,0:T(8,128)(2,1)S(1)} %collective-permute-done.1.rest_7_), channel_id=1, source_target_pairs={{0,56},{8,0},{16,8},{24,16},{32,24},{40,32},{48,40},{56,48},{1,57}... | collective-permute-start | bytes 786440 | tf_op jit(solution)/shard_map/ppermute | solution.py:27
  118.1 2.6 %collective-permute-done.3.rest_2_ = bf16[8,64,256]{2,1,0:T(8,128)(2,1)S(1)} collective-permute-done((bf16[8,64,256]{2,1,0:T(8,128)(2,1)S(1)}, bf16[8,64,256]{2,1,0:T(8,128)(2,1)S(1)}, u32[]{:S(2)}, u32[]{:S(2)}) %collective-permute-start.3) | collective-permute-done | bytes 262176 | tf_op jit(solution)/shard_map/ppermute | solution.py:27
  120.7 2.6 %collective-permute-start.4 = (bf16[8,64,256]{2,1,0:T(8,128)(2,1)S(1)}, bf16[8,64,256]{2,1,0:T(8,128)(2,1)S(1)}, u32[]{:S(2)}, u32[]{:S(2)}) collective-permute-start(bf16[8,64,256]{2,1,0:T(8,128)(2,1)S(1)} %collective-permute-done.3.rest_2_), channel_id=1, source_target_pairs={{0,8},{8,16},{16,24},{24,32},{32,40},{40,48},{48,56},{56,0},{1,9},... | collective-permute-start | bytes 786440 | tf_op jit(solution)/shard_map/ppermute | solution.py:27
  123.3 0.3 collective-permute-done.6.rest_6_
  123.6 4.4 %collective-permute-start.7 = (bf16[8,64,256]{2,1,0:T(8,128)(2,1)S(1)}, bf16[8,64,256]{2,1,0:T(8,128)(2,1)S(1)}, u32[]{:S(2)}, u32[]{:S(2)}) collective-permute-start(bf16[8,64,256]{2,1,0:T(8,128)(2,1)S(1)} %collective-permute-done.6.rest_6_), channel_id=1, source_target_pairs={{0,56},{8,0},{16,8},{24,16},{32,24},{40,32},{48,40},{56,48},{1,57}... | collective-permute-start | bytes 786440 | tf_op jit(solution)/shard_map/ppermute | solution.py:27
  128.0 3.1 %collective-permute-done.4.rest_3_ = bf16[8,64,256]{2,1,0:T(8,128)(2,1)S(1)} collective-permute-done((bf16[8,64,256]{2,1,0:T(8,128)(2,1)S(1)}, bf16[8,64,256]{2,1,0:T(8,128)(2,1)S(1)}, u32[]{:S(2)}, u32[]{:S(2)}) %collective-permute-start.4) | collective-permute-done | bytes 262176 | tf_op jit(solution)/shard_map/ppermute | solution.py:27
  131.1 1.9 %collective-permute-start.5 = (bf16[8,64,256]{2,1,0:T(8,128)(2,1)S(1)}, bf16[8,64,256]{2,1,0:T(8,128)(2,1)S(1)}, u32[]{:S(2)}, u32[]{:S(2)}) collective-permute-start(bf16[8,64,256]{2,1,0:T(8,128)(2,1)S(1)} %collective-permute-done.4.rest_3_), channel_id=1, source_target_pairs={{0,8},{8,16},{16,24},{24,32},{32,40},{40,48},{48,56},{56,0},{1,9},... | collective-permute-start | bytes 786440 | tf_op jit(solution)/shard_map/ppermute | solution.py:27
  133.0 0.0 collective-permute-done.7.rest_5_
  133.0 7.5 %collective-permute-done.5.rest_4_ = bf16[8,64,256]{2,1,0:T(8,128)(2,1)S(1)} collective-permute-done((bf16[8,64,256]{2,1,0:T(8,128)(2,1)S(1)}, bf16[8,64,256]{2,1,0:T(8,128)(2,1)S(1)}, u32[]{:S(2)}, u32[]{:S(2)}) %collective-permute-start.5) | collective-permute-done | bytes 262176 | tf_op jit(solution)/shard_map/ppermute | solution.py:27
  140.6 0.0 all-to-all-done.3.mine
  140.6 1.9 %collective-permute-start.8 = (bf16[4,512,512]{2,1,0:T(8,128)(2,1)S(1)}, bf16[4,512,512]{2,1,0:T(8,128)(2,1)}, u32[]{:S(2)}, u32[]{:S(2)}) collective-permute-start(bf16[4,512,512]{2,1,0:T(8,128)(2,1)S(1)} %all-to-all-done.3.mine), channel_id=1, source_target_pairs={{0,1},{1,0},{2,3},{3,2},{4,5},{5,4},{6,7},{7,6},{8,9},{9,8},{10,11... | collective-permute-start | bytes 6291464 | tf_op jit(solution)/shard_map/ppermute | solution.py:27
  142.5 6.5 %reduce-scatter.2.cloned.1.call-done = bf16[536,256]{1,0:T(8,128)(2,1)} async-done(((bf16[4288,256]{1,0:T(8,128)(2,1)}), bf16[536,256]{1,0:T(8,128)(2,1)}) %reduce-scatter.2.cloned.1.call-update) | async-done | bytes 274448 | tf_op jit(solution)/shard_map/reduce_scatter | solution.py:143
  149.0 1.0 slice.46
  149.9 0.7 convert_reduce_fusion.1
  150.7 0.7 pad_maximum_fusion.1
  151.4 0.0 copy-done.13
  151.4 7.1 %all-to-all-start.4 = ((bf16[8,72,256]{2,1,0:T(8,128)(2,1)}), bf16[8,72,256]{2,1,0:T(8,128)(2,1)S(1)}, u32[]{:S(2)}, u32[]{:S(2)}) async-start(bf16[8,72,256]{2,1,0:T(8,128)(2,1)} %pad_maximum_fusion.1), calls=%async_computation.5 | async-start | bytes 589824 | tf_op jit(solution)/shard_map/all_to_all | solution.py:17
  158.5 0.0 collective-permute-done.8.theirs
  158.5 0.0 copy-done.9
  158.5 0.0 copy-done.10
  158.6 0.0 copy-done.11
  158.6 4.9 %shard_map.95 = bf16[512,256]{1,0:T(8,128)(2,1)} custom-call(s32[2]{0:T(128)} %pad_add_fusion.place, bf16[4,512,512]{2,1,0:T(8,128)(2,1)} %copy-done.1, bf16[4,512,512]{2,1,0:T(8,128)(2,1)} %collective-permute-done.8.theirs, bf16[8,64,256]{2,1,0:T(8,128)(2,1)} %copy-done.4, bf16[8,64,256]{2,1,0:T(8,128)(2,1)} %copy-done.8, bf16[8,64,256]{2,1,0:T(8,128)(2,1)} %copy-done.9, ...), custom_call_target="tpu_custom_call" | custom-call | tf_op jit(solution)/shard_map/pallas_call | solution.py:92
  163.4 5.9 %all-to-all-done.4 = bf16[8,72,256]{2,1,0:T(8,128)(2,1)S(1)} async-done(((bf16[8,72,256]{2,1,0:T(8,128)(2,1)}), bf16[8,72,256]{2,1,0:T(8,128)(2,1)S(1)}, u32[]{:S(2)}, u32[]{:S(2)}) %all-to-all-start.4) | async-done | bytes 294944 | tf_op jit(solution)/shard_map/all_to_all | solution.py:17
  169.4 3.0 %collective-permute-start.9 = (f32[64,256]{1,0:T(8,128)S(1)}, f32[64,256]{1,0:T(8,128)S(1)}, u32[]{:S(2)}, u32[]{:S(2)}) collective-permute-start(f32[64,256]{1,0:T(8,128)S(1)} %slice.48), channel_id=1, source_target_pairs={{0,0},{1,64},{2,128},{3,192},{4,256},{5,320},{6,384},{7,448},{64,1... | collective-permute-start | bytes 196616 | tf_op jit(solution)/shard_map/ppermute | solution.py:165
  172.4 0.6 slice_reduce_fusion
  173.0 6.8 %collective-permute-done.9 = f32[64,256]{1,0:T(8,128)S(1)} collective-permute-done((f32[64,256]{1,0:T(8,128)S(1)}, f32[64,256]{1,0:T(8,128)S(1)}, u32[]{:S(2)}, u32[]{:S(2)}) %collective-permute-start.9) | collective-permute-done | bytes 65568 | tf_op jit(solution)/shard_map/ppermute | solution.py:165
  179.8 0.6 copy.15
  (36 shorter events, 0.2 us)
Async XLA Ops:
  7.2 39.0 %copy-start.3 = (bf16[512,256]{1,0:T(8,128)(2,1)S(1)}, bf16[512,256]{1,0:T(8,128)(2,1)}, u32[]{:S(2)}) copy-start(bf16[512,256]{1,0:T(8,128)(2,1)} %param.13) | copy-start | bytes 786436
  7.2 39.0 %copy-start.14 = (f32[256]{0:T(256)S(1)}, f32[256]{0:T(256)}, u32[]{:S(2)}) copy-start(f32[256]{0:T(256)} %param.10) | copy-start | bytes 3076
  7.2 39.0 %copy-start.2 = (bf16[512,256]{1,0:T(8,128)(2,1)S(1)}, bf16[512,256]{1,0:T(8,128)(2,1)}, u32[]{:S(2)}) copy-start(bf16[512,256]{1,0:T(8,128)(2,1)} %param.9) | copy-start | bytes 786436
  8.8 37.7 %copy-start.6 = (bf16[512,256]{1,0:T(8,128)(2,1)S(1)}, bf16[512,256]{1,0:T(8,128)(2,1)}, u32[]{:S(2)}) copy-start(bf16[512,256]{1,0:T(8,128)(2,1)} %param.7) | copy-start | bytes 786436
  9.6 27.8 %all-to-all-start = ((bf16[8,128,256]{2,1,0:T(8,128)(2,1)}), bf16[8,128,256]{2,1,0:T(8,128)(2,1)S(1)}, u32[]{:S(2)}, u32[]{:S(2)}) async-start(bf16[8,128,256]{2,1,0:T(8,128)(2,1)} %broadcast_in_dim.10), calls=%async_computation | async-start | bytes 1048576 | tf_op jit(solution)/shard_map/all_to_all | solution.py:17
  38.2 21.7 %copy-start.4 = (bf16[8,64,256]{2,1,0:T(8,128)(2,1)}, bf16[8,64,256]{2,1,0:T(8,128)(2,1)S(1)}, u32[]{:S(2)}) copy-start(bf16[8,64,256]{2,1,0:T(8,128)(2,1)S(1)} %get-tuple-element.21.rest_0_) | copy-start | bytes 786436
  48.0 30.1 %all-to-all-start.2 = ((bf16[4,2,512,256]{3,2,1,0:T(8,128)(2,1)}), bf16[4,2,512,256]{3,2,1,0:T(8,128)(2,1)S(1)}, u32[]{:S(2)}, u32[]{:S(2)}) async-start(bf16[4,2,512,256]{3,2,1,0:T(8,128)(2,1)} %broadcast_in_dim.12), calls=%async_computation.2 | async-start | bytes 4194304 | tf_op jit(solution)/shard_map/all_to_all | solution.py:17
  53.7 43.1 %all-gather.2.cloned.1.call-start = ((), (), s32[]{:S(2)}) async-start(), calls=%async_computation.6 | async-start | bytes 2359296 | tf_op jit(solution)/shard_map/all_gather | solution.py:121
  54.4 94.6 %reduce-scatter.2.cloned.1.call-start = ((), (), s32[]{:S(2)}) async-start(), calls=%async_computation.7 | async-start | bytes 2469888 | tf_op jit(solution)/shard_map/reduce_scatter | solution.py:143
  54.4 10.6 %collective-permute-start.1 = (bf16[8,64,256]{2,1,0:T(8,128)(2,1)S(1)}, bf16[8,64,256]{2,1,0:T(8,128)(2,1)S(1)}, u32[]{:S(2)}, u32[]{:S(2)}) collective-permute-start(bf16[8,64,256]{2,1,0:T(8,128)(2,1)S(1)} %get-tuple-element.21.rest_0_), channel_id=1, source_target_pairs={{0,56},{8,0},{16,8},{24,16},{32,24},{40,32},{48,40},{56,48},{1,57}... | collective-permute-start | bytes 786440 | tf_op jit(solution)/shard_map/ppermute | solution.py:27
  59.8 10.5 %collective-permute-start = (bf16[8,64,256]{2,1,0:T(8,128)(2,1)S(1)}, bf16[8,64,256]{2,1,0:T(8,128)(2,1)S(1)}, u32[]{:S(2)}, u32[]{:S(2)}) collective-permute-start(bf16[8,64,256]{2,1,0:T(8,128)(2,1)S(1)} %get-tuple-element.21.rest_0_), channel_id=1, source_target_pairs={{0,8},{8,16},{16,24},{24,32},{32,40},{40,48},{48,56},{56,0},{1,9},... | collective-permute-start | bytes 786440 | tf_op jit(solution)/shard_map/ppermute | solution.py:27
  65.0 49.0 %copy-start.7 = (bf16[8,64,256]{2,1,0:T(8,128)(2,1)}, bf16[8,64,256]{2,1,0:T(8,128)(2,1)S(1)}, u32[]{:S(2)}) copy-start(bf16[8,64,256]{2,1,0:T(8,128)(2,1)S(1)} %collective-permute-done.1.rest_7_) | copy-start | bytes 786436
  70.4 40.7 %copy-start.8 = (bf16[8,64,256]{2,1,0:T(8,128)(2,1)}, bf16[8,64,256]{2,1,0:T(8,128)(2,1)S(1)}, u32[]{:S(2)}) copy-start(bf16[8,64,256]{2,1,0:T(8,128)(2,1)S(1)} %collective-permute-done.rest_1_) | copy-start | bytes 786436
  78.2 18.6 %copy-start = (bf16[4,2,512,256]{3,2,1,0:T(8,128)(2,1)}, bf16[4,2,512,256]{3,2,1,0:T(8,128)(2,1)S(1)}, u32[]{:S(2)}) copy-start(bf16[4,2,512,256]{3,2,1,0:T(8,128)(2,1)S(1)} %all-to-all-done.2.mine) | copy-start | bytes 6291460
  78.2 18.6 %collective-permute-start.2 = (bf16[4,2,512,256]{3,2,1,0:T(8,128)(2,1)S(1)}, bf16[4,2,512,256]{3,2,1,0:T(8,128)(2,1)}, u32[]{:S(2)}, u32[]{:S(2)}) collective-permute-start(bf16[4,2,512,256]{3,2,1,0:T(8,128)(2,1)S(1)} %all-to-all-done.2.mine), channel_id=1, source_target_pairs={{0,1},{1,0},{2,3},{3,2},{4,5},{5,4},{6,7},{7,6},{8,9},{9,8},{10,11... | collective-permute-start | bytes 6291464 | tf_op jit(solution)/shard_map/ppermute | solution.py:27
  103.8 1.0 copy-start.5
  106.3 34.3 %all-to-all-start.3 = ((bf16[4,512,512]{2,1,0:T(8,128)(2,1)}), bf16[4,512,512]{2,1,0:T(8,128)(2,1)S(1)}, u32[]{:S(2)}, u32[]{:S(2)}) async-start(bf16[4,512,512]{2,1,0:T(8,128)(2,1)} %broadcast_in_dim.13), calls=%async_computation.3 | async-start | bytes 4194304 | tf_op jit(solution)/shard_map/all_to_all | solution.py:17
  111.1 9.6 %collective-permute-start.3 = (bf16[8,64,256]{2,1,0:T(8,128)(2,1)S(1)}, bf16[8,64,256]{2,1,0:T(8,128)(2,1)S(1)}, u32[]{:S(2)}, u32[]{:S(2)}) collective-permute-start(bf16[8,64,256]{2,1,0:T(8,128)(2,1)S(1)} %collective-permute-done.rest_1_), channel_id=1, source_target_pairs={{0,8},{8,16},{16,24},{24,32},{32,40},{40,48},{48,56},{56,0},{1,9},... | collective-permute-start | bytes 786440 | tf_op jit(solution)/shard_map/ppermute | solution.py:27
  114.1 9.5 %collective-permute-start.6 = (bf16[8,64,256]{2,1,0:T(8,128)(2,1)S(1)}, bf16[8,64,256]{2,1,0:T(8,128)(2,1)S(1)}, u32[]{:S(2)}, u32[]{:S(2)}) collective-permute-start(bf16[8,64,256]{2,1,0:T(8,128)(2,1)S(1)} %collective-permute-done.1.rest_7_), channel_id=1, source_target_pairs={{0,56},{8,0},{16,8},{24,16},{32,24},{40,32},{48,40},{56,48},{1,57}... | collective-permute-start | bytes 786440 | tf_op jit(solution)/shard_map/ppermute | solution.py:27
  120.7 37.8 %copy-start.9 = (bf16[8,64,256]{2,1,0:T(8,128)(2,1)}, bf16[8,64,256]{2,1,0:T(8,128)(2,1)S(1)}, u32[]{:S(2)}) copy-start(bf16[8,64,256]{2,1,0:T(8,128)(2,1)S(1)} %collective-permute-done.3.rest_2_) | copy-start | bytes 786436
  120.7 10.4 %collective-permute-start.4 = (bf16[8,64,256]{2,1,0:T(8,128)(2,1)S(1)}, bf16[8,64,256]{2,1,0:T(8,128)(2,1)S(1)}, u32[]{:S(2)}, u32[]{:S(2)}) collective-permute-start(bf16[8,64,256]{2,1,0:T(8,128)(2,1)S(1)} %collective-permute-done.3.rest_2_), channel_id=1, source_target_pairs={{0,8},{8,16},{16,24},{24,32},{32,40},{40,48},{48,56},{56,0},{1,9},... | collective-permute-start | bytes 786440 | tf_op jit(solution)/shard_map/ppermute | solution.py:27
  123.6 34.9 %copy-start.10 = (bf16[8,64,256]{2,1,0:T(8,128)(2,1)}, bf16[8,64,256]{2,1,0:T(8,128)(2,1)S(1)}, u32[]{:S(2)}) copy-start(bf16[8,64,256]{2,1,0:T(8,128)(2,1)S(1)} %collective-permute-done.6.rest_6_) | copy-start | bytes 786436
  123.6 9.4 %collective-permute-start.7 = (bf16[8,64,256]{2,1,0:T(8,128)(2,1)S(1)}, bf16[8,64,256]{2,1,0:T(8,128)(2,1)S(1)}, u32[]{:S(2)}, u32[]{:S(2)}) collective-permute-start(bf16[8,64,256]{2,1,0:T(8,128)(2,1)S(1)} %collective-permute-done.6.rest_6_), channel_id=1, source_target_pairs={{0,56},{8,0},{16,8},{24,16},{32,24},{40,32},{48,40},{56,48},{1,57}... | collective-permute-start | bytes 786440 | tf_op jit(solution)/shard_map/ppermute | solution.py:27
  131.1 27.5 %copy-start.11 = (bf16[8,64,256]{2,1,0:T(8,128)(2,1)}, bf16[8,64,256]{2,1,0:T(8,128)(2,1)S(1)}, u32[]{:S(2)}) copy-start(bf16[8,64,256]{2,1,0:T(8,128)(2,1)S(1)} %collective-permute-done.4.rest_3_) | copy-start | bytes 786436
  131.1 9.5 %collective-permute-start.5 = (bf16[8,64,256]{2,1,0:T(8,128)(2,1)S(1)}, bf16[8,64,256]{2,1,0:T(8,128)(2,1)S(1)}, u32[]{:S(2)}, u32[]{:S(2)}) collective-permute-start(bf16[8,64,256]{2,1,0:T(8,128)(2,1)S(1)} %collective-permute-done.4.rest_3_), channel_id=1, source_target_pairs={{0,8},{8,16},{16,24},{24,32},{32,40},{40,48},{48,56},{56,0},{1,9},... | collective-permute-start | bytes 786440 | tf_op jit(solution)/shard_map/ppermute | solution.py:27
  133.0 25.5 %copy-start.12 = (bf16[8,64,256]{2,1,0:T(8,128)(2,1)}, bf16[8,64,256]{2,1,0:T(8,128)(2,1)S(1)}, u32[]{:S(2)}) copy-start(bf16[8,64,256]{2,1,0:T(8,128)(2,1)S(1)} %collective-permute-done.7.rest_5_) | copy-start | bytes 786436
  140.6 10.9 %copy-start.13 = (bf16[8,64,256]{2,1,0:T(8,128)(2,1)}, bf16[8,64,256]{2,1,0:T(8,128)(2,1)S(1)}, u32[]{:S(2)}) copy-start(bf16[8,64,256]{2,1,0:T(8,128)(2,1)S(1)} %collective-permute-done.5.rest_4_) | copy-start | bytes 786436
  140.6 18.0 %copy-start.1 = (bf16[4,512,512]{2,1,0:T(8,128)(2,1)}, bf16[4,512,512]{2,1,0:T(8,128)(2,1)S(1)}, u32[]{:S(2)}) copy-start(bf16[4,512,512]{2,1,0:T(8,128)(2,1)S(1)} %all-to-all-done.3.mine) | copy-start | bytes 6291460
  140.6 18.0 %collective-permute-start.8 = (bf16[4,512,512]{2,1,0:T(8,128)(2,1)S(1)}, bf16[4,512,512]{2,1,0:T(8,128)(2,1)}, u32[]{:S(2)}, u32[]{:S(2)}) collective-permute-start(bf16[4,512,512]{2,1,0:T(8,128)(2,1)S(1)} %all-to-all-done.3.mine), channel_id=1, source_target_pairs={{0,1},{1,0},{2,3},{3,2},{4,5},{5,4},{6,7},{7,6},{8,9},{9,8},{10,11... | collective-permute-start | bytes 6291464 | tf_op jit(solution)/shard_map/ppermute | solution.py:27
  151.4 17.9 %all-to-all-start.4 = ((bf16[8,72,256]{2,1,0:T(8,128)(2,1)}), bf16[8,72,256]{2,1,0:T(8,128)(2,1)S(1)}, u32[]{:S(2)}, u32[]{:S(2)}) async-start(bf16[8,72,256]{2,1,0:T(8,128)(2,1)} %pad_maximum_fusion.1), calls=%async_computation.5 | async-start | bytes 589824 | tf_op jit(solution)/shard_map/all_to_all | solution.py:17
  169.4 10.4 %collective-permute-start.9 = (f32[64,256]{1,0:T(8,128)S(1)}, f32[64,256]{1,0:T(8,128)S(1)}, u32[]{:S(2)}, u32[]{:S(2)}) collective-permute-start(f32[64,256]{1,0:T(8,128)S(1)} %slice.48), channel_id=1, source_target_pairs={{0,0},{1,64},{2,128},{3,192},{4,256},{5,320},{6,384},{7,448},{64,1... | collective-permute-start | bytes 196616 | tf_op jit(solution)/shard_map/ppermute | solution.py:165
Sparse Core Ops, SparseCore 0:
  57.1 39.6 all-gather.1
  103.9 45.0 reduce-scatter.1

commit v8 on v7

--- a/solution.py
+++ b/solution.py
@@ -29,6 +29,16 @@
 
 def swapped(value):
     return shifted(value, "c", 1)
+
+
+def pairwise(value, axes):
+    for axis in reversed(axes):
+        n = lax.axis_size(axis)
+        step = 1
+        while step < n:
+            value = value + lax.ppermute(value, axis, [(i, i ^ step) for i in range(n)])
+            step *= 2
+    return value
 
 
 def after(value, earlier):
@@ -117,13 +127,12 @@
     both = jnp.concatenate([wd[:, :half], wd[:, half:], w_up.T], axis=0)
     both = gather_directly(both, "z")
     wd_rows = 2 * wd.shape[0]
-    wd = wd_z = both[:, :wd_rows].reshape(nz * wd_rows, half)
+    wd = both[:, :wd_rows].reshape(nz * wd_rows, half)
     wd = lax.all_gather(wd, "y", axis=0, tiled=True)
     wd = wd.reshape(ny, nz, 2, wd_rows // 2, half)
     wu = both[:, wd_rows:]
 
-    sums = gather_directly(after(sums, wd_z), TP)
-    sums = jnp.sum(sums, axis=0)
+    sums = pairwise(sums, TP)
     inv_rms = lax.rsqrt(sums[0] / width + norm_eps)[:, None]
     cross_mean = (sums[1] / width)[:, None]
     d_out = (weighted * inv_rms - normed * inv_rms * inv_rms * inv_rms * cross_mean).astype(bf16)

time: 190 us -> 185 us (0.974)
  blocking collectives: 7.95 us -> 0 us
  starting transfers between devices: 58 us -> 65.3 us
  waiting for transfers between devices: 81.1 us -> 75.6 us
    all_to_all x4, waiting for transfers between devices: 29.9 us -> 18.9 us  [exchange(): return lax.all_to_all(chunks, axis, 0, 0, tiled=True)]
    ppermute x0 -> x3, starting transfers between devices: none -> 7.97 us  [pairwise(): value = value + lax.ppermute(value, axis, [(i, i ^ step) for i in range(n)])]
    all_to_all x1 -> x0, blocking collectives: 7.95 us -> none  [exchange(): return lax.all_to_all(chunks, axis, 0, 0, tiled=True)]
    ppermute x0 -> x3, waiting for transfers between devices: none -> 6.44 us  [pairwise(): value = value + lax.ppermute(value, axis, [(i, i ^ step) for i in range(n)])]
    all_gather x1, waiting for transfers between devices: 15.2 us -> 12.6 us  [one_device(): wd = lax.all_gather(wd, 'y', axis=0, tiled=True)]
    ppermute x9, waiting for transfers between devices: 22.1 us -> 24.5 us  [shifted(): return lax.ppermute(value, axis, [(i, (i + by) % n) for i in range(n)])]
    broadcast_in_dim x4 -> x3, local copies, waits for them, and re-layouts: 3.77 us -> 3.81 us  [gather_directly(): return exchange(jnp.broadcast_to(value[None], (n, *value.shape)), axis)]
  transfers between devices with their start and end apart: 16 -> 19, of which waited for: 12 -> 15; matrix products, arithmetic and copies ran while one was open for 4% -> 5% of each run, Pallas kernels for 3% -> 3%
where the time goes in v8:
time: 185 us; the launch traced here: 181 us
  waiting for transfers between devices  75.6 us (41%)
  starting transfers between devices  65.3 us (35%)
  between operations  14.4 us (8%)
  Pallas kernels  11.8 us (6%)
  local copies, waits for them, and re-layouts  8.15 us (4%)
  other arithmetic  5.89 us (3%)
    ppermute x9, starting transfers between devices, shifted(): return lax.ppermute(value, axis, [(i, (i + by) % n) for i in range(n)])  27.4 us
    all_to_all x4, starting transfers between devices, exchange(): return lax.all_to_all(chunks, axis, 0, 0, tiled=True)  26.5 us
    ppermute x9, waiting for transfers between devices, shifted(): return lax.ppermute(value, axis, [(i, (i + by) % n) for i in range(n)])  24.5 us
    all_to_all x4, waiting for transfers between devices, exchange(): return lax.all_to_all(chunks, axis, 0, 0, tiled=True)  18.9 us
    all_gather x1, waiting for transfers between devices, one_device(): wd = lax.all_gather(wd, 'y', axis=0, tiled=True)  12.6 us
    pallas_call x2, Pallas kernels, run(): pl.pallas_call(kernel, out_shape=[jax.ShapeDtypeStruct(shape, bf16) for s...  11.8 us
    ppermute x3, starting transfers between devices, pairwise(): value = value + lax.ppermute(value, axis, [(i, i ^ step) for i in range(n)])  7.97 us
    reduce_scatter x1, waiting for transfers between devices, one_device(): lax.psum_scatter(g.reshape(-1, feats), 'z', scatter_dimension=0, tiled=True)  6.64 us
  transfers between devices with their start and end apart: 19, of which 15 were waited for; matrix products, arithmetic and copies ran while one was open for 5% of the time, Pallas kernels for 3%

profile of v8, /device:TPU:6, one launch (start us, length us, event | category | flops | bytes accessed | tf_op | source)
XLA Modules:
  0.0 181.2 jit_solution(4492700583711251056)
XLA Ops:
  7.2 0.0 copy-start.3
  7.2 0.0 copy-start.14
  7.2 0.0 copy-start.2
  7.2 0.0 copy-start.6
  7.2 1.3 fusion.3
  8.6 1.9 %collective-permute-start = (f32[2,512]{1,0:T(2,128)S(1)}, f32[2,512]{1,0:T(2,128)S(1)}, u32[]{:S(2)}, u32[]{:S(2)}) collective-permute-start(f32[2,512]{1,0:T(2,128)S(1)} %pad_maximum_fusion.3), channel_id=1, source_target_pairs={{0,1},{1,0},{2,3},{3,2},{4,5},{5,4},{6,7},{7,6},{8,9},{9,8},{10,11... | collective-permute-start | bytes 12296 | tf_op jit(solution)/shard_map/ppermute | solution.py:39
  10.5 0.7 fusion.21
  11.2 0.8 pad_maximum_fusion.2
  12.0 0.8 broadcast_in_dim.9
  12.8 10.3 %all-to-all-start.1 = ((bf16[8,128,256]{2,1,0:T(8,128)(2,1)}), bf16[8,128,256]{2,1,0:T(8,128)(2,1)S(1)}, u32[]{:S(2)}, u32[]{:S(2)}) async-start(bf16[8,128,256]{2,1,0:T(8,128)(2,1)} %broadcast_in_dim.9), calls=%async_computation.1 | async-start | bytes 1048576 | tf_op jit(solution)/shard_map/all_to_all | solution.py:17
  23.1 0.0 collective-permute-done
  23.2 2.7 %collective-permute-start.1 = (f32[2,512]{1,0:T(2,128)S(1)}, f32[2,512]{1,0:T(2,128)S(1)}, u32[]{:S(2)}, u32[]{:S(2)}) collective-permute-start(f32[2,512]{1,0:T(2,128)S(1)} %fusion.19), channel_id=1, source_target_pairs={{0,2},{2,0},{4,6},{6,4},{1,3},{3,1},{5,7},{7,5},{8,10},{10,8},{12,... | collective-permute-start | bytes 12296 | tf_op jit(solution)/shard_map/ppermute | solution.py:39
  25.9 2.8 %collective-permute-done.1 = f32[2,512]{1,0:T(2,128)S(1)} collective-permute-done((f32[2,512]{1,0:T(2,128)S(1)}, f32[2,512]{1,0:T(2,128)S(1)}, u32[]{:S(2)}, u32[]{:S(2)}) %collective-permute-start.1) | collective-permute-done | bytes 4128 | tf_op jit(solution)/shard_map/ppermute | solution.py:39
  28.7 3.3 %collective-permute-start.2 = (f32[2,512]{1,0:T(2,128)S(1)}, f32[2,512]{1,0:T(2,128)S(1)}, u32[]{:S(2)}, u32[]{:S(2)}) collective-permute-start(f32[2,512]{1,0:T(2,128)S(1)} %fusion.23), channel_id=1, source_target_pairs={{0,4},{2,6},{4,0},{6,2},{1,5},{3,7},{5,1},{7,3},{8,12},{10,14},{12... | collective-permute-start | bytes 12296 | tf_op jit(solution)/shard_map/ppermute | solution.py:39
  32.0 3.7 %collective-permute-done.2 = f32[2,512]{1,0:T(2,128)S(1)} collective-permute-done((f32[2,512]{1,0:T(2,128)S(1)}, f32[2,512]{1,0:T(2,128)S(1)}, u32[]{:S(2)}, u32[]{:S(2)}) %collective-permute-start.2) | collective-permute-done | bytes 4128 | tf_op jit(solution)/shard_map/ppermute | solution.py:39
  35.7 0.3 fusion.9
  36.1 0.1 pad_maximum_fusion
  36.1 5.2 %all-to-all-done.1 = bf16[8,128,256]{2,1,0:T(8,128)(2,1)S(1)} async-done(((bf16[8,128,256]{2,1,0:T(8,128)(2,1)}), bf16[8,128,256]{2,1,0:T(8,128)(2,1)S(1)}, u32[]{:S(2)}, u32[]{:S(2)}) %all-to-all-start.1) | async-done | bytes 524320 | tf_op jit(solution)/shard_map/all_to_all | solution.py:17
  41.3 1.5 broadcast_in_dim.8
  42.8 4.8 %all-to-all-start = ((bf16[4,2,512,256]{3,2,1,0:T(8,128)(2,1)}), bf16[4,2,512,256]{3,2,1,0:T(8,128)(2,1)S(1)}, u32[]{:S(2)}, u32[]{:S(2)}) async-start(bf16[4,2,512,256]{3,2,1,0:T(8,128)(2,1)} %broadcast_in_dim.8), calls=%async_computation | async-start | bytes 4194304 | tf_op jit(solution)/shard_map/all_to_all | solution.py:17
  47.6 0.7 fusion.20
  48.3 0.0 all-gather.2.cloned.1.call-update
  48.4 0.0 reduce-scatter.2.cloned.1.call-start
  48.4 5.4 %collective-permute-start.4 = (bf16[8,64,256]{2,1,0:T(8,128)(2,1)S(1)}, bf16[8,64,256]{2,1,0:T(8,128)(2,1)S(1)}, u32[]{:S(2)}, u32[]{:S(2)}) collective-permute-start(bf16[8,64,256]{2,1,0:T(8,128)(2,1)S(1)} %get-tuple-element.20.rest_0_), channel_id=1, source_target_pairs={{0,56},{8,0},{16,8},{24,16},{32,24},{40,32},{48,40},{56,48},{1,57}... | collective-permute-start | bytes 786440 | tf_op jit(solution)/shard_map/ppermute | solution.py:27
  53.8 1.9 %collective-permute-start.3 = (bf16[8,64,256]{2,1,0:T(8,128)(2,1)S(1)}, bf16[8,64,256]{2,1,0:T(8,128)(2,1)S(1)}, u32[]{:S(2)}, u32[]{:S(2)}) collective-permute-start(bf16[8,64,256]{2,1,0:T(8,128)(2,1)S(1)} %get-tuple-element.20.rest_0_), channel_id=1, source_target_pairs={{0,8},{8,16},{16,24},{24,32},{32,40},{40,48},{48,56},{56,0},{1,9},... | collective-permute-start | bytes 786440 | tf_op jit(solution)/shard_map/ppermute | solution.py:27
  55.7 3.3 %collective-permute-done.4.rest_7_ = bf16[8,64,256]{2,1,0:T(8,128)(2,1)S(1)} collective-permute-done((bf16[8,64,256]{2,1,0:T(8,128)(2,1)S(1)}, bf16[8,64,256]{2,1,0:T(8,128)(2,1)S(1)}, u32[]{:S(2)}, u32[]{:S(2)}) %collective-permute-start.4) | collective-permute-done | bytes 262176 | tf_op jit(solution)/shard_map/ppermute | solution.py:27
  59.0 5.3 %collective-permute-done.3.rest_1_ = bf16[8,64,256]{2,1,0:T(8,128)(2,1)S(1)} collective-permute-done((bf16[8,64,256]{2,1,0:T(8,128)(2,1)S(1)}, bf16[8,64,256]{2,1,0:T(8,128)(2,1)S(1)}, u32[]{:S(2)}, u32[]{:S(2)}) %collective-permute-start.3) | collective-permute-done | bytes 262176 | tf_op jit(solution)/shard_map/ppermute | solution.py:27
  64.3 7.7 %all-to-all-done.mine = bf16[4,2,512,256]{3,2,1,0:T(8,128)(2,1)S(1)} async-done(((bf16[4,2,512,256]{3,2,1,0:T(8,128)(2,1)}), bf16[4,2,512,256]{3,2,1,0:T(8,128)(2,1)S(1)}, u32[]{:S(2)}, u32[]{:S(2)}) %all-to-all-start) | async-done | bytes 2097184 | tf_op jit(solution)/shard_map/all_to_all | solution.py:17
  72.1 1.9 %collective-permute-start.5 = (bf16[4,2,512,256]{3,2,1,0:T(8,128)(2,1)S(1)}, bf16[4,2,512,256]{3,2,1,0:T(8,128)(2,1)}, u32[]{:S(2)}, u32[]{:S(2)}) collective-permute-start(bf16[4,2,512,256]{3,2,1,0:T(8,128)(2,1)S(1)} %all-to-all-done.mine), channel_id=1, source_target_pairs={{0,1},{1,0},{2,3},{3,2},{4,5},{5,4},{6,7},{7,6},{8,9},{9,8},{10,11... | collective-permute-start | bytes 6291464 | tf_op jit(solution)/shard_map/ppermute | solution.py:27
  74.0 0.1 mul.94
  74.1 0.1 mul.95
  74.2 0.6 pad_add_fusion.place
  74.8 0.7 multiply_convert_fusion.gain_rows
  75.5 2.8 %collective-permute-done.5.theirs = bf16[4,2,512,256]{3,2,1,0:T(8,128)(2,1)} collective-permute-done((bf16[4,2,512,256]{3,2,1,0:T(8,128)(2,1)S(1)}, bf16[4,2,512,256]{3,2,1,0:T(8,128)(2,1)}, u32[]{:S(2)}, u32[]{:S(2)}) %collective-permute-start.5) | collective-permute-done | bytes 2097184 | tf_op jit(solution)/shard_map/ppermute | solution.py:27
  78.2 12.6 %all-gather.2.cloned.1.call-done = bf16[4096,256]{1,0:T(8,128)(2,1)} async-done(((bf16[512,256]{1,0:T(8,128)(2,1)}), bf16[4096,256]{1,0:T(8,128)(2,1)}) %all-gather.2.cloned.1.call-update) | async-done | bytes 2097168 | tf_op jit(solution)/shard_map/all_gather | solution.py:131
  90.9 7.0 %shard_map.94 = (bf16[512,512]{1,0:T(8,128)(2,1)}, bf16[8,536,256]{2,1,0:T(8,128)(2,1)}) custom-call(s32[2]{0:T(128)} %pad_add_fusion.place, bf16[4,2,512,256]{3,2,1,0:T(8,128)(2,1)} %copy-done, bf16[4,2,512,256]{3,2,1,0:T(8,128)(2,1)} %collective-permute-done.5.theirs, bf16[8,8,2,32,256]{4,3,2,1,0:T(8,128)(2,1)} %bitcast.19, bf16[512,512]{1,0:T(8,128)(2,1)} %hidden.1, ...), custom_call_target="tpu_custom_call" | custom-call | tf_op jit(solution)/shard_map/pallas_call | solution.py:102
  97.9 0.0 reduce-scatter.2.cloned.1.call-update
  97.9 1.0 copy-done.5
  98.9 1.5 broadcast_in_dim.10
  100.4 4.7 %all-to-all-start.2 = ((bf16[4,512,512]{2,1,0:T(8,128)(2,1)}), bf16[4,512,512]{2,1,0:T(8,128)(2,1)S(1)}, u32[]{:S(2)}, u32[]{:S(2)}) async-start(bf16[4,512,512]{2,1,0:T(8,128)(2,1)} %broadcast_in_dim.10), calls=%async_computation.2 | async-start | bytes 4194304 | tf_op jit(solution)/shard_map/all_to_all | solution.py:17
  105.1 3.1 %collective-permute-start.6 = (bf16[8,64,256]{2,1,0:T(8,128)(2,1)S(1)}, bf16[8,64,256]{2,1,0:T(8,128)(2,1)S(1)}, u32[]{:S(2)}, u32[]{:S(2)}) collective-permute-start(bf16[8,64,256]{2,1,0:T(8,128)(2,1)S(1)} %collective-permute-done.3.rest_1_), channel_id=1, source_target_pairs={{0,8},{8,16},{16,24},{24,32},{32,40},{40,48},{48,56},{56,0},{1,9},... | collective-permute-start | bytes 786440 | tf_op jit(solution)/shard_map/ppermute | solution.py:27
  108.2 3.9 %collective-permute-start.9 = (bf16[8,64,256]{2,1,0:T(8,128)(2,1)S(1)}, bf16[8,64,256]{2,1,0:T(8,128)(2,1)S(1)}, u32[]{:S(2)}, u32[]{:S(2)}) collective-permute-start(bf16[8,64,256]{2,1,0:T(8,128)(2,1)S(1)} %collective-permute-done.4.rest_7_), channel_id=1, source_target_pairs={{0,56},{8,0},{16,8},{24,16},{32,24},{40,32},{48,40},{56,48},{1,57}... | collective-permute-start | bytes 786440 | tf_op jit(solution)/shard_map/ppermute | solution.py:27
  112.2 2.6 %collective-permute-done.6.rest_2_ = bf16[8,64,256]{2,1,0:T(8,128)(2,1)S(1)} collective-permute-done((bf16[8,64,256]{2,1,0:T(8,128)(2,1)S(1)}, bf16[8,64,256]{2,1,0:T(8,128)(2,1)S(1)}, u32[]{:S(2)}, u32[]{:S(2)}) %collective-permute-start.6) | collective-permute-done | bytes 262176 | tf_op jit(solution)/shard_map/ppermute | solution.py:27
  114.8 2.8 %collective-permute-start.7 = (bf16[8,64,256]{2,1,0:T(8,128)(2,1)S(1)}, bf16[8,64,256]{2,1,0:T(8,128)(2,1)S(1)}, u32[]{:S(2)}, u32[]{:S(2)}) collective-permute-start(bf16[8,64,256]{2,1,0:T(8,128)(2,1)S(1)} %collective-permute-done.6.rest_2_), channel_id=1, source_target_pairs={{0,8},{8,16},{16,24},{24,32},{32,40},{40,48},{48,56},{56,0},{1,9},... | collective-permute-start | bytes 786440 | tf_op jit(solution)/shard_map/ppermute | solution.py:27
  117.6 0.3 collective-permute-done.9.rest_6_
  117.9 4.2 %collective-permute-start.10 = (bf16[8,64,256]{2,1,0:T(8,128)(2,1)S(1)}, bf16[8,64,256]{2,1,0:T(8,128)(2,1)S(1)}, u32[]{:S(2)}, u32[]{:S(2)}) collective-permute-start(bf16[8,64,256]{2,1,0:T(8,128)(2,1)S(1)} %collective-permute-done.9.rest_6_), channel_id=1, source_target_pairs={{0,56},{8,0},{16,8},{24,16},{32,24},{40,32},{48,40},{56,48},{1,57}... | collective-permute-start | bytes 786440 | tf_op jit(solution)/shard_map/ppermute | solution.py:27
  122.1 3.1 %collective-permute-done.7.rest_3_ = bf16[8,64,256]{2,1,0:T(8,128)(2,1)S(1)} collective-permute-done((bf16[8,64,256]{2,1,0:T(8,128)(2,1)S(1)}, bf16[8,64,256]{2,1,0:T(8,128)(2,1)S(1)}, u32[]{:S(2)}, u32[]{:S(2)}) %collective-permute-start.7) | collective-permute-done | bytes 262176 | tf_op jit(solution)/shard_map/ppermute | solution.py:27
  125.2 2.2 %collective-permute-start.8 = (bf16[8,64,256]{2,1,0:T(8,128)(2,1)S(1)}, bf16[8,64,256]{2,1,0:T(8,128)(2,1)S(1)}, u32[]{:S(2)}, u32[]{:S(2)}) collective-permute-start(bf16[8,64,256]{2,1,0:T(8,128)(2,1)S(1)} %collective-permute-done.7.rest_3_), channel_id=1, source_target_pairs={{0,8},{8,16},{16,24},{24,32},{32,40},{40,48},{48,56},{56,0},{1,9},... | collective-permute-start | bytes 786440 | tf_op jit(solution)/shard_map/ppermute | solution.py:27
  127.4 0.0 collective-permute-done.10.rest_5_
  127.4 7.2 %collective-permute-done.8.rest_4_ = bf16[8,64,256]{2,1,0:T(8,128)(2,1)S(1)} collective-permute-done((bf16[8,64,256]{2,1,0:T(8,128)(2,1)S(1)}, bf16[8,64,256]{2,1,0:T(8,128)(2,1)S(1)}, u32[]{:S(2)}, u32[]{:S(2)}) %collective-permute-start.8) | collective-permute-done | bytes 262176 | tf_op jit(solution)/shard_map/ppermute | solution.py:27
  134.6 0.0 all-to-all-done.2.mine
  134.7 1.9 %collective-permute-start.11 = (bf16[4,512,512]{2,1,0:T(8,128)(2,1)S(1)}, bf16[4,512,512]{2,1,0:T(8,128)(2,1)}, u32[]{:S(2)}, u32[]{:S(2)}) collective-permute-start(bf16[4,512,512]{2,1,0:T(8,128)(2,1)S(1)} %all-to-all-done.2.mine), channel_id=1, source_target_pairs={{0,1},{1,0},{2,3},{3,2},{4,5},{5,4},{6,7},{7,6},{8,9},{9,8},{10,11... | collective-permute-start | bytes 6291464 | tf_op jit(solution)/shard_map/ppermute | solution.py:27
  136.6 6.6 %reduce-scatter.2.cloned.1.call-done = bf16[536,256]{1,0:T(8,128)(2,1)} async-done(((bf16[4288,256]{1,0:T(8,128)(2,1)}), bf16[536,256]{1,0:T(8,128)(2,1)}) %reduce-scatter.2.cloned.1.call-update) | async-done | bytes 274448 | tf_op jit(solution)/shard_map/reduce_scatter | solution.py:152
  143.2 1.0 slice.46
  144.2 0.7 convert_reduce_fusion.1
  145.0 0.7 pad_maximum_fusion.1
  145.7 6.7 %all-to-all-start.3 = ((bf16[8,72,256]{2,1,0:T(8,128)(2,1)}), bf16[8,72,256]{2,1,0:T(8,128)(2,1)S(1)}, u32[]{:S(2)}, u32[]{:S(2)}) async-start(bf16[8,72,256]{2,1,0:T(8,128)(2,1)} %pad_maximum_fusion.1), calls=%async_computation.4 | async-start | bytes 589824 | tf_op jit(solution)/shard_map/all_to_all | solution.py:17
  152.4 0.0 collective-permute-done.11.theirs
  152.4 4.9 %shard_map.95 = bf16[512,256]{1,0:T(8,128)(2,1)} custom-call(s32[2]{0:T(128)} %pad_add_fusion.place, bf16[4,512,512]{2,1,0:T(8,128)(2,1)} %copy-done.1, bf16[4,512,512]{2,1,0:T(8,128)(2,1)} %collective-permute-done.11.theirs, bf16[8,64,256]{2,1,0:T(8,128)(2,1)} %copy-done.4, bf16[8,64,256]{2,1,0:T(8,128)(2,1)} %copy-done.8, bf16[8,64,256]{2,1,0:T(8,128)(2,1)} %copy-done.9, ...), custom_call_target="tpu_custom_call" | custom-call | tf_op jit(solution)/shard_map/pallas_call | solution.py:102
  157.3 5.9 %all-to-all-done.3 = bf16[8,72,256]{2,1,0:T(8,128)(2,1)S(1)} async-done(((bf16[8,72,256]{2,1,0:T(8,128)(2,1)}), bf16[8,72,256]{2,1,0:T(8,128)(2,1)S(1)}, u32[]{:S(2)}, u32[]{:S(2)}) %all-to-all-start.3) | async-done | bytes 294944 | tf_op jit(solution)/shard_map/all_to_all | solution.py:17
  163.3 3.4 %collective-permute-start.12 = (f32[64,256]{1,0:T(8,128)S(1)}, f32[64,256]{1,0:T(8,128)S(1)}, u32[]{:S(2)}, u32[]{:S(2)}) collective-permute-start(f32[64,256]{1,0:T(8,128)S(1)} %slice.48), channel_id=1, source_target_pairs={{0,0},{1,64},{2,128},{3,192},{4,256},{5,320},{6,384},{7,448},{64,1... | collective-permute-start | bytes 196616 | tf_op jit(solution)/shard_map/ppermute | solution.py:174
  166.7 0.6 slice_reduce_fusion
  167.3 6.4 %collective-permute-done.12 = f32[64,256]{1,0:T(8,128)S(1)} collective-permute-done((f32[64,256]{1,0:T(8,128)S(1)}, f32[64,256]{1,0:T(8,128)S(1)}, u32[]{:S(2)}, u32[]{:S(2)}) %collective-permute-start.12) | collective-permute-done | bytes 65568 | tf_op jit(solution)/shard_map/ppermute | solution.py:174
  173.7 0.6 copy.11
  (42 shorter events, 0.2 us)
Async XLA Ops:
  7.2 28.5 %copy-start.3 = (bf16[512,256]{1,0:T(8,128)(2,1)S(1)}, bf16[512,256]{1,0:T(8,128)(2,1)}, u32[]{:S(2)}) copy-start(bf16[512,256]{1,0:T(8,128)(2,1)} %param.13) | copy-start | bytes 786436
  7.2 28.5 %copy-start.14 = (f32[256]{0:T(256)S(1)}, f32[256]{0:T(256)}, u32[]{:S(2)}) copy-start(f32[256]{0:T(256)} %param.10) | copy-start | bytes 3076
  7.2 28.5 %copy-start.2 = (bf16[512,256]{1,0:T(8,128)(2,1)S(1)}, bf16[512,256]{1,0:T(8,128)(2,1)}, u32[]{:S(2)}) copy-start(bf16[512,256]{1,0:T(8,128)(2,1)} %param.9) | copy-start | bytes 786436
  7.2 28.8 %copy-start.6 = (bf16[512,256]{1,0:T(8,128)(2,1)S(1)}, bf16[512,256]{1,0:T(8,128)(2,1)}, u32[]{:S(2)}) copy-start(bf16[512,256]{1,0:T(8,128)(2,1)} %param.7) | copy-start | bytes 786436
  8.6 14.6 %collective-permute-start = (f32[2,512]{1,0:T(2,128)S(1)}, f32[2,512]{1,0:T(2,128)S(1)}, u32[]{:S(2)}, u32[]{:S(2)}) collective-permute-start(f32[2,512]{1,0:T(2,128)S(1)} %pad_maximum_fusion.3), channel_id=1, source_target_pairs={{0,1},{1,0},{2,3},{3,2},{4,5},{5,4},{6,7},{7,6},{8,9},{9,8},{10,11... | collective-permute-start | bytes 12296 | tf_op jit(solution)/shard_map/ppermute | solution.py:39
  12.8 28.5 %all-to-all-start.1 = ((bf16[8,128,256]{2,1,0:T(8,128)(2,1)}), bf16[8,128,256]{2,1,0:T(8,128)(2,1)S(1)}, u32[]{:S(2)}, u32[]{:S(2)}) async-start(bf16[8,128,256]{2,1,0:T(8,128)(2,1)} %broadcast_in_dim.9), calls=%async_computation.1 | async-start | bytes 1048576 | tf_op jit(solution)/shard_map/all_to_all | solution.py:17
  23.2 5.5 %collective-permute-start.1 = (f32[2,512]{1,0:T(2,128)S(1)}, f32[2,512]{1,0:T(2,128)S(1)}, u32[]{:S(2)}, u32[]{:S(2)}) collective-permute-start(f32[2,512]{1,0:T(2,128)S(1)} %fusion.19), channel_id=1, source_target_pairs={{0,2},{2,0},{4,6},{6,4},{1,3},{3,1},{5,7},{7,5},{8,10},{10,8},{12,... | collective-permute-start | bytes 12296 | tf_op jit(solution)/shard_map/ppermute | solution.py:39
  28.7 7.0 %collective-permute-start.2 = (f32[2,512]{1,0:T(2,128)S(1)}, f32[2,512]{1,0:T(2,128)S(1)}, u32[]{:S(2)}, u32[]{:S(2)}) collective-permute-start(f32[2,512]{1,0:T(2,128)S(1)} %fusion.23), channel_id=1, source_target_pairs={{0,4},{2,6},{4,0},{6,2},{1,5},{3,7},{5,1},{7,3},{8,12},{10,14},{12... | collective-permute-start | bytes 12296 | tf_op jit(solution)/shard_map/ppermute | solution.py:39
  42.8 29.2 %all-to-all-start = ((bf16[4,2,512,256]{3,2,1,0:T(8,128)(2,1)}), bf16[4,2,512,256]{3,2,1,0:T(8,128)(2,1)S(1)}, u32[]{:S(2)}, u32[]{:S(2)}) async-start(bf16[4,2,512,256]{3,2,1,0:T(8,128)(2,1)} %broadcast_in_dim.8), calls=%async_computation | async-start | bytes 4194304 | tf_op jit(solution)/shard_map/all_to_all | solution.py:17
  47.6 43.3 %all-gather.2.cloned.1.call-start = ((), (), s32[]{:S(2)}) async-start(), calls=%async_computation.5 | async-start | bytes 2359296 | tf_op jit(solution)/shard_map/all_gather | solution.py:131
  48.3 49.5 %copy-start.4 = (bf16[8,64,256]{2,1,0:T(8,128)(2,1)}, bf16[8,64,256]{2,1,0:T(8,128)(2,1)S(1)}, u32[]{:S(2)}) copy-start(bf16[8,64,256]{2,1,0:T(8,128)(2,1)S(1)} %get-tuple-element.20.rest_0_) | copy-start | bytes 786436
  48.4 94.9 %reduce-scatter.2.cloned.1.call-start = ((), (), s32[]{:S(2)}) async-start(), calls=%async_computation.6 | async-start | bytes 2469888 | tf_op jit(solution)/shard_map/reduce_scatter | solution.py:152
  48.4 10.6 %collective-permute-start.4 = (bf16[8,64,256]{2,1,0:T(8,128)(2,1)S(1)}, bf16[8,64,256]{2,1,0:T(8,128)(2,1)S(1)}, u32[]{:S(2)}, u32[]{:S(2)}) collective-permute-start(bf16[8,64,256]{2,1,0:T(8,128)(2,1)S(1)} %get-tuple-element.20.rest_0_), channel_id=1, source_target_pairs={{0,56},{8,0},{16,8},{24,16},{32,24},{40,32},{48,40},{56,48},{1,57}... | collective-permute-start | bytes 786440 | tf_op jit(solution)/shard_map/ppermute | solution.py:27
  53.8 10.5 %collective-permute-start.3 = (bf16[8,64,256]{2,1,0:T(8,128)(2,1)S(1)}, bf16[8,64,256]{2,1,0:T(8,128)(2,1)S(1)}, u32[]{:S(2)}, u32[]{:S(2)}) collective-permute-start(bf16[8,64,256]{2,1,0:T(8,128)(2,1)S(1)} %get-tuple-element.20.rest_0_), channel_id=1, source_target_pairs={{0,8},{8,16},{16,24},{24,32},{32,40},{40,48},{48,56},{56,0},{1,9},... | collective-permute-start | bytes 786440 | tf_op jit(solution)/shard_map/ppermute | solution.py:27
  59.0 49.2 %copy-start.7 = (bf16[8,64,256]{2,1,0:T(8,128)(2,1)}, bf16[8,64,256]{2,1,0:T(8,128)(2,1)S(1)}, u32[]{:S(2)}) copy-start(bf16[8,64,256]{2,1,0:T(8,128)(2,1)S(1)} %collective-permute-done.4.rest_7_) | copy-start | bytes 786436
  64.3 40.8 %copy-start.8 = (bf16[8,64,256]{2,1,0:T(8,128)(2,1)}, bf16[8,64,256]{2,1,0:T(8,128)(2,1)S(1)}, u32[]{:S(2)}) copy-start(bf16[8,64,256]{2,1,0:T(8,128)(2,1)S(1)} %collective-permute-done.3.rest_1_) | copy-start | bytes 786436
  72.1 18.8 %copy-start = (bf16[4,2,512,256]{3,2,1,0:T(8,128)(2,1)}, bf16[4,2,512,256]{3,2,1,0:T(8,128)(2,1)S(1)}, u32[]{:S(2)}) copy-start(bf16[4,2,512,256]{3,2,1,0:T(8,128)(2,1)S(1)} %all-to-all-done.mine) | copy-start | bytes 6291460
  72.1 6.2 %collective-permute-start.5 = (bf16[4,2,512,256]{3,2,1,0:T(8,128)(2,1)S(1)}, bf16[4,2,512,256]{3,2,1,0:T(8,128)(2,1)}, u32[]{:S(2)}, u32[]{:S(2)}) collective-permute-start(bf16[4,2,512,256]{3,2,1,0:T(8,128)(2,1)S(1)} %all-to-all-done.mine), channel_id=1, source_target_pairs={{0,1},{1,0},{2,3},{3,2},{4,5},{5,4},{6,7},{7,6},{8,9},{9,8},{10,11... | collective-permute-start | bytes 6291464 | tf_op jit(solution)/shard_map/ppermute | solution.py:27
  97.8 1.0 copy-start.5
  100.4 34.3 %all-to-all-start.2 = ((bf16[4,512,512]{2,1,0:T(8,128)(2,1)}), bf16[4,512,512]{2,1,0:T(8,128)(2,1)S(1)}, u32[]{:S(2)}, u32[]{:S(2)}) async-start(bf16[4,512,512]{2,1,0:T(8,128)(2,1)} %broadcast_in_dim.10), calls=%async_computation.2 | async-start | bytes 4194304 | tf_op jit(solution)/shard_map/all_to_all | solution.py:17
  105.1 9.7 %collective-permute-start.6 = (bf16[8,64,256]{2,1,0:T(8,128)(2,1)S(1)}, bf16[8,64,256]{2,1,0:T(8,128)(2,1)S(1)}, u32[]{:S(2)}, u32[]{:S(2)}) collective-permute-start(bf16[8,64,256]{2,1,0:T(8,128)(2,1)S(1)} %collective-permute-done.3.rest_1_), channel_id=1, source_target_pairs={{0,8},{8,16},{16,24},{24,32},{32,40},{40,48},{48,56},{56,0},{1,9},... | collective-permute-start | bytes 786440 | tf_op jit(solution)/shard_map/ppermute | solution.py:27
  108.2 9.6 %collective-permute-start.9 = (bf16[8,64,256]{2,1,0:T(8,128)(2,1)S(1)}, bf16[8,64,256]{2,1,0:T(8,128)(2,1)S(1)}, u32[]{:S(2)}, u32[]{:S(2)}) collective-permute-start(bf16[8,64,256]{2,1,0:T(8,128)(2,1)S(1)} %collective-permute-done.4.rest_7_), channel_id=1, source_target_pairs={{0,56},{8,0},{16,8},{24,16},{32,24},{40,32},{48,40},{56,48},{1,57}... | collective-permute-start | bytes 786440 | tf_op jit(solution)/shard_map/ppermute | solution.py:27
  114.8 37.6 %copy-start.9 = (bf16[8,64,256]{2,1,0:T(8,128)(2,1)}, bf16[8,64,256]{2,1,0:T(8,128)(2,1)S(1)}, u32[]{:S(2)}) copy-start(bf16[8,64,256]{2,1,0:T(8,128)(2,1)S(1)} %collective-permute-done.6.rest_2_) | copy-start | bytes 786436
  114.8 10.4 %collective-permute-start.7 = (bf16[8,64,256]{2,1,0:T(8,128)(2,1)S(1)}, bf16[8,64,256]{2,1,0:T(8,128)(2,1)S(1)}, u32[]{:S(2)}, u32[]{:S(2)}) collective-permute-start(bf16[8,64,256]{2,1,0:T(8,128)(2,1)S(1)} %collective-permute-done.6.rest_2_), channel_id=1, source_target_pairs={{0,8},{8,16},{16,24},{24,32},{32,40},{40,48},{48,56},{56,0},{1,9},... | collective-permute-start | bytes 786440 | tf_op jit(solution)/shard_map/ppermute | solution.py:27
  117.9 34.5 %copy-start.10 = (bf16[8,64,256]{2,1,0:T(8,128)(2,1)}, bf16[8,64,256]{2,1,0:T(8,128)(2,1)S(1)}, u32[]{:S(2)}) copy-start(bf16[8,64,256]{2,1,0:T(8,128)(2,1)S(1)} %collective-permute-done.9.rest_6_) | copy-start | bytes 786436
  117.9 9.5 %collective-permute-start.10 = (bf16[8,64,256]{2,1,0:T(8,128)(2,1)S(1)}, bf16[8,64,256]{2,1,0:T(8,128)(2,1)S(1)}, u32[]{:S(2)}, u32[]{:S(2)}) collective-permute-start(bf16[8,64,256]{2,1,0:T(8,128)(2,1)S(1)} %collective-permute-done.9.rest_6_), channel_id=1, source_target_pairs={{0,56},{8,0},{16,8},{24,16},{32,24},{40,32},{48,40},{56,48},{1,57}... | collective-permute-start | bytes 786440 | tf_op jit(solution)/shard_map/ppermute | solution.py:27
  125.2 27.2 %copy-start.11 = (bf16[8,64,256]{2,1,0:T(8,128)(2,1)}, bf16[8,64,256]{2,1,0:T(8,128)(2,1)S(1)}, u32[]{:S(2)}) copy-start(bf16[8,64,256]{2,1,0:T(8,128)(2,1)S(1)} %collective-permute-done.7.rest_3_) | copy-start | bytes 786436
  125.2 9.5 %collective-permute-start.8 = (bf16[8,64,256]{2,1,0:T(8,128)(2,1)S(1)}, bf16[8,64,256]{2,1,0:T(8,128)(2,1)S(1)}, u32[]{:S(2)}, u32[]{:S(2)}) collective-permute-start(bf16[8,64,256]{2,1,0:T(8,128)(2,1)S(1)} %collective-permute-done.7.rest_3_), channel_id=1, source_target_pairs={{0,8},{8,16},{16,24},{24,32},{32,40},{40,48},{48,56},{56,0},{1,9},... | collective-permute-start | bytes 786440 | tf_op jit(solution)/shard_map/ppermute | solution.py:27
  127.4 25.0 %copy-start.12 = (bf16[8,64,256]{2,1,0:T(8,128)(2,1)}, bf16[8,64,256]{2,1,0:T(8,128)(2,1)S(1)}, u32[]{:S(2)}) copy-start(bf16[8,64,256]{2,1,0:T(8,128)(2,1)S(1)} %collective-permute-done.10.rest_5_) | copy-start | bytes 786436
  134.6 11.0 %copy-start.13 = (bf16[8,64,256]{2,1,0:T(8,128)(2,1)}, bf16[8,64,256]{2,1,0:T(8,128)(2,1)S(1)}, u32[]{:S(2)}) copy-start(bf16[8,64,256]{2,1,0:T(8,128)(2,1)S(1)} %collective-permute-done.8.rest_4_) | copy-start | bytes 786436
  134.6 17.8 %copy-start.1 = (bf16[4,512,512]{2,1,0:T(8,128)(2,1)}, bf16[4,512,512]{2,1,0:T(8,128)(2,1)S(1)}, u32[]{:S(2)}) copy-start(bf16[4,512,512]{2,1,0:T(8,128)(2,1)S(1)} %all-to-all-done.2.mine) | copy-start | bytes 6291460
  134.7 17.7 %collective-permute-start.11 = (bf16[4,512,512]{2,1,0:T(8,128)(2,1)S(1)}, bf16[4,512,512]{2,1,0:T(8,128)(2,1)}, u32[]{:S(2)}, u32[]{:S(2)}) collective-permute-start(bf16[4,512,512]{2,1,0:T(8,128)(2,1)S(1)} %all-to-all-done.2.mine), channel_id=1, source_target_pairs={{0,1},{1,0},{2,3},{3,2},{4,5},{5,4},{6,7},{7,6},{8,9},{9,8},{10,11... | collective-permute-start | bytes 6291464 | tf_op jit(solution)/shard_map/ppermute | solution.py:27
  145.7 17.5 %all-to-all-start.3 = ((bf16[8,72,256]{2,1,0:T(8,128)(2,1)}), bf16[8,72,256]{2,1,0:T(8,128)(2,1)S(1)}, u32[]{:S(2)}, u32[]{:S(2)}) async-start(bf16[8,72,256]{2,1,0:T(8,128)(2,1)} %pad_maximum_fusion.1), calls=%async_computation.4 | async-start | bytes 589824 | tf_op jit(solution)/shard_map/all_to_all | solution.py:17
  163.3 10.4 %collective-permute-start.12 = (f32[64,256]{1,0:T(8,128)S(1)}, f32[64,256]{1,0:T(8,128)S(1)}, u32[]{:S(2)}, u32[]{:S(2)}) collective-permute-start(f32[64,256]{1,0:T(8,128)S(1)} %slice.48), channel_id=1, source_target_pairs={{0,0},{1,64},{2,128},{3,192},{4,256},{5,320},{6,384},{7,448},{64,1... | collective-permute-start | bytes 196616 | tf_op jit(solution)/shard_map/ppermute | solution.py:174
Sparse Core Ops, SparseCore 0:
  51.0 39.7 all-gather.1
  98.0 45.1 reduce-scatter.1

commit v9 on v8

--- a/solution.py
+++ b/solution.py
@@ -140,9 +140,9 @@
 
     wu = after(wu, inv_rms)
     pieces = [wu] * ny
-    pieces[1], pieces[ny - 1] = shifted(wu, "y", 1), shifted(wu, "y", -1)
+    pieces[1] = shifted(wu, "y", 1)
     mine = gather_directly(jnp.stack([d_out, inputs]), "x")
-    theirs = swapped(after(mine, (pieces[1], pieces[ny - 1])))
+    theirs = swapped(after(mine, pieces[1]))
     turn = (jnp.arange(nz) == lax.axis_index("z")).astype(f32)[:, None, None]
     gain_rows = (turn * in_three(gain_part)).reshape(3 * nz, feats).astype(bf16)
     d_pre, g = run(
@@ -151,12 +151,10 @@
     )
     g = lax.psum_scatter(g.reshape(-1, feats), "z", scatter_dimension=0, tiled=True)
 
-    pieces[1] = after(pieces[1], d_pre)
-    pieces[ny - 1] = after(pieces[ny - 1], d_pre)
-    for d in range(2, ny // 2 + 1):
-        pieces[d] = shifted(pieces[d - 1], "y", 1)
-        if ny - d > d:
-            pieces[ny - d] = shifted(pieces[(ny - d + 1) % ny], "y", -1)
+    pieces[1], left = after(pieces[1], d_pre), after(wu, d_pre)
+    for d in range(1, ny // 2):
+        pieces[d + 1] = shifted(pieces[d], "y", 1)
+        pieces[ny - d] = left = shifted(left, "y", -1)
     mine = gather_directly(d_pre, "x")
     theirs = swapped(after(mine, pieces))
     [grad_input] = run(

time: 185 us -> 184 us (level)
    all_to_all x4, waiting for transfers between devices: 18.9 us -> 23.5 us  [exchange(): return lax.all_to_all(chunks, axis, 0, 0, tiled=True)]
    ppermute x9, waiting for transfers between devices: 24.5 us -> 21.3 us  [shifted(): return lax.ppermute(value, axis, [(i, (i + by) % n) for i in range(n)])]
    reduce_scatter x1, waiting for transfers between devices: 6.64 us -> 4.6 us  [one_device(): lax.psum_scatter(g.reshape(-1, feats), 'z', scatter_dimension=0, tiled=True)]
  transfers between devices with their start and end apart: 19 -> 19, of which waited for: 15 -> 16; matrix products, arithmetic and copies ran while one was open for 5% -> 5% of each run, Pallas kernels for 3% -> 3%
where the time goes in v9:
time: 184 us; the launch traced here: 181 us
  waiting for transfers between devices  75.1 us (41%)
  starting transfers between devices  66.1 us (36%)
  between operations  14.3 us (8%)
  Pallas kernels  11.8 us (6%)
  local copies, waits for them, and re-layouts  8.16 us (4%)
  other arithmetic  5.9 us (3%)
    ppermute x9, starting transfers between devices, shifted(): return lax.ppermute(value, axis, [(i, (i + by) % n) for i in range(n)])  28.1 us
    all_to_all x4, starting transfers between devices, exchange(): return lax.all_to_all(chunks, axis, 0, 0, tiled=True)  26.5 us
    all_to_all x4, waiting for transfers between devices, exchange(): return lax.all_to_all(chunks, axis, 0, 0, tiled=True)  23.5 us
    ppermute x9, waiting for transfers between devices, shifted(): return lax.ppermute(value, axis, [(i, (i + by) % n) for i in range(n)])  21.3 us
    all_gather x1, waiting for transfers between devices, one_device(): wd = lax.all_gather(wd, 'y', axis=0, tiled=True)  12.6 us
    pallas_call x2, Pallas kernels, run(): pl.pallas_call(kernel, out_shape=[jax.ShapeDtypeStruct(shape, bf16) for s...  11.8 us
    ppermute x3, starting transfers between devices, pairwise(): value = value + lax.ppermute(value, axis, [(i, i ^ step) for i in range(n)])  7.97 us
    ppermute x1, waiting for transfers between devices, one_device(): grad_up = lax.ppermute(g[:rows], ('z', 'x', 'c'), swap).T  6.63 us
  transfers between devices with their start and end apart: 19, of which 16 were waited for; matrix products, arithmetic and copies ran while one was open for 5% of the time, Pallas kernels for 3%

profile of v9, /device:TPU:6, one launch (start us, length us, event | category | flops | bytes accessed | tf_op | source)
XLA Modules:
  0.0 181.4 jit_solution(5387213180128909202)
XLA Ops:
  7.2 1.3 fusion.3
  8.6 1.9 %collective-permute-start = (f32[2,512]{1,0:T(2,128)S(1)}, f32[2,512]{1,0:T(2,128)S(1)}, u32[]{:S(2)}, u32[]{:S(2)}) collective-permute-start(f32[2,512]{1,0:T(2,128)S(1)} %pad_maximum_fusion.3), channel_id=1, source_target_pairs={{0,1},{1,0},{2,3},{3,2},{4,5},{5,4},{6,7},{7,6},{8,9},{9,8},{10,11... | collective-permute-start | bytes 12296 | tf_op jit(solution)/shard_map/ppermute | solution.py:39
  10.5 0.7 fusion.21
  11.2 0.8 pad_maximum_fusion.2
  12.0 0.8 broadcast_in_dim.9
  12.8 10.3 %all-to-all-start.1 = ((bf16[8,128,256]{2,1,0:T(8,128)(2,1)}), bf16[8,128,256]{2,1,0:T(8,128)(2,1)S(1)}, u32[]{:S(2)}, u32[]{:S(2)}) async-start(bf16[8,128,256]{2,1,0:T(8,128)(2,1)} %broadcast_in_dim.9), calls=%async_computation.1 | async-start | bytes 1048576 | tf_op jit(solution)/shard_map/all_to_all | solution.py:17
  23.1 0.0 collective-permute-done
  23.2 2.7 %collective-permute-start.1 = (f32[2,512]{1,0:T(2,128)S(1)}, f32[2,512]{1,0:T(2,128)S(1)}, u32[]{:S(2)}, u32[]{:S(2)}) collective-permute-start(f32[2,512]{1,0:T(2,128)S(1)} %fusion.19), channel_id=1, source_target_pairs={{0,2},{2,0},{4,6},{6,4},{1,3},{3,1},{5,7},{7,5},{8,10},{10,8},{12,... | collective-permute-start | bytes 12296 | tf_op jit(solution)/shard_map/ppermute | solution.py:39
  25.9 2.8 %collective-permute-done.1 = f32[2,512]{1,0:T(2,128)S(1)} collective-permute-done((f32[2,512]{1,0:T(2,128)S(1)}, f32[2,512]{1,0:T(2,128)S(1)}, u32[]{:S(2)}, u32[]{:S(2)}) %collective-permute-start.1) | collective-permute-done | bytes 4128 | tf_op jit(solution)/shard_map/ppermute | solution.py:39
  28.7 3.3 %collective-permute-start.2 = (f32[2,512]{1,0:T(2,128)S(1)}, f32[2,512]{1,0:T(2,128)S(1)}, u32[]{:S(2)}, u32[]{:S(2)}) collective-permute-start(f32[2,512]{1,0:T(2,128)S(1)} %fusion.23), channel_id=1, source_target_pairs={{0,4},{2,6},{4,0},{6,2},{1,5},{3,7},{5,1},{7,3},{8,12},{10,14},{12... | collective-permute-start | bytes 12296 | tf_op jit(solution)/shard_map/ppermute | solution.py:39
  32.0 3.7 %collective-permute-done.2 = f32[2,512]{1,0:T(2,128)S(1)} collective-permute-done((f32[2,512]{1,0:T(2,128)S(1)}, f32[2,512]{1,0:T(2,128)S(1)}, u32[]{:S(2)}, u32[]{:S(2)}) %collective-permute-start.2) | collective-permute-done | bytes 4128 | tf_op jit(solution)/shard_map/ppermute | solution.py:39
  35.7 0.3 fusion.9
  36.0 0.0 copy-done.6
  36.1 0.1 pad_maximum_fusion
  36.1 5.2 %all-to-all-done.1 = bf16[8,128,256]{2,1,0:T(8,128)(2,1)S(1)} async-done(((bf16[8,128,256]{2,1,0:T(8,128)(2,1)}), bf16[8,128,256]{2,1,0:T(8,128)(2,1)S(1)}, u32[]{:S(2)}, u32[]{:S(2)}) %all-to-all-start.1) | async-done | bytes 524320 | tf_op jit(solution)/shard_map/all_to_all | solution.py:17
  41.3 1.5 broadcast_in_dim.8
  42.8 4.8 %all-to-all-start = ((bf16[4,2,512,256]{3,2,1,0:T(8,128)(2,1)}), bf16[4,2,512,256]{3,2,1,0:T(8,128)(2,1)S(1)}, u32[]{:S(2)}, u32[]{:S(2)}) async-start(bf16[4,2,512,256]{3,2,1,0:T(8,128)(2,1)} %broadcast_in_dim.8), calls=%async_computation | async-start | bytes 4194304 | tf_op jit(solution)/shard_map/all_to_all | solution.py:17
  47.6 0.0 all-gather.2.cloned.1.call-start
  47.6 0.7 fusion.20
  48.3 0.0 all-gather.2.cloned.1.call-update
  48.4 0.0 reduce-scatter.2.cloned.1.call-start
  48.4 3.5 %collective-permute-start.3 = (bf16[8,64,256]{2,1,0:T(8,128)(2,1)S(1)}, bf16[8,64,256]{2,1,0:T(8,128)(2,1)S(1)}, u32[]{:S(2)}, u32[]{:S(2)}) collective-permute-start(bf16[8,64,256]{2,1,0:T(8,128)(2,1)S(1)} %get-tuple-element.12.rest_0_), channel_id=1, source_target_pairs={{0,8},{8,16},{16,24},{24,32},{32,40},{40,48},{48,56},{56,0},{1,9},... | collective-permute-start | bytes 786440 | tf_op jit(solution)/shard_map/ppermute | solution.py:27
  51.9 7.8 %collective-permute-done.3.rest_1_ = bf16[8,64,256]{2,1,0:T(8,128)(2,1)S(1)} collective-permute-done((bf16[8,64,256]{2,1,0:T(8,128)(2,1)S(1)}, bf16[8,64,256]{2,1,0:T(8,128)(2,1)S(1)}, u32[]{:S(2)}, u32[]{:S(2)}) %collective-permute-start.3) | collective-permute-done | bytes 262176 | tf_op jit(solution)/shard_map/ppermute | solution.py:27
  59.7 12.3 %all-to-all-done.mine = bf16[4,2,512,256]{3,2,1,0:T(8,128)(2,1)S(1)} async-done(((bf16[4,2,512,256]{3,2,1,0:T(8,128)(2,1)}), bf16[4,2,512,256]{3,2,1,0:T(8,128)(2,1)S(1)}, u32[]{:S(2)}, u32[]{:S(2)}) %all-to-all-start) | async-done | bytes 2097184 | tf_op jit(solution)/shard_map/all_to_all | solution.py:17
  72.1 1.9 %collective-permute-start.4 = (bf16[4,2,512,256]{3,2,1,0:T(8,128)(2,1)S(1)}, bf16[4,2,512,256]{3,2,1,0:T(8,128)(2,1)}, u32[]{:S(2)}, u32[]{:S(2)}) collective-permute-start(bf16[4,2,512,256]{3,2,1,0:T(8,128)(2,1)S(1)} %all-to-all-done.mine), channel_id=1, source_target_pairs={{0,1},{1,0},{2,3},{3,2},{4,5},{5,4},{6,7},{7,6},{8,9},{9,8},{10,11... | collective-permute-start | bytes 6291464 | tf_op jit(solution)/shard_map/ppermute | solution.py:27
  74.0 0.1 mul.94
  74.1 0.1 mul.95
  74.2 0.6 pad_add_fusion.place
  74.8 0.7 multiply_convert_fusion.gain_rows
  75.5 2.8 %collective-permute-done.4.theirs = bf16[4,2,512,256]{3,2,1,0:T(8,128)(2,1)} collective-permute-done((bf16[4,2,512,256]{3,2,1,0:T(8,128)(2,1)S(1)}, bf16[4,2,512,256]{3,2,1,0:T(8,128)(2,1)}, u32[]{:S(2)}, u32[]{:S(2)}) %collective-permute-start.4) | collective-permute-done | bytes 2097184 | tf_op jit(solution)/shard_map/ppermute | solution.py:27
  78.2 12.6 %all-gather.2.cloned.1.call-done = bf16[4096,256]{1,0:T(8,128)(2,1)} async-done(((bf16[512,256]{1,0:T(8,128)(2,1)}), bf16[4096,256]{1,0:T(8,128)(2,1)}) %all-gather.2.cloned.1.call-update) | async-done | bytes 2097168 | tf_op jit(solution)/shard_map/all_gather | solution.py:131
  90.9 7.0 %shard_map.94 = (bf16[512,512]{1,0:T(8,128)(2,1)}, bf16[8,536,256]{2,1,0:T(8,128)(2,1)}) custom-call(s32[2]{0:T(128)} %pad_add_fusion.place, bf16[4,2,512,256]{3,2,1,0:T(8,128)(2,1)} %copy-done, bf16[4,2,512,256]{3,2,1,0:T(8,128)(2,1)} %collective-permute-done.4.theirs, bf16[8,8,2,32,256]{4,3,2,1,0:T(8,128)(2,1)} %bitcast.19, bf16[512,512]{1,0:T(8,128)(2,1)} %hidden.1, ...), custom_call_target="tpu_custom_call" | custom-call | tf_op jit(solution)/shard_map/pallas_call | solution.py:102
  97.9 0.0 reduce-scatter.2.cloned.1.call-update
  97.9 1.0 copy-done.5
  98.9 1.5 broadcast_in_dim.10
  100.4 4.7 %all-to-all-start.2 = ((bf16[4,512,512]{2,1,0:T(8,128)(2,1)}), bf16[4,512,512]{2,1,0:T(8,128)(2,1)S(1)}, u32[]{:S(2)}, u32[]{:S(2)}) async-start(bf16[4,512,512]{2,1,0:T(8,128)(2,1)} %broadcast_in_dim.10), calls=%async_computation.2 | async-start | bytes 4194304 | tf_op jit(solution)/shard_map/all_to_all | solution.py:17
  105.1 0.0 copy-done.7
  105.1 3.1 %collective-permute-start.5 = (bf16[8,64,256]{2,1,0:T(8,128)(2,1)S(1)}, bf16[8,64,256]{2,1,0:T(8,128)(2,1)S(1)}, u32[]{:S(2)}, u32[]{:S(2)}) collective-permute-start(bf16[8,64,256]{2,1,0:T(8,128)(2,1)S(1)} %collective-permute-done.3.rest_1_), channel_id=1, source_target_pairs={{0,8},{8,16},{16,24},{24,32},{32,40},{40,48},{48,56},{56,0},{1,9},... | collective-permute-start | bytes 786440 | tf_op jit(solution)/shard_map/ppermute | solution.py:27
  108.2 3.9 %collective-permute-start.8 = (bf16[8,64,256]{2,1,0:T(8,128)(2,1)S(1)}, bf16[8,64,256]{2,1,0:T(8,128)(2,1)S(1)}, u32[]{:S(2)}, u32[]{:S(2)}) collective-permute-start(bf16[8,64,256]{2,1,0:T(8,128)(2,1)S(1)} %get-tuple-element.12.rest_0_), channel_id=1, source_target_pairs={{0,56},{8,0},{16,8},{24,16},{32,24},{40,32},{48,40},{56,48},{1,57}... | collective-permute-start | bytes 786440 | tf_op jit(solution)/shard_map/ppermute | solution.py:27
  112.2 2.6 %collective-permute-done.5.rest_2_ = bf16[8,64,256]{2,1,0:T(8,128)(2,1)S(1)} collective-permute-done((bf16[8,64,256]{2,1,0:T(8,128)(2,1)S(1)}, bf16[8,64,256]{2,1,0:T(8,128)(2,1)S(1)}, u32[]{:S(2)}, u32[]{:S(2)}) %collective-permute-start.5) | collective-permute-done | bytes 262176 | tf_op jit(solution)/shard_map/ppermute | solution.py:27
  114.8 2.8 %collective-permute-start.6 = (bf16[8,64,256]{2,1,0:T(8,128)(2,1)S(1)}, bf16[8,64,256]{2,1,0:T(8,128)(2,1)S(1)}, u32[]{:S(2)}, u32[]{:S(2)}) collective-permute-start(bf16[8,64,256]{2,1,0:T(8,128)(2,1)S(1)} %collective-permute-done.5.rest_2_), channel_id=1, source_target_pairs={{0,8},{8,16},{16,24},{24,32},{32,40},{40,48},{48,56},{56,0},{1,9},... | collective-permute-start | bytes 786440 | tf_op jit(solution)/shard_map/ppermute | solution.py:27
  117.6 0.3 collective-permute-done.8.rest_7_
  117.9 4.2 %collective-permute-start.9 = (bf16[8,64,256]{2,1,0:T(8,128)(2,1)S(1)}, bf16[8,64,256]{2,1,0:T(8,128)(2,1)S(1)}, u32[]{:S(2)}, u32[]{:S(2)}) collective-permute-start(bf16[8,64,256]{2,1,0:T(8,128)(2,1)S(1)} %collective-permute-done.8.rest_7_), channel_id=1, source_target_pairs={{0,56},{8,0},{16,8},{24,16},{32,24},{40,32},{48,40},{56,48},{1,57}... | collective-permute-start | bytes 786440 | tf_op jit(solution)/shard_map/ppermute | solution.py:27
  122.1 3.1 %collective-permute-done.6.rest_3_ = bf16[8,64,256]{2,1,0:T(8,128)(2,1)S(1)} collective-permute-done((bf16[8,64,256]{2,1,0:T(8,128)(2,1)S(1)}, bf16[8,64,256]{2,1,0:T(8,128)(2,1)S(1)}, u32[]{:S(2)}, u32[]{:S(2)}) %collective-permute-start.6) | collective-permute-done | bytes 262176 | tf_op jit(solution)/shard_map/ppermute | solution.py:27
  125.2 2.2 %collective-permute-start.7 = (bf16[8,64,256]{2,1,0:T(8,128)(2,1)S(1)}, bf16[8,64,256]{2,1,0:T(8,128)(2,1)S(1)}, u32[]{:S(2)}, u32[]{:S(2)}) collective-permute-start(bf16[8,64,256]{2,1,0:T(8,128)(2,1)S(1)} %collective-permute-done.6.rest_3_), channel_id=1, source_target_pairs={{0,8},{8,16},{16,24},{24,32},{32,40},{40,48},{48,56},{56,0},{1,9},... | collective-permute-start | bytes 786440 | tf_op jit(solution)/shard_map/ppermute | solution.py:27
  127.4 0.8 collective-permute-done.9.rest_6_
  128.2 4.6 %collective-permute-start.10 = (bf16[8,64,256]{2,1,0:T(8,128)(2,1)S(1)}, bf16[8,64,256]{2,1,0:T(8,128)(2,1)}, u32[]{:S(2)}, u32[]{:S(2)}) collective-permute-start(bf16[8,64,256]{2,1,0:T(8,128)(2,1)S(1)} %collective-permute-done.9.rest_6_), channel_id=1, source_target_pairs={{0,56},{8,0},{16,8},{24,16},{32,24},{40,32},{48,40},{56,48},{1,57}... | collective-permute-start | bytes 786440 | tf_op jit(solution)/shard_map/ppermute | solution.py:27
  132.8 1.9 %collective-permute-done.7.rest_4_ = bf16[8,64,256]{2,1,0:T(8,128)(2,1)S(1)} collective-permute-done((bf16[8,64,256]{2,1,0:T(8,128)(2,1)S(1)}, bf16[8,64,256]{2,1,0:T(8,128)(2,1)S(1)}, u32[]{:S(2)}, u32[]{:S(2)}) %collective-permute-start.7) | collective-permute-done | bytes 262176 | tf_op jit(solution)/shard_map/ppermute | solution.py:27
  134.7 2.0 %collective-permute-done.10.rest_5_ = bf16[8,64,256]{2,1,0:T(8,128)(2,1)} collective-permute-done((bf16[8,64,256]{2,1,0:T(8,128)(2,1)S(1)}, bf16[8,64,256]{2,1,0:T(8,128)(2,1)}, u32[]{:S(2)}, u32[]{:S(2)}) %collective-permute-start.10) | collective-permute-done | bytes 262176 | tf_op jit(solution)/shard_map/ppermute | solution.py:27
  136.7 0.0 all-to-all-done.2.mine
  136.7 1.9 %collective-permute-start.11 = (bf16[4,512,512]{2,1,0:T(8,128)(2,1)S(1)}, bf16[4,512,512]{2,1,0:T(8,128)(2,1)}, u32[]{:S(2)}, u32[]{:S(2)}) collective-permute-start(bf16[4,512,512]{2,1,0:T(8,128)(2,1)S(1)} %all-to-all-done.2.mine), channel_id=1, source_target_pairs={{0,1},{1,0},{2,3},{3,2},{4,5},{5,4},{6,7},{7,6},{8,9},{9,8},{10,11... | collective-permute-start | bytes 6291464 | tf_op jit(solution)/shard_map/ppermute | solution.py:27
  138.6 4.6 %reduce-scatter.2.cloned.1.call-done = bf16[536,256]{1,0:T(8,128)(2,1)} async-done(((bf16[4288,256]{1,0:T(8,128)(2,1)}), bf16[536,256]{1,0:T(8,128)(2,1)}) %reduce-scatter.2.cloned.1.call-update) | async-done | bytes 274448 | tf_op jit(solution)/shard_map/reduce_scatter | solution.py:152
  143.2 1.0 slice.46
  144.2 0.7 convert_reduce_fusion.1
  144.9 0.7 pad_maximum_fusion.1
  145.7 6.7 %all-to-all-start.3 = ((bf16[8,72,256]{2,1,0:T(8,128)(2,1)}), bf16[8,72,256]{2,1,0:T(8,128)(2,1)S(1)}, u32[]{:S(2)}, u32[]{:S(2)}) async-start(bf16[8,72,256]{2,1,0:T(8,128)(2,1)} %pad_maximum_fusion.1), calls=%async_computation.4 | async-start | bytes 589824 | tf_op jit(solution)/shard_map/all_to_all | solution.py:17
  152.4 0.0 collective-permute-done.11.theirs
  152.4 0.0 copy-done.8
  152.4 4.9 %shard_map.95 = bf16[512,256]{1,0:T(8,128)(2,1)} custom-call(s32[2]{0:T(128)} %pad_add_fusion.place, bf16[4,512,512]{2,1,0:T(8,128)(2,1)} %copy-done.1, bf16[4,512,512]{2,1,0:T(8,128)(2,1)} %collective-permute-done.11.theirs, bf16[8,64,256]{2,1,0:T(8,128)(2,1)} %copy-done.4, bf16[8,64,256]{2,1,0:T(8,128)(2,1)} %copy-done.7, bf16[8,64,256]{2,1,0:T(8,128)(2,1)} %copy-done.8, ...), custom_call_target="tpu_custom_call" | custom-call | tf_op jit(solution)/shard_map/pallas_call | solution.py:102
  157.3 5.9 %all-to-all-done.3 = bf16[8,72,256]{2,1,0:T(8,128)(2,1)S(1)} async-done(((bf16[8,72,256]{2,1,0:T(8,128)(2,1)}), bf16[8,72,256]{2,1,0:T(8,128)(2,1)S(1)}, u32[]{:S(2)}, u32[]{:S(2)}) %all-to-all-start.3) | async-done | bytes 294944 | tf_op jit(solution)/shard_map/all_to_all | solution.py:17
  163.3 3.4 %collective-permute-start.12 = (f32[64,256]{1,0:T(8,128)S(1)}, f32[64,256]{1,0:T(8,128)S(1)}, u32[]{:S(2)}, u32[]{:S(2)}) collective-permute-start(f32[64,256]{1,0:T(8,128)S(1)} %slice.48), channel_id=1, source_target_pairs={{0,0},{1,64},{2,128},{3,192},{4,256},{5,320},{6,384},{7,448},{64,1... | collective-permute-start | bytes 196616 | tf_op jit(solution)/shard_map/ppermute | solution.py:172
  166.7 0.6 slice_reduce_fusion
  167.3 6.6 %collective-permute-done.12 = f32[64,256]{1,0:T(8,128)S(1)} collective-permute-done((f32[64,256]{1,0:T(8,128)S(1)}, f32[64,256]{1,0:T(8,128)S(1)}, u32[]{:S(2)}, u32[]{:S(2)}) %collective-permute-start.12) | collective-permute-done | bytes 65568 | tf_op jit(solution)/shard_map/ppermute | solution.py:172
  173.9 0.6 copy.11
  (40 shorter events, 0.2 us)
Async XLA Ops:
  7.2 28.5 %copy-start.3 = (bf16[512,256]{1,0:T(8,128)(2,1)S(1)}, bf16[512,256]{1,0:T(8,128)(2,1)}, u32[]{:S(2)}) copy-start(bf16[512,256]{1,0:T(8,128)(2,1)} %param.13) | copy-start | bytes 786436
  7.2 28.5 %copy-start.13 = (f32[256]{0:T(256)S(1)}, f32[256]{0:T(256)}, u32[]{:S(2)}) copy-start(f32[256]{0:T(256)} %param.10) | copy-start | bytes 3076
  7.2 28.5 %copy-start.2 = (bf16[512,256]{1,0:T(8,128)(2,1)S(1)}, bf16[512,256]{1,0:T(8,128)(2,1)}, u32[]{:S(2)}) copy-start(bf16[512,256]{1,0:T(8,128)(2,1)} %param.9) | copy-start | bytes 786436
  7.2 28.9 %copy-start.6 = (bf16[512,256]{1,0:T(8,128)(2,1)S(1)}, bf16[512,256]{1,0:T(8,128)(2,1)}, u32[]{:S(2)}) copy-start(bf16[512,256]{1,0:T(8,128)(2,1)} %param.7) | copy-start | bytes 786436
  8.6 14.6 %collective-permute-start = (f32[2,512]{1,0:T(2,128)S(1)}, f32[2,512]{1,0:T(2,128)S(1)}, u32[]{:S(2)}, u32[]{:S(2)}) collective-permute-start(f32[2,512]{1,0:T(2,128)S(1)} %pad_maximum_fusion.3), channel_id=1, source_target_pairs={{0,1},{1,0},{2,3},{3,2},{4,5},{5,4},{6,7},{7,6},{8,9},{9,8},{10,11... | collective-permute-start | bytes 12296 | tf_op jit(solution)/shard_map/ppermute | solution.py:39
  12.8 28.5 %all-to-all-start.1 = ((bf16[8,128,256]{2,1,0:T(8,128)(2,1)}), bf16[8,128,256]{2,1,0:T(8,128)(2,1)S(1)}, u32[]{:S(2)}, u32[]{:S(2)}) async-start(bf16[8,128,256]{2,1,0:T(8,128)(2,1)} %broadcast_in_dim.9), calls=%async_computation.1 | async-start | bytes 1048576 | tf_op jit(solution)/shard_map/all_to_all | solution.py:17
  23.2 5.5 %collective-permute-start.1 = (f32[2,512]{1,0:T(2,128)S(1)}, f32[2,512]{1,0:T(2,128)S(1)}, u32[]{:S(2)}, u32[]{:S(2)}) collective-permute-start(f32[2,512]{1,0:T(2,128)S(1)} %fusion.19), channel_id=1, source_target_pairs={{0,2},{2,0},{4,6},{6,4},{1,3},{3,1},{5,7},{7,5},{8,10},{10,8},{12,... | collective-permute-start | bytes 12296 | tf_op jit(solution)/shard_map/ppermute | solution.py:39
  28.7 7.0 %collective-permute-start.2 = (f32[2,512]{1,0:T(2,128)S(1)}, f32[2,512]{1,0:T(2,128)S(1)}, u32[]{:S(2)}, u32[]{:S(2)}) collective-permute-start(f32[2,512]{1,0:T(2,128)S(1)} %fusion.23), channel_id=1, source_target_pairs={{0,4},{2,6},{4,0},{6,2},{1,5},{3,7},{5,1},{7,3},{8,12},{10,14},{12... | collective-permute-start | bytes 12296 | tf_op jit(solution)/shard_map/ppermute | solution.py:39
  42.8 29.2 %all-to-all-start = ((bf16[4,2,512,256]{3,2,1,0:T(8,128)(2,1)}), bf16[4,2,512,256]{3,2,1,0:T(8,128)(2,1)S(1)}, u32[]{:S(2)}, u32[]{:S(2)}) async-start(bf16[4,2,512,256]{3,2,1,0:T(8,128)(2,1)} %broadcast_in_dim.8), calls=%async_computation | async-start | bytes 4194304 | tf_op jit(solution)/shard_map/all_to_all | solution.py:17
  47.6 43.3 %all-gather.2.cloned.1.call-start = ((), (), s32[]{:S(2)}) async-start(), calls=%async_computation.5 | async-start | bytes 2359296 | tf_op jit(solution)/shard_map/all_gather | solution.py:131
  48.3 59.9 %copy-start.4 = (bf16[8,64,256]{2,1,0:T(8,128)(2,1)}, bf16[8,64,256]{2,1,0:T(8,128)(2,1)S(1)}, u32[]{:S(2)}) copy-start(bf16[8,64,256]{2,1,0:T(8,128)(2,1)S(1)} %get-tuple-element.12.rest_0_) | copy-start | bytes 786436
  48.4 94.8 %reduce-scatter.2.cloned.1.call-start = ((), (), s32[]{:S(2)}) async-start(), calls=%async_computation.6 | async-start | bytes 2469888 | tf_op jit(solution)/shard_map/reduce_scatter | solution.py:152
  48.4 11.3 %collective-permute-start.3 = (bf16[8,64,256]{2,1,0:T(8,128)(2,1)S(1)}, bf16[8,64,256]{2,1,0:T(8,128)(2,1)S(1)}, u32[]{:S(2)}, u32[]{:S(2)}) collective-permute-start(bf16[8,64,256]{2,1,0:T(8,128)(2,1)S(1)} %get-tuple-element.12.rest_0_), channel_id=1, source_target_pairs={{0,8},{8,16},{16,24},{24,32},{32,40},{40,48},{48,56},{56,0},{1,9},... | collective-permute-start | bytes 786440 | tf_op jit(solution)/shard_map/ppermute | solution.py:27
  59.7 45.4 %copy-start.7 = (bf16[8,64,256]{2,1,0:T(8,128)(2,1)}, bf16[8,64,256]{2,1,0:T(8,128)(2,1)S(1)}, u32[]{:S(2)}) copy-start(bf16[8,64,256]{2,1,0:T(8,128)(2,1)S(1)} %collective-permute-done.3.rest_1_) | copy-start | bytes 786436
  72.1 18.8 %copy-start = (bf16[4,2,512,256]{3,2,1,0:T(8,128)(2,1)}, bf16[4,2,512,256]{3,2,1,0:T(8,128)(2,1)S(1)}, u32[]{:S(2)}) copy-start(bf16[4,2,512,256]{3,2,1,0:T(8,128)(2,1)S(1)} %all-to-all-done.mine) | copy-start | bytes 6291460
  72.1 6.2 %collective-permute-start.4 = (bf16[4,2,512,256]{3,2,1,0:T(8,128)(2,1)S(1)}, bf16[4,2,512,256]{3,2,1,0:T(8,128)(2,1)}, u32[]{:S(2)}, u32[]{:S(2)}) collective-permute-start(bf16[4,2,512,256]{3,2,1,0:T(8,128)(2,1)S(1)} %all-to-all-done.mine), channel_id=1, source_target_pairs={{0,1},{1,0},{2,3},{3,2},{4,5},{5,4},{6,7},{7,6},{8,9},{9,8},{10,11... | collective-permute-start | bytes 6291464 | tf_op jit(solution)/shard_map/ppermute | solution.py:27
  97.9 1.0 copy-start.5
  100.4 36.3 %all-to-all-start.2 = ((bf16[4,512,512]{2,1,0:T(8,128)(2,1)}), bf16[4,512,512]{2,1,0:T(8,128)(2,1)S(1)}, u32[]{:S(2)}, u32[]{:S(2)}) async-start(bf16[4,512,512]{2,1,0:T(8,128)(2,1)} %broadcast_in_dim.10), calls=%async_computation.2 | async-start | bytes 4194304 | tf_op jit(solution)/shard_map/all_to_all | solution.py:17
  105.1 9.7 %collective-permute-start.5 = (bf16[8,64,256]{2,1,0:T(8,128)(2,1)S(1)}, bf16[8,64,256]{2,1,0:T(8,128)(2,1)S(1)}, u32[]{:S(2)}, u32[]{:S(2)}) collective-permute-start(bf16[8,64,256]{2,1,0:T(8,128)(2,1)S(1)} %collective-permute-done.3.rest_1_), channel_id=1, source_target_pairs={{0,8},{8,16},{16,24},{24,32},{32,40},{40,48},{48,56},{56,0},{1,9},... | collective-permute-start | bytes 786440 | tf_op jit(solution)/shard_map/ppermute | solution.py:27
  108.2 9.6 %collective-permute-start.8 = (bf16[8,64,256]{2,1,0:T(8,128)(2,1)S(1)}, bf16[8,64,256]{2,1,0:T(8,128)(2,1)S(1)}, u32[]{:S(2)}, u32[]{:S(2)}) collective-permute-start(bf16[8,64,256]{2,1,0:T(8,128)(2,1)S(1)} %get-tuple-element.12.rest_0_), channel_id=1, source_target_pairs={{0,56},{8,0},{16,8},{24,16},{32,24},{40,32},{48,40},{56,48},{1,57}... | collective-permute-start | bytes 786440 | tf_op jit(solution)/shard_map/ppermute | solution.py:27
  114.8 37.6 %copy-start.8 = (bf16[8,64,256]{2,1,0:T(8,128)(2,1)}, bf16[8,64,256]{2,1,0:T(8,128)(2,1)S(1)}, u32[]{:S(2)}) copy-start(bf16[8,64,256]{2,1,0:T(8,128)(2,1)S(1)} %collective-permute-done.5.rest_2_) | copy-start | bytes 786436
  114.8 10.4 %collective-permute-start.6 = (bf16[8,64,256]{2,1,0:T(8,128)(2,1)S(1)}, bf16[8,64,256]{2,1,0:T(8,128)(2,1)S(1)}, u32[]{:S(2)}, u32[]{:S(2)}) collective-permute-start(bf16[8,64,256]{2,1,0:T(8,128)(2,1)S(1)} %collective-permute-done.5.rest_2_), channel_id=1, source_target_pairs={{0,8},{8,16},{16,24},{24,32},{32,40},{40,48},{48,56},{56,0},{1,9},... | collective-permute-start | bytes 786440 | tf_op jit(solution)/shard_map/ppermute | solution.py:27
  117.9 34.5 %copy-start.9 = (bf16[8,64,256]{2,1,0:T(8,128)(2,1)}, bf16[8,64,256]{2,1,0:T(8,128)(2,1)S(1)}, u32[]{:S(2)}) copy-start(bf16[8,64,256]{2,1,0:T(8,128)(2,1)S(1)} %collective-permute-done.8.rest_7_) | copy-start | bytes 786436
  117.9 10.3 %collective-permute-start.9 = (bf16[8,64,256]{2,1,0:T(8,128)(2,1)S(1)}, bf16[8,64,256]{2,1,0:T(8,128)(2,1)S(1)}, u32[]{:S(2)}, u32[]{:S(2)}) collective-permute-start(bf16[8,64,256]{2,1,0:T(8,128)(2,1)S(1)} %collective-permute-done.8.rest_7_), channel_id=1, source_target_pairs={{0,56},{8,0},{16,8},{24,16},{32,24},{40,32},{48,40},{56,48},{1,57}... | collective-permute-start | bytes 786440 | tf_op jit(solution)/shard_map/ppermute | solution.py:27
  125.2 27.2 %copy-start.10 = (bf16[8,64,256]{2,1,0:T(8,128)(2,1)}, bf16[8,64,256]{2,1,0:T(8,128)(2,1)S(1)}, u32[]{:S(2)}) copy-start(bf16[8,64,256]{2,1,0:T(8,128)(2,1)S(1)} %collective-permute-done.6.rest_3_) | copy-start | bytes 786436
  125.2 9.5 %collective-permute-start.7 = (bf16[8,64,256]{2,1,0:T(8,128)(2,1)S(1)}, bf16[8,64,256]{2,1,0:T(8,128)(2,1)S(1)}, u32[]{:S(2)}, u32[]{:S(2)}) collective-permute-start(bf16[8,64,256]{2,1,0:T(8,128)(2,1)S(1)} %collective-permute-done.6.rest_3_), channel_id=1, source_target_pairs={{0,8},{8,16},{16,24},{24,32},{32,40},{40,48},{48,56},{56,0},{1,9},... | collective-permute-start | bytes 786440 | tf_op jit(solution)/shard_map/ppermute | solution.py:27
  128.2 24.2 %copy-start.11 = (bf16[8,64,256]{2,1,0:T(8,128)(2,1)}, bf16[8,64,256]{2,1,0:T(8,128)(2,1)S(1)}, u32[]{:S(2)}) copy-start(bf16[8,64,256]{2,1,0:T(8,128)(2,1)S(1)} %collective-permute-done.9.rest_6_) | copy-start | bytes 786436
  128.2 8.4 %collective-permute-start.10 = (bf16[8,64,256]{2,1,0:T(8,128)(2,1)S(1)}, bf16[8,64,256]{2,1,0:T(8,128)(2,1)}, u32[]{:S(2)}, u32[]{:S(2)}) collective-permute-start(bf16[8,64,256]{2,1,0:T(8,128)(2,1)S(1)} %collective-permute-done.9.rest_6_), channel_id=1, source_target_pairs={{0,56},{8,0},{16,8},{24,16},{32,24},{40,32},{48,40},{56,48},{1,57}... | collective-permute-start | bytes 786440 | tf_op jit(solution)/shard_map/ppermute | solution.py:27
  134.7 11.0 %copy-start.12 = (bf16[8,64,256]{2,1,0:T(8,128)(2,1)}, bf16[8,64,256]{2,1,0:T(8,128)(2,1)S(1)}, u32[]{:S(2)}) copy-start(bf16[8,64,256]{2,1,0:T(8,128)(2,1)S(1)} %collective-permute-done.7.rest_4_) | copy-start | bytes 786436
  136.7 15.7 %copy-start.1 = (bf16[4,512,512]{2,1,0:T(8,128)(2,1)}, bf16[4,512,512]{2,1,0:T(8,128)(2,1)S(1)}, u32[]{:S(2)}) copy-start(bf16[4,512,512]{2,1,0:T(8,128)(2,1)S(1)} %all-to-all-done.2.mine) | copy-start | bytes 6291460
  136.7 15.7 %collective-permute-start.11 = (bf16[4,512,512]{2,1,0:T(8,128)(2,1)S(1)}, bf16[4,512,512]{2,1,0:T(8,128)(2,1)}, u32[]{:S(2)}, u32[]{:S(2)}) collective-permute-start(bf16[4,512,512]{2,1,0:T(8,128)(2,1)S(1)} %all-to-all-done.2.mine), channel_id=1, source_target_pairs={{0,1},{1,0},{2,3},{3,2},{4,5},{5,4},{6,7},{7,6},{8,9},{9,8},{10,11... | collective-permute-start | bytes 6291464 | tf_op jit(solution)/shard_map/ppermute | solution.py:27
  145.7 17.5 %all-to-all-start.3 = ((bf16[8,72,256]{2,1,0:T(8,128)(2,1)}), bf16[8,72,256]{2,1,0:T(8,128)(2,1)S(1)}, u32[]{:S(2)}, u32[]{:S(2)}) async-start(bf16[8,72,256]{2,1,0:T(8,128)(2,1)} %pad_maximum_fusion.1), calls=%async_computation.4 | async-start | bytes 589824 | tf_op jit(solution)/shard_map/all_to_all | solution.py:17
  163.3 10.6 %collective-permute-start.12 = (f32[64,256]{1,0:T(8,128)S(1)}, f32[64,256]{1,0:T(8,128)S(1)}, u32[]{:S(2)}, u32[]{:S(2)}) collective-permute-start(f32[64,256]{1,0:T(8,128)S(1)} %slice.48), channel_id=1, source_target_pairs={{0,0},{1,64},{2,128},{3,192},{4,256},{5,320},{6,384},{7,448},{64,1... | collective-permute-start | bytes 196616 | tf_op jit(solution)/shard_map/ppermute | solution.py:172
Sparse Core Ops, SparseCore 0:
  51.0 39.7 all-gather.1
  98.0 45.1 reduce-scatter.1

commit v10 on v9

--- a/solution.py
+++ b/solution.py
@@ -47,6 +47,14 @@
 
 def summed(parts):
     return jnp.sum(parts.astype(f32), axis=0)
+
+
+def spread_kernel(wd, wu, out):
+    rows, half = wd.shape[0], wd.shape[1] // 2
+    for k in range(out.shape[0]):
+        out[k, :rows] = wd[:, :half]
+        out[k, rows : 2 * rows] = wd[:, half:]
+        out[k, 2 * rows :] = wu[...]
 
 
 def in_three(value):
@@ -124,8 +132,13 @@
     sums = jnp.stack([jnp.sum(normed * normed, axis=1), jnp.sum(weighted * normed, axis=1)])
 
     wd = w_down.T
-    both = jnp.concatenate([wd[:, :half], wd[:, half:], w_up.T], axis=0)
-    both = gather_directly(both, "z")
+    rows = 2 * wd.shape[0] + w_up.shape[1]
+    both = pl.pallas_call(
+        spread_kernel,
+        out_shape=jax.ShapeDtypeStruct((nz, rows, feats), bf16),
+        name="spread_kernel",
+    )(wd, w_up.T)
+    both = exchange(both, "z")
     wd_rows = 2 * wd.shape[0]
     wd = both[:, :wd_rows].reshape(nz * wd_rows, half)
     wd = lax.all_gather(wd, "y", axis=0, tiled=True)

time: 184 us -> 184 us (level)
    broadcast_in_dim x3 -> x2, local copies, waits for them, and re-layouts: 3.82 us -> 2.95 us  [gather_directly(): return exchange(jnp.broadcast_to(value[None], (n, *value.shape)), axis)]
  transfers between devices with their start and end apart: 19 -> 19, of which waited for: 16 -> 16; matrix products, arithmetic and copies ran while one was open for 5% -> 4% of each run, Pallas kernels for 3% -> 4%
where the time goes in v10:
time: 184 us; the launch traced here: 181 us
  waiting for transfers between devices  75.1 us (41%)
  starting transfers between devices  66 us (36%)
  between operations  14.3 us (8%)
  Pallas kernels  13.5 us (7%)
  local copies, waits for them, and re-layouts  6.55 us (4%)
  other arithmetic  5.2 us (3%)
    ppermute x9, starting transfers between devices, shifted(): return lax.ppermute(value, axis, [(i, (i + by) % n) for i in range(n)])  28.1 us
    all_to_all x4, starting transfers between devices, exchange(): return lax.all_to_all(chunks, axis, 0, 0, tiled=True)  26.6 us
    all_to_all x4, waiting for transfers between devices, exchange(): return lax.all_to_all(chunks, axis, 0, 0, tiled=True)  23.5 us
    ppermute x9, waiting for transfers between devices, shifted(): return lax.ppermute(value, axis, [(i, (i + by) % n) for i in range(n)])  21.3 us
    all_gather x1, waiting for transfers between devices, one_device(): wd = lax.all_gather(wd, 'y', axis=0, tiled=True)  12.6 us
    pallas_call x2, Pallas kernels, run(): pl.pallas_call(kernel, out_shape=[jax.ShapeDtypeStruct(shape, bf16) for s...  11.8 us
    ppermute x3, starting transfers between devices, pairwise(): value = value + lax.ppermute(value, axis, [(i, i ^ step) for i in range(n)])  7.97 us
    ppermute x1, waiting for transfers between devices, one_device(): grad_up = lax.ppermute(g[:rows], ('z', 'x', 'c'), swap).T  6.69 us
  transfers between devices with their start and end apart: 19, of which 16 were waited for; matrix products, arithmetic and copies ran while one was open for 4% of the time, Pallas kernels for 4%

profile of v10, /device:TPU:6, one launch (start us, length us, event | category | flops | bytes accessed | tf_op | source)
XLA Modules:
  0.0 180.6 jit_solution(3825738758787603305)
XLA Ops:
  7.2 0.0 copy-start.3
  7.2 0.0 copy-start.13
  7.2 0.0 copy-start.2
  7.2 0.0 copy-start.6
  7.2 1.3 fusion.3
  8.6 1.9 %collective-permute-start = (f32[2,512]{1,0:T(2,128)S(1)}, f32[2,512]{1,0:T(2,128)S(1)}, u32[]{:S(2)}, u32[]{:S(2)}) collective-permute-start(f32[2,512]{1,0:T(2,128)S(1)} %pad_maximum_fusion.2), channel_id=1, source_target_pairs={{0,1},{1,0},{2,3},{3,2},{4,5},{5,4},{6,7},{7,6},{8,9},{9,8},{10,11... | collective-permute-start | bytes 12296 | tf_op jit(solution)/shard_map/ppermute | solution.py:39
  10.5 1.6 spread_kernel.1
  12.1 10.3 %all-to-all-start.1 = ((bf16[8,128,256]{2,1,0:T(8,128)(2,1)}), bf16[8,128,256]{2,1,0:T(8,128)(2,1)S(1)}, u32[]{:S(2)}, u32[]{:S(2)}) async-start(bf16[8,128,256]{2,1,0:T(8,128)(2,1)} %spread_kernel.1), calls=%async_computation.1 | async-start | bytes 1048576 | tf_op jit(solution)/shard_map/all_to_all | solution.py:17
  22.4 0.0 collective-permute-done
  22.4 2.7 %collective-permute-start.1 = (f32[2,512]{1,0:T(2,128)S(1)}, f32[2,512]{1,0:T(2,128)S(1)}, u32[]{:S(2)}, u32[]{:S(2)}) collective-permute-start(f32[2,512]{1,0:T(2,128)S(1)} %fusion.19), channel_id=1, source_target_pairs={{0,2},{2,0},{4,6},{6,4},{1,3},{3,1},{5,7},{7,5},{8,10},{10,8},{12,... | collective-permute-start | bytes 12296 | tf_op jit(solution)/shard_map/ppermute | solution.py:39
  25.2 2.8 %collective-permute-done.1 = f32[2,512]{1,0:T(2,128)S(1)} collective-permute-done((f32[2,512]{1,0:T(2,128)S(1)}, f32[2,512]{1,0:T(2,128)S(1)}, u32[]{:S(2)}, u32[]{:S(2)}) %collective-permute-start.1) | collective-permute-done | bytes 4128 | tf_op jit(solution)/shard_map/ppermute | solution.py:39
  28.0 3.3 %collective-permute-start.2 = (f32[2,512]{1,0:T(2,128)S(1)}, f32[2,512]{1,0:T(2,128)S(1)}, u32[]{:S(2)}, u32[]{:S(2)}) collective-permute-start(f32[2,512]{1,0:T(2,128)S(1)} %fusion.22), channel_id=1, source_target_pairs={{0,4},{2,6},{4,0},{6,2},{1,5},{3,7},{5,1},{7,3},{8,12},{10,14},{12... | collective-permute-start | bytes 12296 | tf_op jit(solution)/shard_map/ppermute | solution.py:39
  31.3 3.7 %collective-permute-done.2 = f32[2,512]{1,0:T(2,128)S(1)} collective-permute-done((f32[2,512]{1,0:T(2,128)S(1)}, f32[2,512]{1,0:T(2,128)S(1)}, u32[]{:S(2)}, u32[]{:S(2)}) %collective-permute-start.2) | collective-permute-done | bytes 4128 | tf_op jit(solution)/shard_map/ppermute | solution.py:39
  35.0 0.0 copy-done.3
  35.0 0.3 fusion.9
  35.3 0.0 copy-done.6
  35.3 0.1 pad_maximum_fusion
  35.4 5.2 %all-to-all-done.1 = bf16[8,128,256]{2,1,0:T(8,128)(2,1)S(1)} async-done(((bf16[8,128,256]{2,1,0:T(8,128)(2,1)}), bf16[8,128,256]{2,1,0:T(8,128)(2,1)S(1)}, u32[]{:S(2)}, u32[]{:S(2)}) %all-to-all-start.1) | async-done | bytes 524320 | tf_op jit(solution)/shard_map/all_to_all | solution.py:17
  40.6 1.5 broadcast_in_dim.6
  42.1 4.8 %all-to-all-start = ((bf16[4,2,512,256]{3,2,1,0:T(8,128)(2,1)}), bf16[4,2,512,256]{3,2,1,0:T(8,128)(2,1)S(1)}, u32[]{:S(2)}, u32[]{:S(2)}) async-start(bf16[4,2,512,256]{3,2,1,0:T(8,128)(2,1)} %broadcast_in_dim.6), calls=%async_computation | async-start | bytes 4194304 | tf_op jit(solution)/shard_map/all_to_all | solution.py:17
  46.9 0.7 fusion.20
  47.6 0.0 all-gather.2.cloned.1.call-update
  47.6 0.0 reduce-scatter.2.cloned.1.call-start
  47.7 3.5 %collective-permute-start.3 = (bf16[8,64,256]{2,1,0:T(8,128)(2,1)S(1)}, bf16[8,64,256]{2,1,0:T(8,128)(2,1)S(1)}, u32[]{:S(2)}, u32[]{:S(2)}) collective-permute-start(bf16[8,64,256]{2,1,0:T(8,128)(2,1)S(1)} %get-tuple-element.12.rest_0_), channel_id=1, source_target_pairs={{0,8},{8,16},{16,24},{24,32},{32,40},{40,48},{48,56},{56,0},{1,9},... | collective-permute-start | bytes 786440 | tf_op jit(solution)/shard_map/ppermute | solution.py:27
  51.2 7.8 %collective-permute-done.3.rest_1_ = bf16[8,64,256]{2,1,0:T(8,128)(2,1)S(1)} collective-permute-done((bf16[8,64,256]{2,1,0:T(8,128)(2,1)S(1)}, bf16[8,64,256]{2,1,0:T(8,128)(2,1)S(1)}, u32[]{:S(2)}, u32[]{:S(2)}) %collective-permute-start.3) | collective-permute-done | bytes 262176 | tf_op jit(solution)/shard_map/ppermute | solution.py:27
  59.0 12.3 %all-to-all-done.mine = bf16[4,2,512,256]{3,2,1,0:T(8,128)(2,1)S(1)} async-done(((bf16[4,2,512,256]{3,2,1,0:T(8,128)(2,1)}), bf16[4,2,512,256]{3,2,1,0:T(8,128)(2,1)S(1)}, u32[]{:S(2)}, u32[]{:S(2)}) %all-to-all-start) | async-done | bytes 2097184 | tf_op jit(solution)/shard_map/all_to_all | solution.py:17
  71.3 1.9 %collective-permute-start.4 = (bf16[4,2,512,256]{3,2,1,0:T(8,128)(2,1)S(1)}, bf16[4,2,512,256]{3,2,1,0:T(8,128)(2,1)}, u32[]{:S(2)}, u32[]{:S(2)}) collective-permute-start(bf16[4,2,512,256]{3,2,1,0:T(8,128)(2,1)S(1)} %all-to-all-done.mine), channel_id=1, source_target_pairs={{0,1},{1,0},{2,3},{3,2},{4,5},{5,4},{6,7},{7,6},{8,9},{9,8},{10,11... | collective-permute-start | bytes 6291464 | tf_op jit(solution)/shard_map/ppermute | solution.py:27
  73.3 0.1 mul.94
  73.3 0.1 mul.95
  73.4 0.7 pad_add_fusion.place
  74.1 0.7 multiply_convert_fusion.gain_rows
  74.8 2.7 %collective-permute-done.4.theirs = bf16[4,2,512,256]{3,2,1,0:T(8,128)(2,1)} collective-permute-done((bf16[4,2,512,256]{3,2,1,0:T(8,128)(2,1)S(1)}, bf16[4,2,512,256]{3,2,1,0:T(8,128)(2,1)}, u32[]{:S(2)}, u32[]{:S(2)}) %collective-permute-start.4) | collective-permute-done | bytes 2097184 | tf_op jit(solution)/shard_map/ppermute | solution.py:27
  77.5 12.6 %all-gather.2.cloned.1.call-done = bf16[4096,256]{1,0:T(8,128)(2,1)} async-done(((bf16[512,256]{1,0:T(8,128)(2,1)}), bf16[4096,256]{1,0:T(8,128)(2,1)}) %all-gather.2.cloned.1.call-update) | async-done | bytes 2097168 | tf_op jit(solution)/shard_map/all_gather | solution.py:144
  90.1 7.0 %shard_map.94 = (bf16[512,512]{1,0:T(8,128)(2,1)}, bf16[8,536,256]{2,1,0:T(8,128)(2,1)}) custom-call(s32[2]{0:T(128)} %pad_add_fusion.place, bf16[4,2,512,256]{3,2,1,0:T(8,128)(2,1)} %copy-done, bf16[4,2,512,256]{3,2,1,0:T(8,128)(2,1)} %collective-permute-done.4.theirs, bf16[8,8,2,32,256]{4,3,2,1,0:T(8,128)(2,1)} %bitcast.19, bf16[512,512]{1,0:T(8,128)(2,1)} %hidden.1, ...), custom_call_target="tpu_custom_call" | custom-call | tf_op jit(solution)/shard_map/pallas_call | solution.py:110
  97.1 0.0 reduce-scatter.2.cloned.1.call-update
  97.1 1.0 copy-done.5
  98.2 1.5 broadcast_in_dim.7
  99.7 4.8 %all-to-all-start.2 = ((bf16[4,512,512]{2,1,0:T(8,128)(2,1)}), bf16[4,512,512]{2,1,0:T(8,128)(2,1)S(1)}, u32[]{:S(2)}, u32[]{:S(2)}) async-start(bf16[4,512,512]{2,1,0:T(8,128)(2,1)} %broadcast_in_dim.7), calls=%async_computation.2 | async-start | bytes 4194304 | tf_op jit(solution)/shard_map/all_to_all | solution.py:17
  104.4 3.0 %collective-permute-start.5 = (bf16[8,64,256]{2,1,0:T(8,128)(2,1)S(1)}, bf16[8,64,256]{2,1,0:T(8,128)(2,1)S(1)}, u32[]{:S(2)}, u32[]{:S(2)}) collective-permute-start(bf16[8,64,256]{2,1,0:T(8,128)(2,1)S(1)} %collective-permute-done.3.rest_1_), channel_id=1, source_target_pairs={{0,8},{8,16},{16,24},{24,32},{32,40},{40,48},{48,56},{56,0},{1,9},... | collective-permute-start | bytes 786440 | tf_op jit(solution)/shard_map/ppermute | solution.py:27
  107.5 4.0 %collective-permute-start.8 = (bf16[8,64,256]{2,1,0:T(8,128)(2,1)S(1)}, bf16[8,64,256]{2,1,0:T(8,128)(2,1)S(1)}, u32[]{:S(2)}, u32[]{:S(2)}) collective-permute-start(bf16[8,64,256]{2,1,0:T(8,128)(2,1)S(1)} %get-tuple-element.12.rest_0_), channel_id=1, source_target_pairs={{0,56},{8,0},{16,8},{24,16},{32,24},{40,32},{48,40},{56,48},{1,57}... | collective-permute-start | bytes 786440 | tf_op jit(solution)/shard_map/ppermute | solution.py:27
  111.5 2.6 %collective-permute-done.5.rest_2_ = bf16[8,64,256]{2,1,0:T(8,128)(2,1)S(1)} collective-permute-done((bf16[8,64,256]{2,1,0:T(8,128)(2,1)S(1)}, bf16[8,64,256]{2,1,0:T(8,128)(2,1)S(1)}, u32[]{:S(2)}, u32[]{:S(2)}) %collective-permute-start.5) | collective-permute-done | bytes 262176 | tf_op jit(solution)/shard_map/ppermute | solution.py:27
  114.2 2.7 %collective-permute-start.6 = (bf16[8,64,256]{2,1,0:T(8,128)(2,1)S(1)}, bf16[8,64,256]{2,1,0:T(8,128)(2,1)S(1)}, u32[]{:S(2)}, u32[]{:S(2)}) collective-permute-start(bf16[8,64,256]{2,1,0:T(8,128)(2,1)S(1)} %collective-permute-done.5.rest_2_), channel_id=1, source_target_pairs={{0,8},{8,16},{16,24},{24,32},{32,40},{40,48},{48,56},{56,0},{1,9},... | collective-permute-start | bytes 786440 | tf_op jit(solution)/shard_map/ppermute | solution.py:27
  116.8 0.3 collective-permute-done.8.rest_7_
  117.1 4.3 %collective-permute-start.9 = (bf16[8,64,256]{2,1,0:T(8,128)(2,1)S(1)}, bf16[8,64,256]{2,1,0:T(8,128)(2,1)S(1)}, u32[]{:S(2)}, u32[]{:S(2)}) collective-permute-start(bf16[8,64,256]{2,1,0:T(8,128)(2,1)S(1)} %collective-permute-done.8.rest_7_), channel_id=1, source_target_pairs={{0,56},{8,0},{16,8},{24,16},{32,24},{40,32},{48,40},{56,48},{1,57}... | collective-permute-start | bytes 786440 | tf_op jit(solution)/shard_map/ppermute | solution.py:27
  121.5 3.1 %collective-permute-done.6.rest_3_ = bf16[8,64,256]{2,1,0:T(8,128)(2,1)S(1)} collective-permute-done((bf16[8,64,256]{2,1,0:T(8,128)(2,1)S(1)}, bf16[8,64,256]{2,1,0:T(8,128)(2,1)S(1)}, u32[]{:S(2)}, u32[]{:S(2)}) %collective-permute-start.6) | collective-permute-done | bytes 262176 | tf_op jit(solution)/shard_map/ppermute | solution.py:27
  124.6 2.0 %collective-permute-start.7 = (bf16[8,64,256]{2,1,0:T(8,128)(2,1)S(1)}, bf16[8,64,256]{2,1,0:T(8,128)(2,1)S(1)}, u32[]{:S(2)}, u32[]{:S(2)}) collective-permute-start(bf16[8,64,256]{2,1,0:T(8,128)(2,1)S(1)} %collective-permute-done.6.rest_3_), channel_id=1, source_target_pairs={{0,8},{8,16},{16,24},{24,32},{32,40},{40,48},{48,56},{56,0},{1,9},... | collective-permute-start | bytes 786440 | tf_op jit(solution)/shard_map/ppermute | solution.py:27
  126.6 0.8 collective-permute-done.9.rest_6_
  127.4 4.8 %collective-permute-start.10 = (bf16[8,64,256]{2,1,0:T(8,128)(2,1)S(1)}, bf16[8,64,256]{2,1,0:T(8,128)(2,1)}, u32[]{:S(2)}, u32[]{:S(2)}) collective-permute-start(bf16[8,64,256]{2,1,0:T(8,128)(2,1)S(1)} %collective-permute-done.9.rest_6_), channel_id=1, source_target_pairs={{0,56},{8,0},{16,8},{24,16},{32,24},{40,32},{48,40},{56,48},{1,57}... | collective-permute-start | bytes 786440 | tf_op jit(solution)/shard_map/ppermute | solution.py:27
  132.2 1.9 %collective-permute-done.7.rest_4_ = bf16[8,64,256]{2,1,0:T(8,128)(2,1)S(1)} collective-permute-done((bf16[8,64,256]{2,1,0:T(8,128)(2,1)S(1)}, bf16[8,64,256]{2,1,0:T(8,128)(2,1)S(1)}, u32[]{:S(2)}, u32[]{:S(2)}) %collective-permute-start.7) | collective-permute-done | bytes 262176 | tf_op jit(solution)/shard_map/ppermute | solution.py:27
  134.1 2.0 %collective-permute-done.10.rest_5_ = bf16[8,64,256]{2,1,0:T(8,128)(2,1)} collective-permute-done((bf16[8,64,256]{2,1,0:T(8,128)(2,1)S(1)}, bf16[8,64,256]{2,1,0:T(8,128)(2,1)}, u32[]{:S(2)}, u32[]{:S(2)}) %collective-permute-start.10) | collective-permute-done | bytes 262176 | tf_op jit(solution)/shard_map/ppermute | solution.py:27
  136.1 0.0 all-to-all-done.2.mine
  136.1 1.9 %collective-permute-start.11 = (bf16[4,512,512]{2,1,0:T(8,128)(2,1)S(1)}, bf16[4,512,512]{2,1,0:T(8,128)(2,1)}, u32[]{:S(2)}, u32[]{:S(2)}) collective-permute-start(bf16[4,512,512]{2,1,0:T(8,128)(2,1)S(1)} %all-to-all-done.2.mine), channel_id=1, source_target_pairs={{0,1},{1,0},{2,3},{3,2},{4,5},{5,4},{6,7},{7,6},{8,9},{9,8},{10,11... | collective-permute-start | bytes 6291464 | tf_op jit(solution)/shard_map/ppermute | solution.py:27
  138.0 4.5 %reduce-scatter.2.cloned.1.call-done = bf16[536,256]{1,0:T(8,128)(2,1)} async-done(((bf16[4288,256]{1,0:T(8,128)(2,1)}), bf16[536,256]{1,0:T(8,128)(2,1)}) %reduce-scatter.2.cloned.1.call-update) | async-done | bytes 274448 | tf_op jit(solution)/shard_map/reduce_scatter | solution.py:165
  142.5 1.0 slice.36
  143.5 0.7 convert_reduce_fusion.1
  144.3 0.7 pad_maximum_fusion.1
  145.0 6.7 %all-to-all-start.3 = ((bf16[8,72,256]{2,1,0:T(8,128)(2,1)}), bf16[8,72,256]{2,1,0:T(8,128)(2,1)S(1)}, u32[]{:S(2)}, u32[]{:S(2)}) async-start(bf16[8,72,256]{2,1,0:T(8,128)(2,1)} %pad_maximum_fusion.1), calls=%async_computation.4 | async-start | bytes 589824 | tf_op jit(solution)/shard_map/all_to_all | solution.py:17
  151.7 0.0 collective-permute-done.11.theirs
  151.7 4.9 %shard_map.95 = bf16[512,256]{1,0:T(8,128)(2,1)} custom-call(s32[2]{0:T(128)} %pad_add_fusion.place, bf16[4,512,512]{2,1,0:T(8,128)(2,1)} %copy-done.1, bf16[4,512,512]{2,1,0:T(8,128)(2,1)} %collective-permute-done.11.theirs, bf16[8,64,256]{2,1,0:T(8,128)(2,1)} %copy-done.4, bf16[8,64,256]{2,1,0:T(8,128)(2,1)} %copy-done.7, bf16[8,64,256]{2,1,0:T(8,128)(2,1)} %copy-done.8, ...), custom_call_target="tpu_custom_call" | custom-call | tf_op jit(solution)/shard_map/pallas_call | solution.py:110
  156.6 5.9 %all-to-all-done.3 = bf16[8,72,256]{2,1,0:T(8,128)(2,1)S(1)} async-done(((bf16[8,72,256]{2,1,0:T(8,128)(2,1)}), bf16[8,72,256]{2,1,0:T(8,128)(2,1)S(1)}, u32[]{:S(2)}, u32[]{:S(2)}) %all-to-all-start.3) | async-done | bytes 294944 | tf_op jit(solution)/shard_map/all_to_all | solution.py:17
  162.6 3.3 %collective-permute-start.12 = (f32[64,256]{1,0:T(8,128)S(1)}, f32[64,256]{1,0:T(8,128)S(1)}, u32[]{:S(2)}, u32[]{:S(2)}) collective-permute-start(f32[64,256]{1,0:T(8,128)S(1)} %slice.38), channel_id=1, source_target_pairs={{0,0},{1,64},{2,128},{3,192},{4,256},{5,320},{6,384},{7,448},{64,1... | collective-permute-start | bytes 196616 | tf_op jit(solution)/shard_map/ppermute | solution.py:185
  165.9 0.6 slice_reduce_fusion
  166.4 6.7 %collective-permute-done.12 = f32[64,256]{1,0:T(8,128)S(1)} collective-permute-done((f32[64,256]{1,0:T(8,128)S(1)}, f32[64,256]{1,0:T(8,128)S(1)}, u32[]{:S(2)}, u32[]{:S(2)}) %collective-permute-start.12) | collective-permute-done | bytes 65568 | tf_op jit(solution)/shard_map/ppermute | solution.py:185
  173.1 0.6 copy.11
  (38 shorter events, 0.2 us)
Async XLA Ops:
  7.2 27.8 %copy-start.3 = (bf16[512,256]{1,0:T(8,128)(2,1)S(1)}, bf16[512,256]{1,0:T(8,128)(2,1)}, u32[]{:S(2)}) copy-start(bf16[512,256]{1,0:T(8,128)(2,1)} %param.13) | copy-start | bytes 786436
  7.2 27.8 %copy-start.13 = (f32[256]{0:T(256)S(1)}, f32[256]{0:T(256)}, u32[]{:S(2)}) copy-start(f32[256]{0:T(256)} %param.10) | copy-start | bytes 3076
  7.2 27.8 %copy-start.2 = (bf16[512,256]{1,0:T(8,128)(2,1)S(1)}, bf16[512,256]{1,0:T(8,128)(2,1)}, u32[]{:S(2)}) copy-start(bf16[512,256]{1,0:T(8,128)(2,1)} %param.9) | copy-start | bytes 786436
  7.2 28.1 %copy-start.6 = (bf16[512,256]{1,0:T(8,128)(2,1)S(1)}, bf16[512,256]{1,0:T(8,128)(2,1)}, u32[]{:S(2)}) copy-start(bf16[512,256]{1,0:T(8,128)(2,1)} %param.7) | copy-start | bytes 786436
  8.6 13.9 %collective-permute-start = (f32[2,512]{1,0:T(2,128)S(1)}, f32[2,512]{1,0:T(2,128)S(1)}, u32[]{:S(2)}, u32[]{:S(2)}) collective-permute-start(f32[2,512]{1,0:T(2,128)S(1)} %pad_maximum_fusion.2), channel_id=1, source_target_pairs={{0,1},{1,0},{2,3},{3,2},{4,5},{5,4},{6,7},{7,6},{8,9},{9,8},{10,11... | collective-permute-start | bytes 12296 | tf_op jit(solution)/shard_map/ppermute | solution.py:39
  12.1 28.5 %all-to-all-start.1 = ((bf16[8,128,256]{2,1,0:T(8,128)(2,1)}), bf16[8,128,256]{2,1,0:T(8,128)(2,1)S(1)}, u32[]{:S(2)}, u32[]{:S(2)}) async-start(bf16[8,128,256]{2,1,0:T(8,128)(2,1)} %spread_kernel.1), calls=%async_computation.1 | async-start | bytes 1048576 | tf_op jit(solution)/shard_map/all_to_all | solution.py:17
  22.4 5.5 %collective-permute-start.1 = (f32[2,512]{1,0:T(2,128)S(1)}, f32[2,512]{1,0:T(2,128)S(1)}, u32[]{:S(2)}, u32[]{:S(2)}) collective-permute-start(f32[2,512]{1,0:T(2,128)S(1)} %fusion.19), channel_id=1, source_target_pairs={{0,2},{2,0},{4,6},{6,4},{1,3},{3,1},{5,7},{7,5},{8,10},{10,8},{12,... | collective-permute-start | bytes 12296 | tf_op jit(solution)/shard_map/ppermute | solution.py:39
  28.0 7.0 %collective-permute-start.2 = (f32[2,512]{1,0:T(2,128)S(1)}, f32[2,512]{1,0:T(2,128)S(1)}, u32[]{:S(2)}, u32[]{:S(2)}) collective-permute-start(f32[2,512]{1,0:T(2,128)S(1)} %fusion.22), channel_id=1, source_target_pairs={{0,4},{2,6},{4,0},{6,2},{1,5},{3,7},{5,1},{7,3},{8,12},{10,14},{12... | collective-permute-start | bytes 12296 | tf_op jit(solution)/shard_map/ppermute | solution.py:39
  42.1 29.2 %all-to-all-start = ((bf16[4,2,512,256]{3,2,1,0:T(8,128)(2,1)}), bf16[4,2,512,256]{3,2,1,0:T(8,128)(2,1)S(1)}, u32[]{:S(2)}, u32[]{:S(2)}) async-start(bf16[4,2,512,256]{3,2,1,0:T(8,128)(2,1)} %broadcast_in_dim.6), calls=%async_computation | async-start | bytes 4194304 | tf_op jit(solution)/shard_map/all_to_all | solution.py:17
  46.9 43.3 %all-gather.2.cloned.1.call-start = ((), (), s32[]{:S(2)}) async-start(), calls=%async_computation.5 | async-start | bytes 2359296 | tf_op jit(solution)/shard_map/all_gather | solution.py:144
  47.6 59.9 %copy-start.4 = (bf16[8,64,256]{2,1,0:T(8,128)(2,1)}, bf16[8,64,256]{2,1,0:T(8,128)(2,1)S(1)}, u32[]{:S(2)}) copy-start(bf16[8,64,256]{2,1,0:T(8,128)(2,1)S(1)} %get-tuple-element.12.rest_0_) | copy-start | bytes 786436
  47.6 94.9 %reduce-scatter.2.cloned.1.call-start = ((), (), s32[]{:S(2)}) async-start(), calls=%async_computation.6 | async-start | bytes 2469888 | tf_op jit(solution)/shard_map/reduce_scatter | solution.py:165
  47.7 11.3 %collective-permute-start.3 = (bf16[8,64,256]{2,1,0:T(8,128)(2,1)S(1)}, bf16[8,64,256]{2,1,0:T(8,128)(2,1)S(1)}, u32[]{:S(2)}, u32[]{:S(2)}) collective-permute-start(bf16[8,64,256]{2,1,0:T(8,128)(2,1)S(1)} %get-tuple-element.12.rest_0_), channel_id=1, source_target_pairs={{0,8},{8,16},{16,24},{24,32},{32,40},{40,48},{48,56},{56,0},{1,9},... | collective-permute-start | bytes 786440 | tf_op jit(solution)/shard_map/ppermute | solution.py:27
  59.0 45.4 %copy-start.7 = (bf16[8,64,256]{2,1,0:T(8,128)(2,1)}, bf16[8,64,256]{2,1,0:T(8,128)(2,1)S(1)}, u32[]{:S(2)}) copy-start(bf16[8,64,256]{2,1,0:T(8,128)(2,1)S(1)} %collective-permute-done.3.rest_1_) | copy-start | bytes 786436
  71.3 18.8 %copy-start = (bf16[4,2,512,256]{3,2,1,0:T(8,128)(2,1)}, bf16[4,2,512,256]{3,2,1,0:T(8,128)(2,1)S(1)}, u32[]{:S(2)}) copy-start(bf16[4,2,512,256]{3,2,1,0:T(8,128)(2,1)S(1)} %all-to-all-done.mine) | copy-start | bytes 6291460
  71.3 6.2 %collective-permute-start.4 = (bf16[4,2,512,256]{3,2,1,0:T(8,128)(2,1)S(1)}, bf16[4,2,512,256]{3,2,1,0:T(8,128)(2,1)}, u32[]{:S(2)}, u32[]{:S(2)}) collective-permute-start(bf16[4,2,512,256]{3,2,1,0:T(8,128)(2,1)S(1)} %all-to-all-done.mine), channel_id=1, source_target_pairs={{0,1},{1,0},{2,3},{3,2},{4,5},{5,4},{6,7},{7,6},{8,9},{9,8},{10,11... | collective-permute-start | bytes 6291464 | tf_op jit(solution)/shard_map/ppermute | solution.py:27
  97.1 1.0 copy-start.5
  99.7 36.4 %all-to-all-start.2 = ((bf16[4,512,512]{2,1,0:T(8,128)(2,1)}), bf16[4,512,512]{2,1,0:T(8,128)(2,1)S(1)}, u32[]{:S(2)}, u32[]{:S(2)}) async-start(bf16[4,512,512]{2,1,0:T(8,128)(2,1)} %broadcast_in_dim.7), calls=%async_computation.2 | async-start | bytes 4194304 | tf_op jit(solution)/shard_map/all_to_all | solution.py:17
  104.4 9.7 %collective-permute-start.5 = (bf16[8,64,256]{2,1,0:T(8,128)(2,1)S(1)}, bf16[8,64,256]{2,1,0:T(8,128)(2,1)S(1)}, u32[]{:S(2)}, u32[]{:S(2)}) collective-permute-start(bf16[8,64,256]{2,1,0:T(8,128)(2,1)S(1)} %collective-permute-done.3.rest_1_), channel_id=1, source_target_pairs={{0,8},{8,16},{16,24},{24,32},{32,40},{40,48},{48,56},{56,0},{1,9},... | collective-permute-start | bytes 786440 | tf_op jit(solution)/shard_map/ppermute | solution.py:27
  107.5 9.6 %collective-permute-start.8 = (bf16[8,64,256]{2,1,0:T(8,128)(2,1)S(1)}, bf16[8,64,256]{2,1,0:T(8,128)(2,1)S(1)}, u32[]{:S(2)}, u32[]{:S(2)}) collective-permute-start(bf16[8,64,256]{2,1,0:T(8,128)(2,1)S(1)} %get-tuple-element.12.rest_0_), channel_id=1, source_target_pairs={{0,56},{8,0},{16,8},{24,16},{32,24},{40,32},{48,40},{56,48},{1,57}... | collective-permute-start | bytes 786440 | tf_op jit(solution)/shard_map/ppermute | solution.py:27
  114.2 37.5 %copy-start.8 = (bf16[8,64,256]{2,1,0:T(8,128)(2,1)}, bf16[8,64,256]{2,1,0:T(8,128)(2,1)S(1)}, u32[]{:S(2)}) copy-start(bf16[8,64,256]{2,1,0:T(8,128)(2,1)S(1)} %collective-permute-done.5.rest_2_) | copy-start | bytes 786436
  114.2 10.5 %collective-permute-start.6 = (bf16[8,64,256]{2,1,0:T(8,128)(2,1)S(1)}, bf16[8,64,256]{2,1,0:T(8,128)(2,1)S(1)}, u32[]{:S(2)}, u32[]{:S(2)}) collective-permute-start(bf16[8,64,256]{2,1,0:T(8,128)(2,1)S(1)} %collective-permute-done.5.rest_2_), channel_id=1, source_target_pairs={{0,8},{8,16},{16,24},{24,32},{32,40},{40,48},{48,56},{56,0},{1,9},... | collective-permute-start | bytes 786440 | tf_op jit(solution)/shard_map/ppermute | solution.py:27
  117.1 34.6 %copy-start.9 = (bf16[8,64,256]{2,1,0:T(8,128)(2,1)}, bf16[8,64,256]{2,1,0:T(8,128)(2,1)S(1)}, u32[]{:S(2)}) copy-start(bf16[8,64,256]{2,1,0:T(8,128)(2,1)S(1)} %collective-permute-done.8.rest_7_) | copy-start | bytes 786436
  117.1 10.3 %collective-permute-start.9 = (bf16[8,64,256]{2,1,0:T(8,128)(2,1)S(1)}, bf16[8,64,256]{2,1,0:T(8,128)(2,1)S(1)}, u32[]{:S(2)}, u32[]{:S(2)}) collective-permute-start(bf16[8,64,256]{2,1,0:T(8,128)(2,1)S(1)} %collective-permute-done.8.rest_7_), channel_id=1, source_target_pairs={{0,56},{8,0},{16,8},{24,16},{32,24},{40,32},{48,40},{56,48},{1,57}... | collective-permute-start | bytes 786440 | tf_op jit(solution)/shard_map/ppermute | solution.py:27
  124.6 27.1 %copy-start.10 = (bf16[8,64,256]{2,1,0:T(8,128)(2,1)}, bf16[8,64,256]{2,1,0:T(8,128)(2,1)S(1)}, u32[]{:S(2)}) copy-start(bf16[8,64,256]{2,1,0:T(8,128)(2,1)S(1)} %collective-permute-done.6.rest_3_) | copy-start | bytes 786436
  124.6 9.5 %collective-permute-start.7 = (bf16[8,64,256]{2,1,0:T(8,128)(2,1)S(1)}, bf16[8,64,256]{2,1,0:T(8,128)(2,1)S(1)}, u32[]{:S(2)}, u32[]{:S(2)}) collective-permute-start(bf16[8,64,256]{2,1,0:T(8,128)(2,1)S(1)} %collective-permute-done.6.rest_3_), channel_id=1, source_target_pairs={{0,8},{8,16},{16,24},{24,32},{32,40},{40,48},{48,56},{56,0},{1,9},... | collective-permute-start | bytes 786440 | tf_op jit(solution)/shard_map/ppermute | solution.py:27
  127.4 24.3 %copy-start.11 = (bf16[8,64,256]{2,1,0:T(8,128)(2,1)}, bf16[8,64,256]{2,1,0:T(8,128)(2,1)S(1)}, u32[]{:S(2)}) copy-start(bf16[8,64,256]{2,1,0:T(8,128)(2,1)S(1)} %collective-permute-done.9.rest_6_) | copy-start | bytes 786436
  127.4 8.7 %collective-permute-start.10 = (bf16[8,64,256]{2,1,0:T(8,128)(2,1)S(1)}, bf16[8,64,256]{2,1,0:T(8,128)(2,1)}, u32[]{:S(2)}, u32[]{:S(2)}) collective-permute-start(bf16[8,64,256]{2,1,0:T(8,128)(2,1)S(1)} %collective-permute-done.9.rest_6_), channel_id=1, source_target_pairs={{0,56},{8,0},{16,8},{24,16},{32,24},{40,32},{48,40},{56,48},{1,57}... | collective-permute-start | bytes 786440 | tf_op jit(solution)/shard_map/ppermute | solution.py:27
  134.1 10.9 %copy-start.12 = (bf16[8,64,256]{2,1,0:T(8,128)(2,1)}, bf16[8,64,256]{2,1,0:T(8,128)(2,1)S(1)}, u32[]{:S(2)}) copy-start(bf16[8,64,256]{2,1,0:T(8,128)(2,1)S(1)} %collective-permute-done.7.rest_4_) | copy-start | bytes 786436
  136.1 15.6 %copy-start.1 = (bf16[4,512,512]{2,1,0:T(8,128)(2,1)}, bf16[4,512,512]{2,1,0:T(8,128)(2,1)S(1)}, u32[]{:S(2)}) copy-start(bf16[4,512,512]{2,1,0:T(8,128)(2,1)S(1)} %all-to-all-done.2.mine) | copy-start | bytes 6291460
  136.1 15.6 %collective-permute-start.11 = (bf16[4,512,512]{2,1,0:T(8,128)(2,1)S(1)}, bf16[4,512,512]{2,1,0:T(8,128)(2,1)}, u32[]{:S(2)}, u32[]{:S(2)}) collective-permute-start(bf16[4,512,512]{2,1,0:T(8,128)(2,1)S(1)} %all-to-all-done.2.mine), channel_id=1, source_target_pairs={{0,1},{1,0},{2,3},{3,2},{4,5},{5,4},{6,7},{7,6},{8,9},{9,8},{10,11... | collective-permute-start | bytes 6291464 | tf_op jit(solution)/shard_map/ppermute | solution.py:27
  145.0 17.5 %all-to-all-start.3 = ((bf16[8,72,256]{2,1,0:T(8,128)(2,1)}), bf16[8,72,256]{2,1,0:T(8,128)(2,1)S(1)}, u32[]{:S(2)}, u32[]{:S(2)}) async-start(bf16[8,72,256]{2,1,0:T(8,128)(2,1)} %pad_maximum_fusion.1), calls=%async_computation.4 | async-start | bytes 589824 | tf_op jit(solution)/shard_map/all_to_all | solution.py:17
  162.6 10.6 %collective-permute-start.12 = (f32[64,256]{1,0:T(8,128)S(1)}, f32[64,256]{1,0:T(8,128)S(1)}, u32[]{:S(2)}, u32[]{:S(2)}) collective-permute-start(f32[64,256]{1,0:T(8,128)S(1)} %slice.38), channel_id=1, source_target_pairs={{0,0},{1,64},{2,128},{3,192},{4,256},{5,320},{6,384},{7,448},{64,1... | collective-permute-start | bytes 196616 | tf_op jit(solution)/shard_map/ppermute | solution.py:185
Sparse Core Ops, SparseCore 0:
  50.3 39.7 all-gather.1
  97.3 45.2 reduce-scatter.1
